TPU v7x, 32 devices: a whole 2x2x4 slice. The times are simulated.
32 devices in a mesh: ep: 4 (over y, x), tp: 8 (over z, core).
Axes of the slice: x: 2, y: 2, z: 4, core: 2. Of those that a mesh axis runs over, the one named last changes fastest.
Arguments:
- pool_in: bfloat16 [16384, 1024], P(('ep', 'tp')), may hold values from -6 to 6
- pool_weight: bfloat16 [4, 256, 256], replicated, may hold values from -0.375 to 0.375
- pool_gain: float32 [1024], replicated, may hold values from 0.1 to 1.9
- out_weight: bfloat16 [1024, 2048], P('tp'), may hold values from -0.1875 to 0.1875
- mix_gain: float32 [2048], replicated, may hold values from 0.1 to 1.9
- expert_in: bfloat16 [1024, 2048], P('ep'), may hold values from -6 to 6
- routes: int32 [1024, 4], P('ep'), may hold values from 0 to 7, all different within a row; in each aligned block of 32 rows (0 to 31, 32 to 63, ...) at most 32 rows name the same one
- route_weight: float32 [1024, 4], P('ep'), may hold values from 0.1 to 1
- pre_gain: float32 [2048], replicated, may hold values from 0.1 to 1.9
- gate_weight: bfloat16 [8, 2048, 4096], P('ep', None, 'tp'), may hold values from -0.39648438 to 0.39648438
- up_weight: bfloat16 [8, 2048, 4096], P('ep', None, 'tp'), may hold values from -0.39648438 to 0.39648438
- down_weight: bfloat16 [8, 4096, 2048], P('ep', 'tp'), may hold values from -0.09375 to 0.09375
- post_gain: float32 [2048], replicated, may hold values from 0.1 to 1.9
Outputs:
- mix_out: bfloat16 [16384, 2048], P(('ep', 'tp'))
- expert_out: bfloat16 [1024, 2048], P(('ep', 'tp'))
Inputs may be any that keep to these rules, and one draw needn't show every extreme that they name: `routes`: each row names 4 different experts. In each aligned block of 32 rows no expert is named by more than 32 rows, a bound that some block reaches.
All inputs are finite; a program needn't handle non-finite values.
Results may differ from a plain program's by a relative error of at most 0.019.
Values may be sent and summed in bfloat16 or wider, within the bound.
No kernel may reach another device: no remote copies, remote signals or barrier semaphores. Data moves between devices by JAX's collectives and lax.ppermute only.
A program may use at most 128 MiB of HBM per device.

v0:
```python
import jax
import jax.numpy as jnp
from jax import lax
from jax.sharding import PartitionSpec as P

WINDOWS = (2, 4, 8, 16)
EPS = 1e-06
LIMIT = 7.0
ALPHA = 1.702


def shifted(block, axis, distance):
    devices = range(lax.axis_size(axis))
    route = [(i - distance, i) for i in devices if i - distance in devices]
    return lax.ppermute(block, axis, route)


def rms_scale(values, gain):
    mean_square = jnp.mean(values * values, axis=-1, keepdims=True)
    return values * lax.rsqrt(mean_square + EPS) * gain


def trailing_pool(padded, first_pos, rows):
    group = padded.shape[1] // 4
    position = first_pos + jnp.arange(rows, dtype=jnp.int32)
    pieces = []
    for which, window in enumerate(WINDOWS):
        channels = padded[:, which * group : (which + 1) * group]
        running = channels[16 : 16 + rows]
        for reach in range(2, window + 1):
            running = running + channels[17 - reach : 17 - reach + rows]
        count = jnp.minimum(position + 1, window).astype(jnp.float32)[:, None]
        pieces.append(running / count)
    pooled = jnp.concatenate(pieces, axis=1)
    return (pooled - padded[16:]).astype(jnp.bfloat16)


def selection(block_routes, experts, capacity):
    flat = block_routes.reshape(-1)
    onehot = (flat[:, None] == jnp.arange(experts, dtype=jnp.int32)[None, :]).astype(jnp.int32)
    earlier = jnp.cumsum(onehot, axis=0) - onehot
    rank = jnp.sum(earlier * onehot, axis=1)
    slots = (flat * capacity + rank).reshape(block_routes.shape)
    return (
        slots[:, :, None] == jnp.arange(experts * capacity, dtype=jnp.int32)[None, None, :]
    ).astype(jnp.bfloat16)


def clamped_unit(gate, up):
    gate = jnp.minimum(gate, LIMIT)
    up = jnp.clip(up, -LIMIT, LIMIT)
    return (up + 1.0) * gate * jax.nn.sigmoid(ALPHA * gate)


def hidden_rows(arrived, gate_weight, up_weight):
    gate = jnp.einsum("necd,edf->necf", arrived, gate_weight, preferred_element_type=jnp.float32)
    up = jnp.einsum("necd,edf->necf", arrived, up_weight, preferred_element_type=jnp.float32)
    return clamped_unit(gate, up).astype(jnp.bfloat16)


def body(
    pool_in,
    pool_weight,
    pool_gain,
    out_weight,
    mix_gain,
    expert_in,
    routes,
    route_weight,
    pre_gain,
    gate_weight,
    up_weight,
    down_weight,
    post_gain,
):
    rows, channels = pool_in.shape
    width = out_weight.shape[1]
    rim = shifted(pool_in[rows - 16 :], ("ep", "tp"), 1)
    padded = jnp.concatenate([rim, pool_in], axis=0).astype(jnp.float32)
    first_pos = (lax.axis_index("ep") * lax.axis_size("tp") + lax.axis_index("tp")) * rows
    diff = trailing_pool(padded, first_pos, rows)
    mixed = jnp.einsum(
        "sgc,gcd->sgd",
        diff.reshape(rows, 4, channels // 4),
        pool_weight,
        preferred_element_type=jnp.float32,
    )
    mixed = (mixed.reshape(rows, channels) * pool_gain).astype(jnp.bfloat16)
    projected = jnp.dot(
        mixed,
        lax.all_gather(out_weight, "tp", axis=0, tiled=True),
        preferred_element_type=jnp.float32,
    )
    mix_out = rms_scale(projected, mix_gain).astype(jnp.bfloat16)
    ep_count = lax.axis_size("ep")
    tp_count = lax.axis_size("tp")
    tp_place = lax.axis_index("tp")
    local_experts = gate_weight.shape[0]
    experts = local_experts * ep_count
    tokens_here, choose = routes.shape
    block_tokens = tokens_here // tp_count
    capacity = 2 * block_tokens * choose // experts
    block_routes = lax.dynamic_slice_in_dim(routes, tp_place * block_tokens, block_tokens, 0)
    block_rows = lax.dynamic_slice_in_dim(expert_in, tp_place * block_tokens, block_tokens, 0)
    normed = rms_scale(block_rows.astype(jnp.float32), pre_gain).astype(jnp.bfloat16)
    own_picks = selection(block_routes, experts, capacity)
    buffer = jnp.einsum(
        "ts,td->sd", jnp.sum(own_picks, axis=1), normed, preferred_element_type=jnp.float32
    ).astype(jnp.bfloat16)
    buffer = buffer.reshape(ep_count, local_experts, capacity, width)
    arrived = lax.all_to_all(buffer, "ep", split_axis=0, concat_axis=0, tiled=True)
    hidden_all = hidden_rows(
        lax.all_gather(arrived, "tp", axis=0, tiled=True), gate_weight, up_weight
    )
    summed = lax.psum_scatter(
        jnp.einsum(
            "necf,efd->necd", hidden_all, down_weight, preferred_element_type=jnp.float32
        ).astype(jnp.bfloat16),
        "tp",
        scatter_dimension=0,
        tiled=True,
    )
    returned = lax.all_to_all(summed, "ep", split_axis=0, concat_axis=0, tiled=True)
    returned = returned.reshape(experts * capacity, width)
    per_route = jnp.einsum("tks,sd->tkd", own_picks, returned, preferred_element_type=jnp.float32)
    weights = lax.dynamic_slice_in_dim(route_weight, tp_place * block_tokens, block_tokens, 0)
    combined = jnp.sum(per_route * weights[:, :, None], axis=1)
    expert_out = rms_scale(combined, post_gain).astype(jnp.bfloat16)
    return (mix_out, expert_out)


def solution(mesh):
    return jax.shard_map(
        body,
        mesh=mesh,
        in_specs=(
            P(("ep", "tp"), None),
            P(),
            P(),
            P("tp", None),
            P(),
            P("ep", None),
            P("ep", None),
            P("ep", None),
            P(),
            P("ep", None, "tp"),
            P("ep", None, "tp"),
            P("ep", "tp", None),
            P(),
        ),
        out_specs=(P(("ep", "tp"), None), P(("ep", "tp"), None)),
        check_vma=False,
    )
```

profile of v0, /device:TPU:0, one launch (start us, length us, event | category | flops | bytes accessed | tf_op | source)
XLA Modules:
  0.0 364.8 jit_solution(16986653693718660319)
XLA Ops:
  7.2 0.0 copy-start
  7.2 0.0 all-gather.5.cloned.1.call-start
  7.2 0.8 constant_dynamic-slice_fusion.1
  8.0 0.1 copy.38
  8.1 0.1 eq.28
  8.2 0.1 fusion.36
  8.3 0.2 reduce_window_sum.11
  8.5 0.2 select_reduce_fusion
  8.7 0.1 reduce_sum.61
  8.8 0.1 copy.29
  8.9 0.1 fusion.34
  9.0 1.0 fusion.26
  10.0 1.4 convolution_convert_fusion
  11.5 19.1 %all_to_all.10 = bf16[4,2,32,2048]{3,2,1,0:T(8,128)(2,1)S(1)} all-to-all(bf16[4,2,32,2048]{3,2,1,0:T(8,128)(2,1)S(1)} %bitcast.56), channel_id=1, replica_groups=mesh['ep'=4,'tp'=8] {'ep'}, dimensions={0} | all-to-all | bytes 2097152 | tf_op jit(solution)/shard_map/all_to_all | solution.py:111
  30.6 1.0 copy.30
  31.6 0.0 all-gather.5.cloned.1.call-update
  31.6 0.0 all-gather.3.cloned.1.call-start
  31.7 0.7 all-gather.3.cloned.1.call-update
  32.4 0.0 all-reduce.3.cloned.1.call-start
  32.4 81.1 %all-gather.5.cloned.1.call-done = bf16[32,2,32,2048]{3,2,0,1:T(8,128)(2,1)} async-done(((bf16[4,2,32,2048]{3,2,0,1:T(8,128)(2,1)}), bf16[32,2,32,2048]{3,2,0,1:T(8,128)(2,1)}) %all-gather.5.cloned.1.call-update) | async-done | bytes 8388624 | tf_op jit(solution)/shard_map/all_gather | solution.py:113
  113.6 11.0 %fusion.3 = f32[2,32,32,512]{3,2,1,0:T(8,128)} fusion(bf16[32,2,32,2048]{3,2,0,1:T(8,128)(2,1)} %all-gather.5.cloned.1.call-done, bf16[2,2048,512]{2,1,0:T(8,128)(2,1)} %param.23), kind=kOutput, calls=%fused_computation.4 | convolution fusion | flops 4294967296 | bytes 16777216 | tf_op jit(solution)/shard_map/necd,edf->necf/dot_general | solution.py:57
  124.6 15.9 %convert_bitcast_fusion = bf16[32,2,32,2048]{3,2,0,1:T(8,128)(2,1)} fusion(bf16[2,512,2048]{2,1,0:T(8,128)(2,1)} %param.24, f32[2,32,32,512]{3,2,1,0:T(8,128)} %fusion.3, bf16[32,2,32,2048]{3,2,0,1:T(8,128)(2,1)} %all-gather.5.cloned.1.call-done, bf16[2,2048,512]{2,1,0:T(8,128)(2,1)} %param.22), kind=kOutput, calls=%fused_computation | convolution fusion | flops 8604614656 | bytes 29360128 | tf_op jit(solution)/shard_map/necf,efd->necd/dot_general | solution.py:116
  140.5 0.0 all-reduce.3.cloned.1.call-update
  140.5 1.2 copy-done.1
  141.7 2.3 collective-permute-start
  144.1 0.0 copy-done.5
  144.1 0.1 constant_dynamic-slice_fusion
  144.2 0.0 copy-done.6
  144.2 0.6 dynamic-slice
  145.4 0.0 collective-permute-done
  145.4 0.3 maximum_convert_fusion
  145.7 0.6 fusion.22
  146.3 0.6 fusion.25
  147.0 0.0 copy-start.4
  147.0 0.4 fusion.7
  147.5 0.5 fusion.19
  148.0 0.2 fusion.8
  148.2 12.7 %all-gather.3.cloned.1.call-done = bf16[1024,2048]{1,0:T(8,128)(2,1)} async-done(((bf16[128,2048]{1,0:T(8,128)(2,1)}), bf16[1024,2048]{1,0:T(8,128)(2,1)}) %all-gather.3.cloned.1.call-update) | async-done | bytes 4194320 | tf_op jit(solution)/shard_map/all_gather | solution.py:91
  160.9 6.6 %multiply_reduce_fusion = (f32[512]{0:T(512)S(1)}, f32[512,2048]{1,0:T(8,128)}) fusion(bf16[512,1024]{0,1:T(8,128)(2,1)S(1)} %fusion.8, bf16[1024,2048]{1,0:T(8,128)(2,1)} %all-gather.3.cloned.1.call-done), kind=kOutput, calls=%fused_computation.8 | convolution fusion | flops 2149580288 | bytes 9439232 | tf_op jit(solution)/shard_map/dot_general | solution.py:89
  167.5 170.1 %all-reduce.3.cloned.1.call-done = bf16[32,2,32,2048]{3,2,0,1:T(8,128)(2,1)} async-done(((bf16[32,2,32,2048]{3,2,0,1:T(8,128)(2,1)}), bf16[32,2,32,2048]{3,2,0,1:T(8,128)(2,1)}) %all-reduce.3.cloned.1.call-update) | async-done | bytes 8388624
  337.6 1.3 constant_dynamic-slice_fusion.2
  338.9 1.1 copy.31
  339.9 3.6 all-to-all-start.1
  343.6 3.9 %multiply_convert_fusion.1 = bf16[512,2048]{1,0:T(8,128)(2,1)} fusion(f32[512,2048]{1,0:T(8,128)} %get-tuple-element.6, f32[2048]{0:T(1024)S(1)} %copy-done.2, f32[512]{0:T(512)S(1)} %add_rsqrt_fusion), kind=kLoop, calls=%fused_computation.7 | loop fusion | flops 3145728 | bytes 6301696 | tf_op jit(solution)/shard_map/convert_element_type | solution.py:94
  347.5 9.5 %all-to-all-done.1 = bf16[4,2,32,2048]{3,2,1,0:T(8,128)(2,1)S(1)} async-done(((bf16[4,2,32,2048]{3,2,1,0:T(8,128)(2,1)}), bf16[4,2,32,2048]{3,2,1,0:T(8,128)(2,1)S(1)}, u32[]{:S(2)}, u32[]{:S(2)}) %all-to-all-start.1) | async-done | bytes 1048608 | tf_op jit(solution)/shard_map/all_to_all | solution.py:123
  357.0 0.3 fusion.18
  357.4 0.1 multiply_reduce_fusion.1
  357.5 0.8 multiply_convert_fusion.2
  (16 shorter events, 0.1 us)
Async XLA Ops:
  7.2 140.3 %copy-start = (bf16[4,256,256]{2,1,0:T(8,128)(2,1)S(1)}, bf16[4,256,256]{2,1,0:T(8,128)(2,1)}, u32[]{:S(2)}) copy-start(bf16[4,256,256]{2,1,0:T(8,128)(2,1)} %param.14) | copy-start | bytes 1572868
  7.2 106.4 %all-gather.5.cloned.1.call-start = ((), (), s32[]{:S(2)}) async-start(), calls=%async_computation.3 | async-start | bytes 9437184 | tf_op jit(solution)/shard_map/all_gather | solution.py:113
  31.6 129.2 %all-gather.3.cloned.1.call-start = ((), (), s32[]{:S(2)}) async-start(), calls=%async_computation.2 | async-start | bytes 4718592 | tf_op jit(solution)/shard_map/all_gather | solution.py:91
  32.4 305.2 %all-reduce.3.cloned.1.call-start = ((), (), s32[]{:S(2)}) async-start(), calls=%async_computation.4 | async-start | bytes 16777216
  140.5 1.2 copy-start.1
  140.5 3.6 copy-start.5
  140.5 3.7 %copy-start.6 = (u32[32]{0:T(128)S(1)}, u32[32]{0:T(128)}, u32[]{:S(2)}) copy-start(u32[32]{0:T(128)} %constant.59) | copy-start | bytes 388
  141.7 3.7 %collective-permute-start = (bf16[16,1024]{1,0:T(8,128)(2,1)S(1)}, bf16[16,1024]{1,0:T(8,128)(2,1)S(1)}, u32[]{:S(2)}, u32[]{:S(2)}) collective-permute-start(bf16[16,1024]{1,0:T(8,128)(2,1)S(1)} %slice.130), channel_id=1, source_target_pairs={{0,1},{1,2},{2,3},{3,4},{4,5},{5,6},{6,7},{7,8},{8,9},{9,10},{10,1... | collective-permute-start | bytes 98312 | tf_op jit(solution)/shard_map/ppermute | solution.py:15
  147.0 1.0 copy-start.4
  167.5 176.1 %copy-start.2 = (f32[2048]{0:T(1024)S(1)}, f32[2048]{0:T(1024)}, u32[]{:S(2)}) copy-start(f32[2048]{0:T(1024)} %param.17) | copy-start | bytes 24580
  339.9 17.1 %all-to-all-start.1 = ((bf16[4,2,32,2048]{3,2,1,0:T(8,128)(2,1)}), bf16[4,2,32,2048]{3,2,1,0:T(8,128)(2,1)S(1)}, u32[]{:S(2)}, u32[]{:S(2)}) async-start(bf16[4,2,32,2048]{3,2,1,0:T(8,128)(2,1)} %copy.31), calls=%async_computation.1 | async-start | bytes 2097152 | tf_op jit(solution)/shard_map/all_to_all | solution.py:123
  343.6 13.9 %copy-start.3 = (f32[2048]{0:T(1024)S(1)}, f32[2048]{0:T(1024)}, u32[]{:S(2)}) copy-start(f32[2048]{0:T(1024)} %param.25) | copy-start | bytes 24580
Sparse Core Ops, SparseCore 0:
  31.8 81.7 all-gather.4
  115.1 45.6 all-gather.2
  163.3 174.2 all-reduce.2
where the time goes:
time: 365 us
  waiting for transfers between devices  274 us (75%)
  matrix products  35.8 us (10%)
  blocking collectives  19.1 us (5%)
  between operations  14.6 us (4%)
  other arithmetic  8.59 us (2%)
  local copies, waits for them, and re-layouts  6.46 us (2%)
  starting transfers between devices  6.08 us (2%)
    unnamed x4, waiting for transfers between devices  171 us
    all_gather x1, waiting for transfers between devices, body(): lax.all_gather(arrived, 'tp', axis=0, tiled=True)  81.1 us
    all_to_all x1, blocking collectives, body(): lax.all_to_all(buffer, 'ep', split_axis=0, concat_axis=0, tiled=True)  19.1 us
    dot_general x1, matrix products, body(): jnp.einsum('necf,efd->necd', hidden_all, down_weight, preferred_element_t...  15.9 us
    all_gather x1, waiting for transfers between devices, body(): lax.all_gather(out_weight, 'tp', axis=0, tiled=True)  12.7 us
    dot_general x1, matrix products, hidden_rows(): jnp.einsum('necd,edf->necf', arrived, up_weight, preferred_element_type=j...  11 us
    all_to_all x1, waiting for transfers between devices, body(): lax.all_to_all(summed, 'ep', split_axis=0, concat_axis=0, tiled=True)  9.5 us
  transfers between devices with their start and end apart: 5, of which 4 were waited for; matrix products, arithmetic and copies ran while one was open for 11% of the time, Pallas kernels for 0%

commit v1 on v0

--- a/solution.py
+++ b/solution.py
@@ -1,12 +1,16 @@
 import jax
 import jax.numpy as jnp
 from jax import lax
+from jax.experimental import pallas as pl
+from jax.experimental.pallas import tpu as pltpu
 from jax.sharding import PartitionSpec as P
+
 
 WINDOWS = (2, 4, 8, 16)
 EPS = 1e-06
 LIMIT = 7.0
 ALPHA = 1.702
+CORES = 2
 
 
 def shifted(block, axis, distance):
@@ -15,24 +19,32 @@
     return lax.ppermute(block, axis, route)
 
 
+def moved(block, target):
+    eps, tps = lax.axis_size("ep"), lax.axis_size("tp")
+    route = []
+    for e in range(eps):
+        for t in range(tps):
+            te, tt = target(e, t)
+            route.append((e * tps + t, te * tps + tt))
+    return lax.ppermute(block, ("ep", "tp"), route)
+
+
+def to_core(block):
+    return moved(block, lambda e, t: (e, t ^ 1))
+
+
+def to_group(block, mask):
+    return moved(block, lambda e, t: (e ^ mask, t))
+
+
+def to_chip(block, step):
+    chips = lax.axis_size("tp") // CORES
+    return moved(block, lambda e, t: (e, (t // CORES + step) % chips * CORES + t % CORES))
+
+
 def rms_scale(values, gain):
     mean_square = jnp.mean(values * values, axis=-1, keepdims=True)
     return values * lax.rsqrt(mean_square + EPS) * gain
-
-
-def trailing_pool(padded, first_pos, rows):
-    group = padded.shape[1] // 4
-    position = first_pos + jnp.arange(rows, dtype=jnp.int32)
-    pieces = []
-    for which, window in enumerate(WINDOWS):
-        channels = padded[:, which * group : (which + 1) * group]
-        running = channels[16 : 16 + rows]
-        for reach in range(2, window + 1):
-            running = running + channels[17 - reach : 17 - reach + rows]
-        count = jnp.minimum(position + 1, window).astype(jnp.float32)[:, None]
-        pieces.append(running / count)
-    pooled = jnp.concatenate(pieces, axis=1)
-    return (pooled - padded[16:]).astype(jnp.bfloat16)
 
 
 def selection(block_routes, experts, capacity):
@@ -58,40 +70,10 @@
     return clamped_unit(gate, up).astype(jnp.bfloat16)
 
 
-def body(
-    pool_in,
-    pool_weight,
-    pool_gain,
-    out_weight,
-    mix_gain,
-    expert_in,
-    routes,
-    route_weight,
-    pre_gain,
-    gate_weight,
-    up_weight,
-    down_weight,
-    post_gain,
+def routed_experts(
+    expert_in, routes, route_weight, pre_gain, gate_weight, up_weight, down_weight, post_gain
 ):
-    rows, channels = pool_in.shape
-    width = out_weight.shape[1]
-    rim = shifted(pool_in[rows - 16 :], ("ep", "tp"), 1)
-    padded = jnp.concatenate([rim, pool_in], axis=0).astype(jnp.float32)
-    first_pos = (lax.axis_index("ep") * lax.axis_size("tp") + lax.axis_index("tp")) * rows
-    diff = trailing_pool(padded, first_pos, rows)
-    mixed = jnp.einsum(
-        "sgc,gcd->sgd",
-        diff.reshape(rows, 4, channels // 4),
-        pool_weight,
-        preferred_element_type=jnp.float32,
-    )
-    mixed = (mixed.reshape(rows, channels) * pool_gain).astype(jnp.bfloat16)
-    projected = jnp.dot(
-        mixed,
-        lax.all_gather(out_weight, "tp", axis=0, tiled=True),
-        preferred_element_type=jnp.float32,
-    )
-    mix_out = rms_scale(projected, mix_gain).astype(jnp.bfloat16)
+    width = expert_in.shape[1]
     ep_count = lax.axis_size("ep")
     tp_count = lax.axis_size("tp")
     tp_place = lax.axis_index("tp")
@@ -125,13 +107,370 @@
     per_route = jnp.einsum("tks,sd->tkd", own_picks, returned, preferred_element_type=jnp.float32)
     weights = lax.dynamic_slice_in_dim(route_weight, tp_place * block_tokens, block_tokens, 0)
     combined = jnp.sum(per_route * weights[:, :, None], axis=1)
-    expert_out = rms_scale(combined, post_gain).astype(jnp.bfloat16)
+    return rms_scale(combined, post_gain).astype(jnp.bfloat16)
+
+
+def seat():
+    place = lax.axis_index("tp")
+    return lax.div(place, CORES), lax.rem(place, CORES)
+
+
+VMEM = pl.BlockSpec(memory_space=pltpu.VMEM)
+
+
+def normed_rows(source, gain):
+    return rms_scale(source[...].astype(jnp.float32), gain[...]).astype(jnp.bfloat16)
+
+
+def fill_hidden(hidden, expert, first, normed, share, gate_weight, up_weight):
+    units = gate_weight.shape[1]
+    lanes = lax.broadcasted_iota(jnp.int32, share.shape, 1)
+    gate = jnp.dot(normed[...], gate_weight[...], preferred_element_type=jnp.float32)
+    up = jnp.dot(normed[...], up_weight[...], preferred_element_type=jnp.float32)
+    scale = jnp.sum(jnp.where(lanes == first + expert, share, 0.0), axis=1, keepdims=True)
+    hidden[:, expert * units : (expert + 1) * units] = (clamped_unit(gate, up) * scale).astype(
+        jnp.bfloat16
+    )
+
+
+def store_halves(hidden, down_weight, total, core, outputs):
+    result = jnp.dot(hidden[...], down_weight[...], preferred_element_type=jnp.float32)
+    total[...] = result.astype(jnp.bfloat16).reshape(total.shape)
+    groups = len(outputs) // 2
+    chips = total.shape[0] // (CORES * groups)
+    block = total.shape[1]
+    for group in range(groups):
+        for chip in range(chips):
+            start = CORES * (group * chips + chip)
+            rows_of = slice(chip * block, (chip + 1) * block)
+            outputs[2 * group][rows_of, :] = total[start + core]
+            outputs[2 * group + 1][rows_of, :] = total[start + 1 - core]
+
+
+def own_kernel(
+    gain_ref, rows_ref, share_ref, gate_in, up_in, down_in,
+    kept_ref, sent_ref, gate_ref, up_ref, down_ref, normed, hidden, total, sems,
+):
+    local, _, units = gate_ref.shape
+    first = lax.axis_index("ep") * local
+    loads = []
+    for expert in range(local):
+        loads.append(pltpu.make_async_copy(gate_in.at[expert], gate_ref.at[expert], sems.at[len(loads)]))
+        loads.append(pltpu.make_async_copy(up_in.at[expert], up_ref.at[expert], sems.at[len(loads)]))
+    for expert in range(local):
+        part = pl.ds(expert * units, units)
+        loads.append(pltpu.make_async_copy(down_in.at[part], down_ref.at[part], sems.at[len(loads)]))
+    for load in loads:
+        load.start()
+    normed[...] = normed_rows(rows_ref, gain_ref)
+    share = jnp.transpose(share_ref[...])
+    for expert in range(local):
+        loads[2 * expert].wait()
+        loads[2 * expert + 1].wait()
+        fill_hidden(
+            hidden, expert, first, normed, share, gate_ref.at[expert], up_ref.at[expert]
+        )
+    for load in loads[2 * local :]:
+        load.wait()
+    store_halves(hidden, down_ref, total, seat()[1], (kept_ref, sent_ref))
+
+
+def own_partial(rows, share, gain, gate_weight, up_weight, down_weight, block):
+    tokens, width = rows.shape
+    local, _, units = gate_weight.shape
+    half = jax.ShapeDtypeStruct((tokens // 2, width), jnp.bfloat16)
+    down_weight = down_weight.reshape(-1, width)
+    held = [pltpu.VMEM(w.shape, w.dtype) for w in (gate_weight, up_weight, down_weight)]
+    hbm = pl.BlockSpec(memory_space=pltpu.HBM)
+    return pl.pallas_call(
+        own_kernel,
+        in_specs=[VMEM] * 3 + [hbm] * 3,
+        out_specs=[VMEM] * 5,
+        out_shape=[half, half] + held,
+        scratch_shapes=[
+            pltpu.VMEM((tokens, width), jnp.bfloat16),
+            pltpu.VMEM((tokens, local * units), jnp.bfloat16),
+            pltpu.VMEM((tokens // block, block, width), jnp.bfloat16),
+            pltpu.SemaphoreType.DMA((3 * local,)),
+        ],
+        compiler_params=pltpu.CompilerParams(vmem_limit_bytes=10 << 20),
+        cost_estimate=pl.CostEstimate(
+            flops=6 * tokens * width * local * units,
+            bytes_accessed=4 * tokens * width + 6 * local * units * width,
+            transcendentals=tokens * local * units,
+        ),
+        name="own",
+    )(
+        gain.reshape(1, width), rows, share,
+        *(
+            pltpu.with_memory_space_constraint(w, pltpu.HBM)
+            for w in (gate_weight, up_weight, down_weight)
+        ),
+    )
+
+
+def expert_kernel(gain_ref, gate_ref, up_ref, down_ref, *refs, groups):
+    inputs, outputs = refs[: 3 * groups], refs[3 * groups : 5 * groups]
+    normed, hidden, total = refs[5 * groups :]
+    first, core = lax.axis_index("ep") * gate_ref.shape[0], seat()[1]
+    half = inputs[0].shape[0]
+    shares = []
+    for group in range(groups):
+        mine_ref, other_ref, share_ref = inputs[3 * group : 3 * group + 3]
+        for source, which in ((mine_ref, core), (other_ref, 1 - core)):
+            start = pl.multiple_of((2 * group + which) * half, half)
+            normed[pl.ds(start, half), :] = normed_rows(source, gain_ref)
+        shares.append(jnp.transpose(share_ref[...]))
+    share = jnp.concatenate(shares, axis=0)
+    for expert in range(gate_ref.shape[0]):
+        fill_hidden(hidden, expert, first, normed, share, gate_ref.at[expert], up_ref.at[expert])
+    store_halves(hidden, down_ref, total, core, outputs)
+
+
+def expert_partial(chunks, gain, gate_weight, up_weight, down_weight, block):
+    groups = len(chunks)
+    half, width = chunks[0][0].shape
+    rows = 2 * half * groups
+    local, _, units = gate_weight.shape
+    inputs = [array for chunk in chunks for array in chunk]
+    outputs = pl.pallas_call(
+        lambda *refs: expert_kernel(*refs, groups=groups),
+        in_specs=[VMEM] * (4 + len(inputs)),
+        out_specs=[VMEM] * (2 * groups),
+        out_shape=[jax.ShapeDtypeStruct((half, width), jnp.bfloat16)] * (2 * groups),
+        scratch_shapes=[
+            pltpu.VMEM((rows, width), jnp.bfloat16),
+            pltpu.VMEM((rows, local * units), jnp.bfloat16),
+            pltpu.VMEM((rows // block, block, width), jnp.bfloat16),
+        ],
+        compiler_params=pltpu.CompilerParams(vmem_limit_bytes=16 << 20),
+        cost_estimate=pl.CostEstimate(
+            flops=6 * rows * width * local * units,
+            bytes_accessed=4 * rows * width,
+            transcendentals=rows * local * units,
+        ),
+        name="experts",
+    )(gain.reshape(1, width), gate_weight, up_weight, down_weight, *inputs)
+    return [(outputs[2 * g], outputs[2 * g + 1]) for g in range(groups)]
+
+
+def spread_kernel(early_ref, late_ref, own_ref, *out_refs):
+    chips = early_ref.shape[0]
+    for step in range(chips):
+        at = lax.rem(seat()[0] + step, chips)
+        part = early_ref[at] + late_ref[at].astype(jnp.float32)
+        if step:
+            out_refs[step - 1][...] = part.astype(jnp.bfloat16)
+        else:
+            own_ref[...] = part
+
+
+def spread(early, late):
+    chips, block, width = early.shape
+    return pl.pallas_call(
+        spread_kernel,
+        in_specs=[VMEM, VMEM],
+        out_specs=[VMEM] * chips,
+        out_shape=[jax.ShapeDtypeStruct((block, width), jnp.float32)]
+        + [jax.ShapeDtypeStruct((block, width), jnp.bfloat16)] * (chips - 1),
+        cost_estimate=pl.CostEstimate(
+            flops=early.size, bytes_accessed=8 * early.size, transcendentals=0
+        ),
+        compiler_params=pltpu.CompilerParams(vmem_limit_bytes=4 << 20),
+        name="spread",
+    )(early, late)
+
+
+def finish_kernel(gain_ref, own_ref, *refs):
+    total = own_ref[...]
+    for ref in refs[:-1]:
+        total = total + ref[...].astype(jnp.float32)
+    refs[-1][...] = rms_scale(total, gain_ref[...]).astype(jnp.bfloat16)
+
+
+def finish(gain, own, parts):
+    return pl.pallas_call(
+        finish_kernel,
+        in_specs=[VMEM] * (2 + len(parts)),
+        out_specs=VMEM,
+        out_shape=jax.ShapeDtypeStruct(own.shape, jnp.bfloat16),
+        compiler_params=pltpu.CompilerParams(vmem_limit_bytes=4 << 20),
+        name="finish",
+    )(gain.reshape(1, -1), own, *parts)
+
+
+def dense_experts(
+    expert_in, routes, route_weight, pre_gain, gate_weight, up_weight, down_weight, post_gain
+):
+    tokens, width = expert_in.shape
+    groups = lax.axis_size("ep")
+    chips = lax.axis_size("tp") // CORES
+    block = tokens // lax.axis_size("tp")
+    local = gate_weight.shape[0]
+    experts = local * groups
+    place = lax.axis_index("tp")
+    core = place % CORES
+    masks = range(1, groups)
+    mine = lax.dynamic_slice_in_dim(expert_in, core * (tokens // CORES), tokens // CORES, 0)
+    mine_from = {}
+    for m in masks:
+        mine_from[m] = to_group(mine, m)
+    numbers = jnp.arange(-(-experts // 8) * 8, dtype=jnp.int32)
+    share = jnp.sum(
+        jnp.where(routes.T[None] == numbers[:, None, None], route_weight.T[None], 0.0), axis=1
+    )
+    share_from = {}
+    for m in masks:
+        share_from[m] = to_group(share, m)
+    kept, sent, *held = own_partial(
+        expert_in, share, pre_gain, gate_weight, up_weight, down_weight, block
+    )
+    weights = (pre_gain, *held, block)
+    early = kept.astype(jnp.float32) + to_core(sent).astype(jnp.float32)
+    near = [m for m in masks if m & (m - 1) == 0]
+    far = [m for m in masks if m & (m - 1) != 0]
+    returned = {}
+    for batch in (near, far):
+        chunks = []
+        for m in batch:
+            chunks.append((mine_from[m], to_core(mine_from[m]), share_from[m]))
+        results = expert_partial(chunks, *weights)
+        for m, (kept, sent) in zip(batch, results):
+            partner = to_core(sent)
+            joined = (kept.astype(jnp.float32) + partner.astype(jnp.float32)).astype(jnp.bfloat16)
+            returned[m] = to_group(joined, m)
+    for m in masks[:-1]:
+        early = early + returned[m].astype(jnp.float32)
+    early = lax.optimization_barrier(early)
+    own, *pieces = spread(
+        early.reshape(chips, block, width),
+        returned[masks[-1]].reshape(chips, block, width),
+    )
+    parts = []
+    for step in range(1, chips):
+        parts.append(to_chip(pieces[step - 1], step))
+    return finish(post_gain, own, parts)
+
+
+def mix_kernel(rim_ref, rows_ref, weight_ref, gain_ref, out_ref):
+    rows = rows_ref.shape[0]
+    group = rows_ref.shape[1] // len(WINDOWS)
+    spare = rim_ref.shape[0]
+    device = lax.axis_index("ep") * lax.axis_size("tp") + lax.axis_index("tp")
+    position = device * rows + lax.broadcasted_iota(jnp.int32, (rows, 1), 0)
+    for which, window in enumerate(WINDOWS):
+        cols = slice(which * group, (which + 1) * group)
+        values = jnp.concatenate([rim_ref[:, cols], rows_ref[:, cols]], axis=0)
+        values = values.astype(jnp.float32)
+        running, reach = values, 1
+        while reach < window:
+            running = running + pltpu.roll(running, reach, 0)
+            reach *= 2
+        count = jnp.minimum(position + 1, window).astype(jnp.float32)
+        diff = running[spare:] / count - values[spare:]
+        mixed = jnp.dot(
+            diff.astype(jnp.bfloat16), weight_ref[which], preferred_element_type=jnp.float32
+        )
+        out_ref[:, cols] = (mixed * gain_ref[:, cols]).astype(jnp.bfloat16)
+
+
+def mix(rim, rows, weight, gain):
+    return pl.pallas_call(
+        mix_kernel,
+        in_specs=[VMEM] * 4,
+        out_specs=VMEM,
+        out_shape=jax.ShapeDtypeStruct(rows.shape, jnp.bfloat16),
+        compiler_params=pltpu.CompilerParams(vmem_limit_bytes=6 << 20),
+        cost_estimate=pl.CostEstimate(
+            flops=2 * rows.size * weight.shape[1],
+            bytes_accessed=4 * rows.size,
+            transcendentals=0,
+        ),
+        name="mix",
+    )(rim, rows, weight, gain.reshape(1, -1))
+
+
+def project_kernel(mixed_ref, gain_ref, *refs):
+    weights, out_ref, joined = refs[:-2], refs[-2], refs[-1]
+
+    @pl.when(pl.program_id(0) == 0)
+    def _():
+        depth = weights[0].shape[0]
+        chip, core = seat()
+        chips = len(weights) // CORES
+        for k, weight in enumerate(weights):
+            source = lax.rem(chip + chips - k // CORES, chips) * CORES
+            shard = source + (core if k % CORES == 0 else 1 - core)
+            joined[pl.ds(pl.multiple_of(shard * depth, depth), depth), :] = weight[...]
+
+    total = jnp.dot(mixed_ref[...], joined[...], preferred_element_type=jnp.float32)
+    out_ref[...] = rms_scale(total, gain_ref[...]).astype(jnp.bfloat16)
+
+
+def project(mixed, gain, weights):
+    rows, depth = mixed.shape
+    width = weights[0].shape[1]
+    tile = min(256, rows)
+    return pl.pallas_call(
+        project_kernel,
+        grid=(rows // tile,),
+        in_specs=[
+            pl.BlockSpec((tile, depth), lambda i: (i, 0)),
+            pl.BlockSpec((1, width), lambda i: (0, 0)),
+        ]
+        + [VMEM] * len(weights),
+        out_specs=pl.BlockSpec((tile, width), lambda i: (i, 0)),
+        out_shape=jax.ShapeDtypeStruct((rows, width), jnp.bfloat16),
+        scratch_shapes=[pltpu.VMEM((depth, width), jnp.bfloat16)],
+        compiler_params=pltpu.CompilerParams(vmem_limit_bytes=18 << 20),
+        cost_estimate=pl.CostEstimate(
+            flops=2 * rows * depth * width,
+            bytes_accessed=2 * (rows * width + depth * (rows + width)),
+            transcendentals=0,
+        ),
+        name="project",
+    )(mixed, gain.reshape(1, width), *weights)
+
+
+def step(
+    pool_in,
+    pool_weight,
+    pool_gain,
+    out_weight,
+    mix_gain,
+    expert_in,
+    routes,
+    route_weight,
+    pre_gain,
+    gate_weight,
+    up_weight,
+    down_weight,
+    post_gain,
+):
+    rows, _ = pool_in.shape
+    ep_count, tp_count = lax.axis_size("ep"), lax.axis_size("tp")
+    chips = tp_count // CORES
+    tokens_here, choose = routes.shape
+    block_tokens = tokens_here // tp_count
+    capacity = 2 * block_tokens * choose // (gate_weight.shape[0] * ep_count)
+    dense = capacity >= block_tokens and ep_count & (ep_count - 1) == 0
+    experts = dense_experts if dense else routed_experts
+    rim = shifted(pool_in[rows - 16 :], ("ep", "tp"), 1)
+    expert_out = experts(
+        expert_in, routes, route_weight, pre_gain, gate_weight, up_weight, down_weight, post_gain
+    )
+    shards = []
+    for step in range(chips):
+        shard = to_chip(out_weight, step) if step else out_weight
+        shards += [shard, to_core(shard)]
+    mixed = mix(rim, pool_in, pool_weight, pool_gain)
+    mix_out = project(mixed, mix_gain, shards)
     return (mix_out, expert_out)
 
 
 def solution(mesh):
     return jax.shard_map(
-        body,
+        step,
         mesh=mesh,
         in_specs=(
             P(("ep", "tp"), None),

time: 365 us -> 139 us (0.38)
  waiting for transfers between devices: 274 us -> 50.8 us
  starting transfers between devices: 6.08 us -> 56.3 us
  matrix products: 35.8 us -> 0 us
  Pallas kernels: 0 us -> 25.1 us
  blocking collectives: 19.1 us -> 0 us
  between operations: 14.6 us -> 0.89 us
  other arithmetic: 8.59 us -> 1.41 us
    unnamed x4 -> x0, waiting for transfers between devices: 171 us -> none
    all_gather x2 -> x0, waiting for transfers between devices: 93.8 us -> none  [the longest x1 81.1 us: body(): lax.all_gather(arrived, 'tp', axis=0, tiled=True)]
    ppermute x0 -> x26, starting transfers between devices: none -> 54 us  [moved(): return lax.ppermute(block, ('ep', 'tp'), route)]
    ppermute x0 -> x26, waiting for transfers between devices: none -> 50.1 us  [moved(): return lax.ppermute(block, ('ep', 'tp'), route)]
    dot_general x6 -> x0, matrix products: 35.8 us -> none  [the longest x1 15.9 us: body(): jnp.einsum('necf,efd->necd', hidden_all, down_weight, preferred_element_t...]
    pallas_call x0 -> x7, Pallas kernels: none -> 25.1 us  [the longest x2 12.2 us: expert_partial(): pl.pallas_call(lambda *refs: expert_kernel(*refs, groups=groups), in_spec...]
    all_to_all x1 -> x0, blocking collectives: 19.1 us -> none  [body(): lax.all_to_all(buffer, 'ep', split_axis=0, concat_axis=0, tiled=True)]
    all_to_all x1 -> x0, waiting for transfers between devices: 9.5 us -> none  [body(): lax.all_to_all(summed, 'ep', split_axis=0, concat_axis=0, tiled=True)]
  transfers between devices with their start and end apart: 5 -> 27, of which waited for: 4 -> 7; matrix products, arithmetic and copies ran while one was open for 11% -> 1% of each run, Pallas kernels for 0% -> 18%
where the time goes in v1:
time: 139 us; the launch traced here: 138 us
  starting transfers between devices  56.3 us (41%)
  waiting for transfers between devices  50.8 us (37%)
  Pallas kernels  25.1 us (18%)
  local copies, waits for them, and re-layouts  3.04 us (2%)
  other arithmetic  1.41 us (1%)
    ppermute x26, starting transfers between devices, moved(): return lax.ppermute(block, ('ep', 'tp'), route)  54 us
    ppermute x26, waiting for transfers between devices, moved(): return lax.ppermute(block, ('ep', 'tp'), route)  50.1 us
    pallas_call x2, Pallas kernels, expert_partial(): pl.pallas_call(lambda *refs: expert_kernel(*refs, groups=groups), in_spec...  12.2 us
    pallas_call x1, Pallas kernels, own_partial(): pl.pallas_call(own_kernel, in_specs=[VMEM] * 3 + [hbm] * 3, out_specs=[VM...  6.45 us
    pallas_call x1, Pallas kernels, project(): pl.pallas_call(project_kernel, grid=(rows // tile,), in_specs=[pl.BlockSp...  4.28 us
  transfers between devices with their start and end apart: 27, of which 7 were waited for; matrix products, arithmetic and copies ran while one was open for 1% of the time, Pallas kernels for 18%

profile of v1, /device:TPU:0, one launch (start us, length us, event | category | flops | bytes accessed | tf_op | source)
XLA Modules:
  0.0 137.5 jit_solution(11373773367732097392)
XLA Ops:
  0.6 1.1 constant_dynamic-slice_fusion
  1.7 3.0 %collective-permute-start.9 = (bf16[128,2048]{1,0:T(8,128)(2,1)S(1)}, bf16[128,2048]{1,0:T(8,128)(2,1)S(1)}, u32[]{:S(2)}, u32[]{:S(2)}) collective-permute-start(bf16[128,2048]{1,0:T(8,128)(2,1)S(1)} %constant_dynamic-slice_fusion), channel_id=1, source_target_pairs={{0,8},{1,9},{2,10},{3,11},{4,12},{5,13},{6,14},{7,15},{8,0},{9,1},... | collective-permute-start | bytes 1572872 | tf_op jit(solution)/shard_map/ppermute | solution.py:29
  4.8 1.5 %collective-permute-start.12 = (bf16[128,2048]{1,0:T(8,128)(2,1)S(1)}, bf16[128,2048]{1,0:T(8,128)(2,1)S(1)}, u32[]{:S(2)}, u32[]{:S(2)}) collective-permute-start(bf16[128,2048]{1,0:T(8,128)(2,1)S(1)} %constant_dynamic-slice_fusion), channel_id=1, source_target_pairs={{0,16},{1,17},{2,18},{3,19},{4,20},{5,21},{6,22},{7,23},{8,24},{9,... | collective-permute-start | bytes 1572872 | tf_op jit(solution)/shard_map/ppermute | solution.py:29
  6.3 0.0 collective-permute-start.19
  6.3 11.2 %collective-permute-done.9.refs_4_ = bf16[128,2048]{1,0:T(8,128)(2,1)S(1)} collective-permute-done((bf16[128,2048]{1,0:T(8,128)(2,1)S(1)}, bf16[128,2048]{1,0:T(8,128)(2,1)S(1)}, u32[]{:S(2)}, u32[]{:S(2)}) %collective-permute-start.9) | collective-permute-done | bytes 524320 | tf_op jit(solution)/shard_map/ppermute | solution.py:29
  17.5 11.8 %collective-permute-done.12.refs_7_ = bf16[128,2048]{1,0:T(8,128)(2,1)S(1)} collective-permute-done((bf16[128,2048]{1,0:T(8,128)(2,1)S(1)}, bf16[128,2048]{1,0:T(8,128)(2,1)S(1)}, u32[]{:S(2)}, u32[]{:S(2)}) %collective-permute-start.12) | collective-permute-done | bytes 524320 | tf_op jit(solution)/shard_map/ppermute | solution.py:29
  29.4 0.7 select_reduce_fusion.share_ref
  30.1 0.1 collective-permute-start.11
  30.2 2.0 %collective-permute-start.14 = (f32[8,256]{1,0:T(8,128)S(1)}, f32[8,256]{1,0:T(8,128)S(1)}, u32[]{:S(2)}, u32[]{:S(2)}) collective-permute-start(f32[8,256]{1,0:T(8,128)S(1)} %select_reduce_fusion.share_ref), channel_id=1, source_target_pairs={{0,16},{1,17},{2,18},{3,19},{4,20},{5,21},{6,22},{7,23},{8,24},{9,... | collective-permute-start | bytes 24584 | tf_op jit(solution)/shard_map/ppermute | solution.py:29
  32.2 1.2 copy-done
  33.4 0.7 copy-done.3
  34.1 6.4 %own.1 = (bf16[128,2048]{1,0:T(8,128)(2,1)S(1)}, bf16[128,2048]{1,0:T(8,128)(2,1)S(1)}, bf16[2,2048,512]{2,1,0:T(8,128)(2,1)S(1)}, bf16[2,2048,512]{2,1,0:T(8,128)(2,1)S(1)}, bf16[1024,2048]{1,0:T(8,128)(2,1)S(1)}) custom-call(f32[1,2048]{1,0:T(1,128)S(1)} %bitcast.11, bf16[256,2048]{1,0:T(8,128)(2,1)S(1)} %copy-done, ...), custom_call_target="tpu_custom_call" | custom-call | flops 3221225472 | bytes 14680064 | tf_op jit(solution)/shard_map/own/pallas_call | solution.py:185
  40.6 0.1 collective-permute-start.20
  40.7 0.0 copy-start.7
  40.7 0.0 copy-start.1
  40.7 8.1 %experts.2 = (bf16[128,2048]{1,0:T(8,128)(2,1)S(1)}, bf16[128,2048]{1,0:T(8,128)(2,1)S(1)}, bf16[128,2048]{1,0:T(8,128)(2,1)S(1)}, bf16[128,2048]{1,0:T(8,128)(2,1)S(1)}) custom-call(f32[1,2048]{1,0:T(1,128)S(1)} %bitcast.12, bf16[2,2048,512]{2,1,0:T(8,128)(2,1)S(1)} %get-tuple-element.19.refs_1_, bf16[2,2048,512]{2,1,0:T(8,128)(2,1)S(1)} %get-tuple-element.20.refs_2_, ...), custom_call_target="tpu_custom_call" | custom-call | flops 6442450944 | bytes 4194304 | tf_op jit(solution)/shard_map/experts/pallas_call | solution.py:236
  48.8 0.6 collective-permute-start.15
  49.4 1.4 %collective-permute-start.21 = (f32[8,256]{1,0:T(8,128)S(1)}, f32[8,256]{1,0:T(8,128)S(1)}, u32[]{:S(2)}, u32[]{:S(2)}) collective-permute-start(f32[8,256]{1,0:T(8,128)S(1)} %select_reduce_fusion.share_ref), channel_id=1, source_target_pairs={{0,24},{1,25},{2,26},{3,27},{4,28},{5,29},{6,30},{7,31},{8,16},{9,... | collective-permute-start | bytes 24584 | tf_op jit(solution)/shard_map/ppermute | solution.py:29
  50.9 1.6 %collective-permute-start.2 = (bf16[128,2048]{1,0:T(8,128)(2,1)S(1)}, bf16[128,2048]{1,0:T(8,128)(2,1)S(1)}, u32[]{:S(2)}, u32[]{:S(2)}) collective-permute-start(bf16[128,2048]{1,0:T(8,128)(2,1)S(1)} %copy-done.7), channel_id=1, source_target_pairs={{0,2},{1,3},{2,4},{3,5},{4,6},{5,7},{6,0},{7,1},{8,10},{9,11},{10,... | collective-permute-start | bytes 1572872 | tf_op jit(solution)/shard_map/ppermute | solution.py:29
  52.4 2.6 %collective-permute-start.4 = (bf16[128,2048]{1,0:T(8,128)(2,1)S(1)}, bf16[128,2048]{1,0:T(8,128)(2,1)S(1)}, u32[]{:S(2)}, u32[]{:S(2)}) collective-permute-start(bf16[128,2048]{1,0:T(8,128)(2,1)S(1)} %copy-done.7), channel_id=1, source_target_pairs={{0,4},{1,5},{2,6},{3,7},{4,0},{5,1},{6,2},{7,3},{8,12},{9,13},{10,... | collective-permute-start | bytes 1572872 | tf_op jit(solution)/shard_map/ppermute | solution.py:29
  55.1 0.1 collective-permute-start.8
  55.1 0.0 copy-start.2
  55.2 0.5 collective-permute-start.17
  55.6 4.2 %experts.3 = (bf16[128,2048]{1,0:T(8,128)(2,1)S(1)}, bf16[128,2048]{1,0:T(8,128)(2,1)S(1)}) custom-call(f32[1,2048]{1,0:T(1,128)S(1)} %bitcast.13, bf16[2,2048,512]{2,1,0:T(8,128)(2,1)S(1)} %get-tuple-element.19.refs_1_, bf16[2,2048,512]{2,1,0:T(8,128)(2,1)S(1)} %get-tuple-element.20.refs_2_, bf16[1024,2048]{1,0:T(8,128)(2,1)S(1)} %get-tuple-element.21.refs_3_, ...), custom_call_target="tpu_custom_call" | custom-call | flops 3221225472 | bytes 2097152 | tf_op jit(solution)/shard_map/experts/pallas_call | solution.py:236
  59.8 0.2 collective-permute-start.22
  60.0 0.1 add_convert_fusion.2
  60.2 2.3 %collective-permute-start = (bf16[16,1024]{1,0:T(8,128)(2,1)S(1)}, bf16[16,1024]{1,0:T(8,128)(2,1)S(1)}, u32[]{:S(2)}, u32[]{:S(2)}) collective-permute-start(bf16[16,1024]{1,0:T(8,128)(2,1)S(1)} %slice.3), channel_id=1, source_target_pairs={{0,1},{1,2},{2,3},{3,4},{4,5},{5,6},{6,7},{7,8},{8,9},{9,10},{10,1... | collective-permute-start | bytes 98312 | tf_op jit(solution)/shard_map/ppermute | solution.py:19
  62.5 0.1 add_convert_fusion.1
  62.6 0.7 collective-permute-done.rim_ref
  63.3 5.1 %collective-permute-start.6 = (bf16[128,2048]{1,0:T(8,128)(2,1)S(1)}, bf16[128,2048]{1,0:T(8,128)(2,1)S(1)}, u32[]{:S(2)}, u32[]{:S(2)}) collective-permute-start(bf16[128,2048]{1,0:T(8,128)(2,1)S(1)} %copy-done.7), channel_id=1, source_target_pairs={{0,6},{1,7},{2,0},{3,1},{4,2},{5,3},{6,4},{7,5},{8,14},{9,15},{10,... | collective-permute-start | bytes 1572872 | tf_op jit(solution)/shard_map/ppermute | solution.py:29
  68.4 10.3 %collective-permute-start.16 = (bf16[128,2048]{1,0:T(8,128)(2,1)S(1)}, bf16[128,2048]{1,0:T(8,128)(2,1)S(1)}, u32[]{:S(2)}, u32[]{:S(2)}) collective-permute-start(bf16[128,2048]{1,0:T(8,128)(2,1)S(1)} %add_convert_fusion.2), channel_id=1, source_target_pairs={{0,8},{1,9},{2,10},{3,11},{4,12},{5,13},{6,14},{7,15},{8,0},{9,1},... | collective-permute-start | bytes 1572872 | tf_op jit(solution)/shard_map/ppermute | solution.py:29
  78.8 1.5 %collective-permute-start.18 = (bf16[128,2048]{1,0:T(8,128)(2,1)S(1)}, bf16[128,2048]{1,0:T(8,128)(2,1)S(1)}, u32[]{:S(2)}, u32[]{:S(2)}) collective-permute-start(bf16[128,2048]{1,0:T(8,128)(2,1)S(1)} %add_convert_fusion.1), channel_id=1, source_target_pairs={{0,16},{1,17},{2,18},{3,19},{4,20},{5,21},{6,22},{7,23},{8,24},{9,... | collective-permute-start | bytes 1572872 | tf_op jit(solution)/shard_map/ppermute | solution.py:29
  80.3 1.2 mix.1.mixed_ref
  81.5 0.1 add_convert_fusion
  81.7 0.1 collective-permute-start.1
  81.7 7.5 %collective-permute-done.4.refs_4_ = bf16[128,2048]{1,0:T(8,128)(2,1)S(1)} collective-permute-done((bf16[128,2048]{1,0:T(8,128)(2,1)S(1)}, bf16[128,2048]{1,0:T(8,128)(2,1)S(1)}, u32[]{:S(2)}, u32[]{:S(2)}) %collective-permute-start.4) | collective-permute-done | bytes 524320 | tf_op jit(solution)/shard_map/ppermute | solution.py:29
  89.3 5.5 %collective-permute-done.6.refs_6_ = bf16[128,2048]{1,0:T(8,128)(2,1)S(1)} collective-permute-done((bf16[128,2048]{1,0:T(8,128)(2,1)S(1)}, bf16[128,2048]{1,0:T(8,128)(2,1)S(1)}, u32[]{:S(2)}, u32[]{:S(2)}) %collective-permute-start.6) | collective-permute-done | bytes 524320 | tf_op jit(solution)/shard_map/ppermute | solution.py:29
  94.8 10.0 %collective-permute-start.5 = (bf16[128,2048]{1,0:T(8,128)(2,1)S(1)}, bf16[128,2048]{1,0:T(8,128)(2,1)S(1)}, u32[]{:S(2)}, u32[]{:S(2)}) collective-permute-start(bf16[128,2048]{1,0:T(8,128)(2,1)S(1)} %collective-permute-done.4.refs_4_), channel_id=1, source_target_pairs={{0,1},{1,0},{2,3},{3,2},{4,5},{5,4},{6,7},{7,6},{8,9},{9,8},{10,11... | collective-permute-start | bytes 1572872 | tf_op jit(solution)/shard_map/ppermute | solution.py:29
  104.8 1.6 %collective-permute-start.23 = (bf16[128,2048]{1,0:T(8,128)(2,1)S(1)}, bf16[128,2048]{1,0:T(8,128)(2,1)S(1)}, u32[]{:S(2)}, u32[]{:S(2)}) collective-permute-start(bf16[128,2048]{1,0:T(8,128)(2,1)S(1)} %add_convert_fusion), channel_id=1, source_target_pairs={{0,24},{1,25},{2,26},{3,27},{4,28},{5,29},{6,30},{7,31},{8,16},{9,... | collective-permute-start | bytes 1572872 | tf_op jit(solution)/shard_map/ppermute | solution.py:29
  106.4 0.3 convert_add_fusion
  106.7 13.3 %collective-permute-done.23 = bf16[128,2048]{1,0:T(8,128)(2,1)S(1)} collective-permute-done((bf16[128,2048]{1,0:T(8,128)(2,1)S(1)}, bf16[128,2048]{1,0:T(8,128)(2,1)S(1)}, u32[]{:S(2)}, u32[]{:S(2)}) %collective-permute-start.23) | collective-permute-done | bytes 524320 | tf_op jit(solution)/shard_map/ppermute | solution.py:29
  120.1 0.1 spread.1
  120.2 7.7 %collective-permute-start.24 = (bf16[32,2048]{1,0:T(8,128)(2,1)S(1)}, bf16[32,2048]{1,0:T(8,128)(2,1)S(1)}, u32[]{:S(2)}, u32[]{:S(2)}) collective-permute-start(bf16[32,2048]{1,0:T(8,128)(2,1)S(1)} %get-tuple-element.29), channel_id=1, source_target_pairs={{0,2},{1,3},{2,4},{3,5},{4,6},{5,7},{6,0},{7,1},{8,10},{9,11},{10,... | collective-permute-start | bytes 393224 | tf_op jit(solution)/shard_map/ppermute | solution.py:29
  127.8 1.2 collective-permute-start.25
  129.0 2.8 %collective-permute-start.26 = (bf16[32,2048]{1,0:T(8,128)(2,1)S(1)}, bf16[32,2048]{1,0:T(8,128)(2,1)S(1)}, u32[]{:S(2)}, u32[]{:S(2)}) collective-permute-start(bf16[32,2048]{1,0:T(8,128)(2,1)S(1)} %get-tuple-element.31), channel_id=1, source_target_pairs={{0,6},{1,7},{2,0},{3,1},{4,2},{5,3},{6,4},{7,5},{8,14},{9,15},{10,... | collective-permute-start | bytes 393224 | tf_op jit(solution)/shard_map/ppermute | solution.py:29
  131.9 4.3 %project.1 = bf16[512,2048]{1,0:T(8,128)(2,1)} custom-call(bf16[512,1024]{1,0:T(8,128)(2,1)S(1)} %mix.1.mixed_ref, f32[1,2048]{1,0:T(1,128)S(1)} %bitcast.16, bf16[128,2048]{1,0:T(8,128)(2,1)S(1)} %copy-done.7, bf16[128,2048]{1,0:T(8,128)(2,1)S(1)} %collective-permute-done.1.refs_1_, bf16[128,2048]{1,0:T(8,128)(2,1)S(1)} %collective-permute-done.2.refs_2_, ...), custom_call_target="tpu_custom_call" | custom-call | flops 2147483648 | bytes 7340032 | tf_op jit(solution)/shard_map/project/pallas_call | solution.py:414
  136.2 0.5 collective-permute-done.25.refs_1_
  136.7 0.8 finish.1
  (38 shorter events, 0.1 us)
Async XLA Ops:
  1.7 15.8 %collective-permute-start.9 = (bf16[128,2048]{1,0:T(8,128)(2,1)S(1)}, bf16[128,2048]{1,0:T(8,128)(2,1)S(1)}, u32[]{:S(2)}, u32[]{:S(2)}) collective-permute-start(bf16[128,2048]{1,0:T(8,128)(2,1)S(1)} %constant_dynamic-slice_fusion), channel_id=1, source_target_pairs={{0,8},{1,9},{2,10},{3,11},{4,12},{5,13},{6,14},{7,15},{8,0},{9,1},... | collective-permute-start | bytes 1572872 | tf_op jit(solution)/shard_map/ppermute | solution.py:29
  4.8 24.6 %collective-permute-start.12 = (bf16[128,2048]{1,0:T(8,128)(2,1)S(1)}, bf16[128,2048]{1,0:T(8,128)(2,1)S(1)}, u32[]{:S(2)}, u32[]{:S(2)}) collective-permute-start(bf16[128,2048]{1,0:T(8,128)(2,1)S(1)} %constant_dynamic-slice_fusion), channel_id=1, source_target_pairs={{0,16},{1,17},{2,18},{3,19},{4,20},{5,21},{6,22},{7,23},{8,24},{9,... | collective-permute-start | bytes 1572872 | tf_op jit(solution)/shard_map/ppermute | solution.py:29
  6.3 34.3 %collective-permute-start.19 = (bf16[128,2048]{1,0:T(8,128)(2,1)S(1)}, bf16[128,2048]{1,0:T(8,128)(2,1)S(1)}, u32[]{:S(2)}, u32[]{:S(2)}) collective-permute-start(bf16[128,2048]{1,0:T(8,128)(2,1)S(1)} %constant_dynamic-slice_fusion), channel_id=1, source_target_pairs={{0,24},{1,25},{2,26},{3,27},{4,28},{5,29},{6,30},{7,31},{8,16},{9,... | collective-permute-start | bytes 1572872 | tf_op jit(solution)/shard_map/ppermute | solution.py:29
  17.5 23.2 %collective-permute-start.10 = (bf16[128,2048]{1,0:T(8,128)(2,1)S(1)}, bf16[128,2048]{1,0:T(8,128)(2,1)S(1)}, u32[]{:S(2)}, u32[]{:S(2)}) collective-permute-start(bf16[128,2048]{1,0:T(8,128)(2,1)S(1)} %collective-permute-done.9.refs_4_), channel_id=1, source_target_pairs={{0,1},{1,0},{2,3},{3,2},{4,5},{5,4},{6,7},{7,6},{8,9},{9,8},{10,11... | collective-permute-start | bytes 1572872 | tf_op jit(solution)/shard_map/ppermute | solution.py:29
  29.4 11.3 %collective-permute-start.13 = (bf16[128,2048]{1,0:T(8,128)(2,1)S(1)}, bf16[128,2048]{1,0:T(8,128)(2,1)S(1)}, u32[]{:S(2)}, u32[]{:S(2)}) collective-permute-start(bf16[128,2048]{1,0:T(8,128)(2,1)S(1)} %collective-permute-done.12.refs_7_), channel_id=1, source_target_pairs={{0,1},{1,0},{2,3},{3,2},{4,5},{5,4},{6,7},{7,6},{8,9},{9,8},{10,11... | collective-permute-start | bytes 1572872 | tf_op jit(solution)/shard_map/ppermute | solution.py:29
  30.1 10.6 %collective-permute-start.11 = (f32[8,256]{1,0:T(8,128)S(1)}, f32[8,256]{1,0:T(8,128)S(1)}, u32[]{:S(2)}, u32[]{:S(2)}) collective-permute-start(f32[8,256]{1,0:T(8,128)S(1)} %select_reduce_fusion.share_ref), channel_id=1, source_target_pairs={{0,8},{1,9},{2,10},{3,11},{4,12},{5,13},{6,14},{7,15},{8,0},{9,1},... | collective-permute-start | bytes 24584 | tf_op jit(solution)/shard_map/ppermute | solution.py:29
  30.2 10.5 %collective-permute-start.14 = (f32[8,256]{1,0:T(8,128)S(1)}, f32[8,256]{1,0:T(8,128)S(1)}, u32[]{:S(2)}, u32[]{:S(2)}) collective-permute-start(f32[8,256]{1,0:T(8,128)S(1)} %select_reduce_fusion.share_ref), channel_id=1, source_target_pairs={{0,16},{1,17},{2,18},{3,19},{4,20},{5,21},{6,22},{7,23},{8,24},{9,... | collective-permute-start | bytes 24584 | tf_op jit(solution)/shard_map/ppermute | solution.py:29
  32.2 1.2 copy-start
  33.4 0.7 copy-start.3
  34.1 6.6 %copy-start.4 = (f32[2048]{0:T(1024)S(1)}, f32[2048]{0:T(1024)}, u32[]{:S(2)}) copy-start(f32[2048]{0:T(1024)} %param.21) | copy-start | bytes 24580
  40.6 14.5 %collective-permute-start.20 = (bf16[128,2048]{1,0:T(8,128)(2,1)S(1)}, bf16[128,2048]{1,0:T(8,128)(2,1)S(1)}, u32[]{:S(2)}, u32[]{:S(2)}) collective-permute-start(bf16[128,2048]{1,0:T(8,128)(2,1)S(1)} %collective-permute-done.19.refs_4_), channel_id=1, source_target_pairs={{0,1},{1,0},{2,3},{3,2},{4,5},{5,4},{6,7},{7,6},{8,9},{9,8},{10,11... | collective-permute-start | bytes 1572872 | tf_op jit(solution)/shard_map/ppermute | solution.py:29
  40.7 10.1 %copy-start.7 = (bf16[128,2048]{1,0:T(8,128)(2,1)S(1)}, bf16[128,2048]{1,0:T(8,128)(2,1)}, u32[]{:S(2)}) copy-start(bf16[128,2048]{1,0:T(8,128)(2,1)} %refs_0_.1) | copy-start | bytes 1572868
  40.7 14.3 %copy-start.1 = (bf16[512,1024]{1,0:T(8,128)(2,1)S(1)}, bf16[512,1024]{1,0:T(8,128)(2,1)}, u32[]{:S(2)}) copy-start(bf16[512,1024]{1,0:T(8,128)(2,1)} %rows_ref.2) | copy-start | bytes 3145732
  48.8 11.0 %collective-permute-start.15 = (bf16[128,2048]{1,0:T(8,128)(2,1)S(1)}, bf16[128,2048]{1,0:T(8,128)(2,1)S(1)}, u32[]{:S(2)}, u32[]{:S(2)}) collective-permute-start(bf16[128,2048]{1,0:T(8,128)(2,1)S(1)} %get-tuple-element.23), channel_id=1, source_target_pairs={{0,1},{1,0},{2,3},{3,2},{4,5},{5,4},{6,7},{7,6},{8,9},{9,8},{10,11... | collective-permute-start | bytes 1572872 | tf_op jit(solution)/shard_map/ppermute | solution.py:29
  49.4 5.6 %collective-permute-start.21 = (f32[8,256]{1,0:T(8,128)S(1)}, f32[8,256]{1,0:T(8,128)S(1)}, u32[]{:S(2)}, u32[]{:S(2)}) collective-permute-start(f32[8,256]{1,0:T(8,128)S(1)} %select_reduce_fusion.share_ref), channel_id=1, source_target_pairs={{0,24},{1,25},{2,26},{3,27},{4,28},{5,29},{6,30},{7,31},{8,16},{9,... | collective-permute-start | bytes 24584 | tf_op jit(solution)/shard_map/ppermute | solution.py:29
  50.9 30.8 %collective-permute-start.2 = (bf16[128,2048]{1,0:T(8,128)(2,1)S(1)}, bf16[128,2048]{1,0:T(8,128)(2,1)S(1)}, u32[]{:S(2)}, u32[]{:S(2)}) collective-permute-start(bf16[128,2048]{1,0:T(8,128)(2,1)S(1)} %copy-done.7), channel_id=1, source_target_pairs={{0,2},{1,3},{2,4},{3,5},{4,6},{5,7},{6,0},{7,1},{8,10},{9,11},{10,... | collective-permute-start | bytes 1572872 | tf_op jit(solution)/shard_map/ppermute | solution.py:29
  52.4 36.8 %collective-permute-start.4 = (bf16[128,2048]{1,0:T(8,128)(2,1)S(1)}, bf16[128,2048]{1,0:T(8,128)(2,1)S(1)}, u32[]{:S(2)}, u32[]{:S(2)}) collective-permute-start(bf16[128,2048]{1,0:T(8,128)(2,1)S(1)} %copy-done.7), channel_id=1, source_target_pairs={{0,4},{1,5},{2,6},{3,7},{4,0},{5,1},{6,2},{7,3},{8,12},{9,13},{10,... | collective-permute-start | bytes 1572872 | tf_op jit(solution)/shard_map/ppermute | solution.py:29
  55.1 13.4 %collective-permute-start.8 = (bf16[128,2048]{1,0:T(8,128)(2,1)S(1)}, bf16[128,2048]{1,0:T(8,128)(2,1)S(1)}, u32[]{:S(2)}, u32[]{:S(2)}) collective-permute-start(bf16[128,2048]{1,0:T(8,128)(2,1)S(1)} %get-tuple-element.18), channel_id=1, source_target_pairs={{0,1},{1,0},{2,3},{3,2},{4,5},{5,4},{6,7},{7,6},{8,9},{9,8},{10,11... | collective-permute-start | bytes 1572872 | tf_op jit(solution)/shard_map/ppermute | solution.py:29
  55.1 25.1 %copy-start.2 = (bf16[4,256,256]{2,1,0:T(8,128)(2,1)S(1)}, bf16[4,256,256]{2,1,0:T(8,128)(2,1)}, u32[]{:S(2)}) copy-start(bf16[4,256,256]{2,1,0:T(8,128)(2,1)} %weight_ref.1) | copy-start | bytes 1572868
  55.2 25.1 %copy-start.6 = (f32[1024]{0:T(1024)S(1)}, f32[1024]{0:T(1024)}, u32[]{:S(2)}) copy-start(f32[1024]{0:T(1024)} %param.15) | copy-start | bytes 12292
  55.2 5.0 %collective-permute-start.17 = (bf16[128,2048]{1,0:T(8,128)(2,1)S(1)}, bf16[128,2048]{1,0:T(8,128)(2,1)S(1)}, u32[]{:S(2)}, u32[]{:S(2)}) collective-permute-start(bf16[128,2048]{1,0:T(8,128)(2,1)S(1)} %get-tuple-element.25), channel_id=1, source_target_pairs={{0,1},{1,0},{2,3},{3,2},{4,5},{5,4},{6,7},{7,6},{8,9},{9,8},{10,11... | collective-permute-start | bytes 1572872 | tf_op jit(solution)/shard_map/ppermute | solution.py:29
  59.8 18.9 %collective-permute-start.22 = (bf16[128,2048]{1,0:T(8,128)(2,1)S(1)}, bf16[128,2048]{1,0:T(8,128)(2,1)S(1)}, u32[]{:S(2)}, u32[]{:S(2)}) collective-permute-start(bf16[128,2048]{1,0:T(8,128)(2,1)S(1)} %get-tuple-element.27), channel_id=1, source_target_pairs={{0,1},{1,0},{2,3},{3,2},{4,5},{5,4},{6,7},{7,6},{8,9},{9,8},{10,11... | collective-permute-start | bytes 1572872 | tf_op jit(solution)/shard_map/ppermute | solution.py:29
  60.2 3.1 %collective-permute-start = (bf16[16,1024]{1,0:T(8,128)(2,1)S(1)}, bf16[16,1024]{1,0:T(8,128)(2,1)S(1)}, u32[]{:S(2)}, u32[]{:S(2)}) collective-permute-start(bf16[16,1024]{1,0:T(8,128)(2,1)S(1)} %slice.3), channel_id=1, source_target_pairs={{0,1},{1,2},{2,3},{3,4},{4,5},{5,6},{6,7},{7,8},{8,9},{9,10},{10,1... | collective-permute-start | bytes 98312 | tf_op jit(solution)/shard_map/ppermute | solution.py:19
  63.3 31.5 %collective-permute-start.6 = (bf16[128,2048]{1,0:T(8,128)(2,1)S(1)}, bf16[128,2048]{1,0:T(8,128)(2,1)S(1)}, u32[]{:S(2)}, u32[]{:S(2)}) collective-permute-start(bf16[128,2048]{1,0:T(8,128)(2,1)S(1)} %copy-done.7), channel_id=1, source_target_pairs={{0,6},{1,7},{2,0},{3,1},{4,2},{5,3},{6,4},{7,5},{8,14},{9,15},{10,... | collective-permute-start | bytes 1572872 | tf_op jit(solution)/shard_map/ppermute | solution.py:29
  68.4 36.4 %collective-permute-start.16 = (bf16[128,2048]{1,0:T(8,128)(2,1)S(1)}, bf16[128,2048]{1,0:T(8,128)(2,1)S(1)}, u32[]{:S(2)}, u32[]{:S(2)}) collective-permute-start(bf16[128,2048]{1,0:T(8,128)(2,1)S(1)} %add_convert_fusion.2), channel_id=1, source_target_pairs={{0,8},{1,9},{2,10},{3,11},{4,12},{5,13},{6,14},{7,15},{8,0},{9,1},... | collective-permute-start | bytes 1572872 | tf_op jit(solution)/shard_map/ppermute | solution.py:29
  78.8 26.0 %collective-permute-start.18 = (bf16[128,2048]{1,0:T(8,128)(2,1)S(1)}, bf16[128,2048]{1,0:T(8,128)(2,1)S(1)}, u32[]{:S(2)}, u32[]{:S(2)}) collective-permute-start(bf16[128,2048]{1,0:T(8,128)(2,1)S(1)} %add_convert_fusion.1), channel_id=1, source_target_pairs={{0,16},{1,17},{2,18},{3,19},{4,20},{5,21},{6,22},{7,23},{8,24},{9,... | collective-permute-start | bytes 1572872 | tf_op jit(solution)/shard_map/ppermute | solution.py:29
  80.3 51.6 %copy-start.8 = (f32[2048]{0:T(1024)S(1)}, f32[2048]{0:T(1024)}, u32[]{:S(2)}) copy-start(f32[2048]{0:T(1024)} %param.17) | copy-start | bytes 24580
  81.7 46.2 %collective-permute-start.1 = (bf16[128,2048]{1,0:T(8,128)(2,1)S(1)}, bf16[128,2048]{1,0:T(8,128)(2,1)S(1)}, u32[]{:S(2)}, u32[]{:S(2)}) collective-permute-start(bf16[128,2048]{1,0:T(8,128)(2,1)S(1)} %copy-done.7), channel_id=1, source_target_pairs={{0,1},{1,0},{2,3},{3,2},{4,5},{5,4},{6,7},{7,6},{8,9},{9,8},{10,11... | collective-permute-start | bytes 1572872 | tf_op jit(solution)/shard_map/ppermute | solution.py:29
  89.3 39.7 %collective-permute-start.3 = (bf16[128,2048]{1,0:T(8,128)(2,1)S(1)}, bf16[128,2048]{1,0:T(8,128)(2,1)S(1)}, u32[]{:S(2)}, u32[]{:S(2)}) collective-permute-start(bf16[128,2048]{1,0:T(8,128)(2,1)S(1)} %collective-permute-done.2.refs_2_), channel_id=1, source_target_pairs={{0,1},{1,0},{2,3},{3,2},{4,5},{5,4},{6,7},{7,6},{8,9},{9,8},{10,11... | collective-permute-start | bytes 1572872 | tf_op jit(solution)/shard_map/ppermute | solution.py:29
  94.8 37.1 %collective-permute-start.5 = (bf16[128,2048]{1,0:T(8,128)(2,1)S(1)}, bf16[128,2048]{1,0:T(8,128)(2,1)S(1)}, u32[]{:S(2)}, u32[]{:S(2)}) collective-permute-start(bf16[128,2048]{1,0:T(8,128)(2,1)S(1)} %collective-permute-done.4.refs_4_), channel_id=1, source_target_pairs={{0,1},{1,0},{2,3},{3,2},{4,5},{5,4},{6,7},{7,6},{8,9},{9,8},{10,11... | collective-permute-start | bytes 1572872 | tf_op jit(solution)/shard_map/ppermute | solution.py:29
  104.8 27.1 %collective-permute-start.7 = (bf16[128,2048]{1,0:T(8,128)(2,1)S(1)}, bf16[128,2048]{1,0:T(8,128)(2,1)S(1)}, u32[]{:S(2)}, u32[]{:S(2)}) collective-permute-start(bf16[128,2048]{1,0:T(8,128)(2,1)S(1)} %collective-permute-done.6.refs_6_), channel_id=1, source_target_pairs={{0,1},{1,0},{2,3},{3,2},{4,5},{5,4},{6,7},{7,6},{8,9},{9,8},{10,11... | collective-permute-start | bytes 1572872 | tf_op jit(solution)/shard_map/ppermute | solution.py:29
  104.8 15.2 %collective-permute-start.23 = (bf16[128,2048]{1,0:T(8,128)(2,1)S(1)}, bf16[128,2048]{1,0:T(8,128)(2,1)S(1)}, u32[]{:S(2)}, u32[]{:S(2)}) collective-permute-start(bf16[128,2048]{1,0:T(8,128)(2,1)S(1)} %add_convert_fusion), channel_id=1, source_target_pairs={{0,24},{1,25},{2,26},{3,27},{4,28},{5,29},{6,30},{7,31},{8,16},{9,... | collective-permute-start | bytes 1572872 | tf_op jit(solution)/shard_map/ppermute | solution.py:29
  120.1 16.6 %copy-start.5 = (f32[2048]{0:T(1024)S(1)}, f32[2048]{0:T(1024)}, u32[]{:S(2)}) copy-start(f32[2048]{0:T(1024)} %param.25) | copy-start | bytes 24580
  120.2 16.0 %collective-permute-start.24 = (bf16[32,2048]{1,0:T(8,128)(2,1)S(1)}, bf16[32,2048]{1,0:T(8,128)(2,1)S(1)}, u32[]{:S(2)}, u32[]{:S(2)}) collective-permute-start(bf16[32,2048]{1,0:T(8,128)(2,1)S(1)} %get-tuple-element.29), channel_id=1, source_target_pairs={{0,2},{1,3},{2,4},{3,5},{4,6},{5,7},{6,0},{7,1},{8,10},{9,11},{10,... | collective-permute-start | bytes 393224 | tf_op jit(solution)/shard_map/ppermute | solution.py:29
  127.8 8.9 %collective-permute-start.25 = (bf16[32,2048]{1,0:T(8,128)(2,1)S(1)}, bf16[32,2048]{1,0:T(8,128)(2,1)S(1)}, u32[]{:S(2)}, u32[]{:S(2)}) collective-permute-start(bf16[32,2048]{1,0:T(8,128)(2,1)S(1)} %get-tuple-element.30), channel_id=1, source_target_pairs={{0,4},{1,5},{2,6},{3,7},{4,0},{5,1},{6,2},{7,3},{8,12},{9,13},{10,... | collective-permute-start | bytes 393224 | tf_op jit(solution)/shard_map/ppermute | solution.py:29
  129.0 7.7 %collective-permute-start.26 = (bf16[32,2048]{1,0:T(8,128)(2,1)S(1)}, bf16[32,2048]{1,0:T(8,128)(2,1)S(1)}, u32[]{:S(2)}, u32[]{:S(2)}) collective-permute-start(bf16[32,2048]{1,0:T(8,128)(2,1)S(1)} %get-tuple-element.31), channel_id=1, source_target_pairs={{0,6},{1,7},{2,0},{3,1},{4,2},{5,3},{6,4},{7,5},{8,14},{9,15},{10,... | collective-permute-start | bytes 393224 | tf_op jit(solution)/shard_map/ppermute | solution.py:29

commit v2 on v1

--- a/solution.py
+++ b/solution.py
@@ -37,9 +37,22 @@
     return moved(block, lambda e, t: (e ^ mask, t))
 
 
+def paired(chips):
+    return chips & (chips - 1) == 0
+
+
 def to_chip(block, step):
     chips = lax.axis_size("tp") // CORES
-    return moved(block, lambda e, t: (e, (t // CORES + step) % chips * CORES + t % CORES))
+    target = (lambda z: z ^ step) if paired(chips) else (lambda z: (z + step) % chips)
+    return moved(block, lambda e, t: (e, target(t // CORES) * CORES + t % CORES))
+
+
+def chip_after(chip, step, chips):
+    return lax.bitwise_xor(chip, step) if paired(chips) else lax.rem(chip + step, chips)
+
+
+def chip_before(chip, step, chips):
+    return lax.bitwise_xor(chip, step) if paired(chips) else lax.rem(chip + chips - step, chips)
 
 
 def rms_scale(values, gain):
@@ -116,18 +129,24 @@
 
 
 VMEM = pl.BlockSpec(memory_space=pltpu.VMEM)
+HBM = pl.BlockSpec(memory_space=pltpu.HBM)
 
 
 def normed_rows(source, gain):
     return rms_scale(source[...].astype(jnp.float32), gain[...]).astype(jnp.bfloat16)
 
 
-def fill_hidden(hidden, expert, first, normed, share, gate_weight, up_weight):
+def share_of(message, expert, tokens):
+    start = pl.multiple_of(expert * tokens, tokens)
+    notes = message[tokens // CORES :, pl.ds(start, tokens)].astype(jnp.float32)
+    notes = jnp.transpose(notes)
+    return notes[:, 0:1] + notes[:, 1:2]
+
+
+def fill_hidden(hidden, expert, scale, normed, gate_weight, up_weight):
     units = gate_weight.shape[1]
-    lanes = lax.broadcasted_iota(jnp.int32, share.shape, 1)
     gate = jnp.dot(normed[...], gate_weight[...], preferred_element_type=jnp.float32)
     up = jnp.dot(normed[...], up_weight[...], preferred_element_type=jnp.float32)
-    scale = jnp.sum(jnp.where(lanes == first + expert, share, 0.0), axis=1, keepdims=True)
     hidden[:, expert * units : (expert + 1) * units] = (clamped_unit(gate, up) * scale).astype(
         jnp.bfloat16
     )
@@ -147,51 +166,111 @@
             outputs[2 * group + 1][rows_of, :] = total[start + 1 - core]
 
 
+def start_all(pairs, sems):
+    copies = [
+        pltpu.make_async_copy(source, target, sems.at[k])
+        for k, (source, target) in enumerate(pairs)
+    ]
+    for copy in copies:
+        copy.start()
+    return copies
+
+
+def from_hbm(*arrays):
+    return [pltpu.with_memory_space_constraint(array, pltpu.HBM) for array in arrays]
+
+
+def pack_kernel(rows_ref, routes_in, weight_in, message_ref, routes_ref, weight_ref, sems):
+    half = rows_ref.shape[0] // CORES
+    tokens = routes_ref.shape[1]
+    experts = message_ref.shape[1] // tokens
+    start = pl.multiple_of(seat()[1] * half, half)
+    copies = start_all(
+        [
+            (routes_in, routes_ref),
+            (weight_in, weight_ref),
+            (rows_ref.at[pl.ds(start, half)], message_ref.at[pl.ds(0, half)]),
+        ],
+        sems,
+    )
+    copies[0].wait()
+    copies[1].wait()
+    notes = message_ref.shape[0] - half
+    line = lax.broadcasted_iota(jnp.int32, (notes, tokens), 0)
+    for expert in range(experts):
+        share = jnp.sum(
+            jnp.where(routes_ref[...] == expert, weight_ref[...], 0.0), axis=0, keepdims=True
+        )
+        coarse = share.astype(jnp.bfloat16).astype(jnp.float32)
+        both = jnp.where(line == 0, coarse, jnp.where(line == 1, share - coarse, 0.0))
+        message_ref[half:, expert * tokens : (expert + 1) * tokens] = both.astype(jnp.bfloat16)
+    copies[2].wait()
+
+
+def pack(rows, routes, route_weight):
+    tokens, width = rows.shape
+    choose = routes.shape[1]
+    return pl.pallas_call(
+        pack_kernel,
+        in_specs=[HBM] * 3,
+        out_specs=VMEM,
+        out_shape=jax.ShapeDtypeStruct((tokens // CORES + 8, width), rows.dtype),
+        scratch_shapes=[
+            pltpu.VMEM((choose, tokens), jnp.int32),
+            pltpu.VMEM((choose, tokens), jnp.float32),
+            pltpu.SemaphoreType.DMA((3,)),
+        ],
+        compiler_params=pltpu.CompilerParams(vmem_limit_bytes=2 << 20),
+        name="pack",
+    )(*from_hbm(rows, routes.T, route_weight.T))
+
+
 def own_kernel(
-    gain_ref, rows_ref, share_ref, gate_in, up_in, down_in,
-    kept_ref, sent_ref, gate_ref, up_ref, down_ref, normed, hidden, total, sems,
+    gain_in, rows_in, gate_in, up_in, down_in, message_ref,
+    kept_ref, sent_ref, gate_ref, up_ref, down_ref,
+    gain_ref, rows_ref, normed, hidden, total, sems,
 ):
     local, _, units = gate_ref.shape
+    tokens = rows_ref.shape[0]
     first = lax.axis_index("ep") * local
-    loads = []
+    pairs = [(rows_in, rows_ref), (gain_in, gain_ref)]
     for expert in range(local):
-        loads.append(pltpu.make_async_copy(gate_in.at[expert], gate_ref.at[expert], sems.at[len(loads)]))
-        loads.append(pltpu.make_async_copy(up_in.at[expert], up_ref.at[expert], sems.at[len(loads)]))
+        pairs.append((gate_in.at[expert], gate_ref.at[expert]))
+        pairs.append((up_in.at[expert], up_ref.at[expert]))
     for expert in range(local):
         part = pl.ds(expert * units, units)
-        loads.append(pltpu.make_async_copy(down_in.at[part], down_ref.at[part], sems.at[len(loads)]))
-    for load in loads:
-        load.start()
+        pairs.append((down_in.at[part], down_ref.at[part]))
+    copies = start_all(pairs, sems)
+    copies[0].wait()
+    copies[1].wait()
     normed[...] = normed_rows(rows_ref, gain_ref)
-    share = jnp.transpose(share_ref[...])
     for expert in range(local):
-        loads[2 * expert].wait()
-        loads[2 * expert + 1].wait()
-        fill_hidden(
-            hidden, expert, first, normed, share, gate_ref.at[expert], up_ref.at[expert]
-        )
-    for load in loads[2 * local :]:
-        load.wait()
+        copies[2 + 2 * expert].wait()
+        copies[3 + 2 * expert].wait()
+        scale = share_of(message_ref, first + expert, tokens)
+        fill_hidden(hidden, expert, scale, normed, gate_ref.at[expert], up_ref.at[expert])
+    for copy in copies[2 + 2 * local :]:
+        copy.wait()
     store_halves(hidden, down_ref, total, seat()[1], (kept_ref, sent_ref))
 
 
-def own_partial(rows, share, gain, gate_weight, up_weight, down_weight, block):
+def own_partial(rows, message, gain, gate_weight, up_weight, down_weight, block):
     tokens, width = rows.shape
     local, _, units = gate_weight.shape
     half = jax.ShapeDtypeStruct((tokens // 2, width), jnp.bfloat16)
-    down_weight = down_weight.reshape(-1, width)
     held = [pltpu.VMEM(w.shape, w.dtype) for w in (gate_weight, up_weight, down_weight)]
-    hbm = pl.BlockSpec(memory_space=pltpu.HBM)
     return pl.pallas_call(
         own_kernel,
-        in_specs=[VMEM] * 3 + [hbm] * 3,
+        in_specs=[HBM] * 5 + [VMEM],
         out_specs=[VMEM] * 5,
         out_shape=[half, half] + held,
         scratch_shapes=[
+            pltpu.VMEM((1, width), jnp.float32),
+            pltpu.VMEM((tokens, width), rows.dtype),
             pltpu.VMEM((tokens, width), jnp.bfloat16),
             pltpu.VMEM((tokens, local * units), jnp.bfloat16),
             pltpu.VMEM((tokens // block, block, width), jnp.bfloat16),
-            pltpu.SemaphoreType.DMA((3 * local,)),
+            pltpu.SemaphoreType.DMA((2 + 3 * local,)),
         ],
         compiler_params=pltpu.CompilerParams(vmem_limit_bytes=10 << 20),
         cost_estimate=pl.CostEstimate(
@@ -200,36 +279,30 @@
             transcendentals=tokens * local * units,
         ),
         name="own",
-    )(
-        gain.reshape(1, width), rows, share,
-        *(
-            pltpu.with_memory_space_constraint(w, pltpu.HBM)
-            for w in (gate_weight, up_weight, down_weight)
-        ),
-    )
+    )(*from_hbm(gain.reshape(1, width), rows, gate_weight, up_weight, down_weight), message)
 
 
 def expert_kernel(gain_ref, gate_ref, up_ref, down_ref, *refs, groups):
-    inputs, outputs = refs[: 3 * groups], refs[3 * groups : 5 * groups]
-    normed, hidden, total = refs[5 * groups :]
+    inputs, outputs = refs[: 2 * groups], refs[2 * groups : 4 * groups]
+    normed, hidden, total = refs[4 * groups :]
     first, core = lax.axis_index("ep") * gate_ref.shape[0], seat()[1]
-    half = inputs[0].shape[0]
-    shares = []
+    half = normed.shape[0] // (2 * groups)
     for group in range(groups):
-        mine_ref, other_ref, share_ref = inputs[3 * group : 3 * group + 3]
+        mine_ref, other_ref = inputs[2 * group : 2 * group + 2]
         for source, which in ((mine_ref, core), (other_ref, 1 - core)):
             start = pl.multiple_of((2 * group + which) * half, half)
-            normed[pl.ds(start, half), :] = normed_rows(source, gain_ref)
-        shares.append(jnp.transpose(share_ref[...]))
-    share = jnp.concatenate(shares, axis=0)
+            normed[pl.ds(start, half), :] = normed_rows(source.at[:half], gain_ref)
     for expert in range(gate_ref.shape[0]):
-        fill_hidden(hidden, expert, first, normed, share, gate_ref.at[expert], up_ref.at[expert])
+        shares = [share_of(ref, first + expert, 2 * half) for ref in inputs[::2]]
+        scale = jnp.concatenate(shares, axis=0)
+        fill_hidden(hidden, expert, scale, normed, gate_ref.at[expert], up_ref.at[expert])
     store_halves(hidden, down_ref, total, core, outputs)
 
 
 def expert_partial(chunks, gain, gate_weight, up_weight, down_weight, block):
     groups = len(chunks)
     half, width = chunks[0][0].shape
+    half -= 8
     rows = 2 * half * groups
     local, _, units = gate_weight.shape
     inputs = [array for chunk in chunks for array in chunk]
@@ -257,7 +330,7 @@
 def spread_kernel(early_ref, late_ref, own_ref, *out_refs):
     chips = early_ref.shape[0]
     for step in range(chips):
-        at = lax.rem(seat()[0] + step, chips)
+        at = chip_after(seat()[0], step, chips)
         part = early_ref[at] + late_ref[at].astype(jnp.float32)
         if step:
             out_refs[step - 1][...] = part.astype(jnp.bfloat16)
@@ -306,25 +379,13 @@
     groups = lax.axis_size("ep")
     chips = lax.axis_size("tp") // CORES
     block = tokens // lax.axis_size("tp")
-    local = gate_weight.shape[0]
-    experts = local * groups
-    place = lax.axis_index("tp")
-    core = place % CORES
     masks = range(1, groups)
-    mine = lax.dynamic_slice_in_dim(expert_in, core * (tokens // CORES), tokens // CORES, 0)
+    message = pack(expert_in, routes, route_weight)
     mine_from = {}
     for m in masks:
-        mine_from[m] = to_group(mine, m)
-    numbers = jnp.arange(-(-experts // 8) * 8, dtype=jnp.int32)
-    share = jnp.sum(
-        jnp.where(routes.T[None] == numbers[:, None, None], route_weight.T[None], 0.0), axis=1
-    )
-    share_from = {}
-    for m in masks:
-        share_from[m] = to_group(share, m)
-    kept, sent, *held = own_partial(
-        expert_in, share, pre_gain, gate_weight, up_weight, down_weight, block
-    )
+        mine_from[m] = to_group(message, m)
+    weights = (pre_gain, gate_weight, up_weight, down_weight.reshape(-1, width), block)
+    kept, sent, *held = own_partial(expert_in, message, *weights)
     weights = (pre_gain, *held, block)
     early = kept.astype(jnp.float32) + to_core(sent).astype(jnp.float32)
     near = [m for m in masks if m & (m - 1) == 0]
@@ -333,7 +394,7 @@
     for batch in (near, far):
         chunks = []
         for m in batch:
-            chunks.append((mine_from[m], to_core(mine_from[m]), share_from[m]))
+            chunks.append((mine_from[m], to_core(mine_from[m])))
         results = expert_partial(chunks, *weights)
         for m, (kept, sent) in zip(batch, results):
             partner = to_core(sent)
@@ -399,7 +460,7 @@
         chip, core = seat()
         chips = len(weights) // CORES
         for k, weight in enumerate(weights):
-            source = lax.rem(chip + chips - k // CORES, chips) * CORES
+            source = chip_before(chip, k // CORES, chips) * CORES
             shard = source + (core if k % CORES == 0 else 1 - core)
             joined[pl.ds(pl.multiple_of(shard * depth, depth), depth), :] = weight[...]
 
@@ -453,7 +514,9 @@
     tokens_here, choose = routes.shape
     block_tokens = tokens_here // tp_count
     capacity = 2 * block_tokens * choose // (gate_weight.shape[0] * ep_count)
+    experts_in_all = gate_weight.shape[0] * ep_count
     dense = capacity >= block_tokens and ep_count & (ep_count - 1) == 0
+    dense = dense and experts_in_all * tokens_here <= expert_in.shape[1]
     experts = dense_experts if dense else routed_experts
     rim = shifted(pool_in[rows - 16 :], ("ep", "tp"), 1)
     expert_out = experts(

time: 139 us -> 127 us (0.914)
  starting transfers between devices: 56.3 us -> 47.8 us
  local copies, waits for them, and re-layouts: 3.04 us -> 0.04 us
  Pallas kernels: 25.1 us -> 26.8 us
    ppermute x26 -> x23, starting transfers between devices: 54 us -> 45.4 us  [moved(): return lax.ppermute(block, ('ep', 'tp'), route)]
    unnamed x18 -> x14, local copies, waits for them, and re-layouts: 1.96 us -> 0.04 us
    pallas_call x1 -> x2, Pallas kernels: 6.45 us -> 7.93 us  [the longest x1 6.83 us: own_partial(): pl.pallas_call(own_kernel, in_specs=[HBM] * 5 + [VMEM], out_specs=[VMEM]...]
    ppermute x26 -> x23, waiting for transfers between devices: 50.1 us -> 49.6 us  [moved(): return lax.ppermute(block, ('ep', 'tp'), route)]
  transfers between devices with their start and end apart: 27 -> 24, of which waited for: 7 -> 7; matrix products, arithmetic and copies ran while one was open for 1% -> 1% of each run, Pallas kernels for 18% -> 20%
where the time goes in v2:
time: 127 us; the launch traced here: 126 us
  waiting for transfers between devices  50.3 us (40%)
  starting transfers between devices  47.8 us (38%)
  Pallas kernels  26.8 us (21%)
    ppermute x23, waiting for transfers between devices, moved(): return lax.ppermute(block, ('ep', 'tp'), route)  49.6 us
    ppermute x23, starting transfers between devices, moved(): return lax.ppermute(block, ('ep', 'tp'), route)  45.4 us
    pallas_call x2, Pallas kernels, expert_partial(): pl.pallas_call(lambda *refs: expert_kernel(*refs, groups=groups), in_spec...  12.4 us
    pallas_call x1, Pallas kernels, own_partial(): pl.pallas_call(own_kernel, in_specs=[HBM] * 5 + [VMEM], out_specs=[VMEM]...  6.83 us
    pallas_call x1, Pallas kernels, project(): pl.pallas_call(project_kernel, grid=(rows // tile,), in_specs=[pl.BlockSp...  4.27 us
  transfers between devices with their start and end apart: 24, of which 7 were waited for; matrix products, arithmetic and copies ran while one was open for 1% of the time, Pallas kernels for 20%

profile of v2, /device:TPU:0, one launch (start us, length us, event | category | flops | bytes accessed | tf_op | source)
XLA Modules:
  0.0 126.4 jit_solution(14543268473931985839)
XLA Ops:
  0.6 1.1 pack.1.message_ref
  1.7 3.0 %collective-permute-start.9 = (bf16[136,2048]{1,0:T(8,128)(2,1)S(1)}, bf16[136,2048]{1,0:T(8,128)(2,1)S(1)}, u32[]{:S(2)}, u32[]{:S(2)}) collective-permute-start(bf16[136,2048]{1,0:T(8,128)(2,1)S(1)} %pack.1.message_ref), channel_id=1, source_target_pairs={{0,8},{1,9},{2,10},{3,11},{4,12},{5,13},{6,14},{7,15},{8,0},{9,1},... | collective-permute-start | bytes 1671176 | tf_op jit(solution)/shard_map/ppermute | solution.py:29
  4.8 1.5 %collective-permute-start.11 = (bf16[136,2048]{1,0:T(8,128)(2,1)S(1)}, bf16[136,2048]{1,0:T(8,128)(2,1)S(1)}, u32[]{:S(2)}, u32[]{:S(2)}) collective-permute-start(bf16[136,2048]{1,0:T(8,128)(2,1)S(1)} %pack.1.message_ref), channel_id=1, source_target_pairs={{0,16},{1,17},{2,18},{3,19},{4,20},{5,21},{6,22},{7,23},{8,24},{9,... | collective-permute-start | bytes 1671176 | tf_op jit(solution)/shard_map/ppermute | solution.py:29
  6.3 0.0 collective-permute-start.17
  6.3 11.9 %collective-permute-done.9.refs_4_ = bf16[136,2048]{1,0:T(8,128)(2,1)S(1)} collective-permute-done((bf16[136,2048]{1,0:T(8,128)(2,1)S(1)}, bf16[136,2048]{1,0:T(8,128)(2,1)S(1)}, u32[]{:S(2)}, u32[]{:S(2)}) %collective-permute-start.9) | collective-permute-done | bytes 557088 | tf_op jit(solution)/shard_map/ppermute | solution.py:29
  18.2 0.0 collective-permute-start.10
  18.3 12.5 %collective-permute-done.11.refs_6_ = bf16[136,2048]{1,0:T(8,128)(2,1)S(1)} collective-permute-done((bf16[136,2048]{1,0:T(8,128)(2,1)S(1)}, bf16[136,2048]{1,0:T(8,128)(2,1)S(1)}, u32[]{:S(2)}, u32[]{:S(2)}) %collective-permute-start.11) | collective-permute-done | bytes 557088 | tf_op jit(solution)/shard_map/ppermute | solution.py:29
  30.8 6.8 %own.1 = (bf16[128,2048]{1,0:T(8,128)(2,1)S(1)}, bf16[128,2048]{1,0:T(8,128)(2,1)S(1)}, bf16[2,2048,512]{2,1,0:T(8,128)(2,1)S(1)}, bf16[2,2048,512]{2,1,0:T(8,128)(2,1)S(1)}, bf16[1024,2048]{1,0:T(8,128)(2,1)S(1)}) custom-call(f32[1,2048]{1,0:T(1,128)} %bitcast.11, bf16[256,2048]{1,0:T(8,128)(2,1)} %rows_in.1, bf16[2,2048,512]{2,1,0:T(8,128)(2,1)} %gate_in.1, ...), custom_call_target="tpu_custom_call" | custom-call | flops 3221225472 | bytes 14680064 | tf_op jit(solution)/shard_map/own/pallas_call | solution.py:262
  37.6 0.0 collective-permute-done.17.refs_4_
  37.6 0.6 collective-permute-start.18
  38.2 0.0 collective-permute-done.10.refs_5_
  38.2 0.0 collective-permute-done.12.refs_7_
  38.3 0.0 copy-start.5
  38.3 0.0 copy-start
  38.3 8.0 %experts.2 = (bf16[128,2048]{1,0:T(8,128)(2,1)S(1)}, bf16[128,2048]{1,0:T(8,128)(2,1)S(1)}, bf16[128,2048]{1,0:T(8,128)(2,1)S(1)}, bf16[128,2048]{1,0:T(8,128)(2,1)S(1)}) custom-call(f32[1,2048]{1,0:T(1,128)S(1)} %bitcast.12, bf16[2,2048,512]{2,1,0:T(8,128)(2,1)S(1)} %get-tuple-element.19.refs_1_, bf16[2,2048,512]{2,1,0:T(8,128)(2,1)S(1)} %get-tuple-element.20.refs_2_, ...), custom_call_target="tpu_custom_call" | custom-call | flops 6442450944 | bytes 4194304 | tf_op jit(solution)/shard_map/experts/pallas_call | solution.py:309
  46.3 0.2 collective-permute-start.13
  46.5 1.6 %collective-permute-start.2 = (bf16[128,2048]{1,0:T(8,128)(2,1)S(1)}, bf16[128,2048]{1,0:T(8,128)(2,1)S(1)}, u32[]{:S(2)}, u32[]{:S(2)}) collective-permute-start(bf16[128,2048]{1,0:T(8,128)(2,1)S(1)} %copy-done.5), channel_id=1, source_target_pairs={{0,2},{1,3},{2,0},{3,1},{4,6},{5,7},{6,4},{7,5},{8,10},{9,11},{10,... | collective-permute-start | bytes 1572872 | tf_op jit(solution)/shard_map/ppermute | solution.py:29
  48.1 2.6 %collective-permute-start.4 = (bf16[128,2048]{1,0:T(8,128)(2,1)S(1)}, bf16[128,2048]{1,0:T(8,128)(2,1)S(1)}, u32[]{:S(2)}, u32[]{:S(2)}) collective-permute-start(bf16[128,2048]{1,0:T(8,128)(2,1)S(1)} %copy-done.5), channel_id=1, source_target_pairs={{0,4},{1,5},{2,6},{3,7},{4,0},{5,1},{6,2},{7,3},{8,12},{9,13},{10,... | collective-permute-start | bytes 1572872 | tf_op jit(solution)/shard_map/ppermute | solution.py:29
  50.7 0.0 copy-start.1
  50.7 0.0 copy-start.4
  50.7 0.6 collective-permute-start.15
  51.3 4.4 %experts.3 = (bf16[128,2048]{1,0:T(8,128)(2,1)S(1)}, bf16[128,2048]{1,0:T(8,128)(2,1)S(1)}) custom-call(f32[1,2048]{1,0:T(1,128)S(1)} %bitcast.13, bf16[2,2048,512]{2,1,0:T(8,128)(2,1)S(1)} %get-tuple-element.19.refs_1_, bf16[2,2048,512]{2,1,0:T(8,128)(2,1)S(1)} %get-tuple-element.20.refs_2_, bf16[1024,2048]{1,0:T(8,128)(2,1)S(1)} %get-tuple-element.21.refs_3_, ...), custom_call_target="tpu_custom_call" | custom-call | flops 3221225472 | bytes 2097152 | tf_op jit(solution)/shard_map/experts/pallas_call | solution.py:309
  55.7 0.1 collective-permute-start.19
  55.8 0.1 add_convert_fusion.2
  55.9 2.4 %collective-permute-start = (bf16[16,1024]{1,0:T(8,128)(2,1)S(1)}, bf16[16,1024]{1,0:T(8,128)(2,1)S(1)}, u32[]{:S(2)}, u32[]{:S(2)}) collective-permute-start(bf16[16,1024]{1,0:T(8,128)(2,1)S(1)} %slice.3), channel_id=1, source_target_pairs={{0,1},{1,2},{2,3},{3,4},{4,5},{5,6},{6,7},{7,8},{8,9},{9,10},{10,1... | collective-permute-start | bytes 98312 | tf_op jit(solution)/shard_map/ppermute | solution.py:19
  58.3 0.1 add_convert_fusion.1
  58.5 0.7 collective-permute-done.rim_ref
  59.2 15.2 %collective-permute-start.6 = (bf16[128,2048]{1,0:T(8,128)(2,1)S(1)}, bf16[128,2048]{1,0:T(8,128)(2,1)S(1)}, u32[]{:S(2)}, u32[]{:S(2)}) collective-permute-start(bf16[128,2048]{1,0:T(8,128)(2,1)S(1)} %copy-done.5), channel_id=1, source_target_pairs={{0,6},{1,7},{2,4},{3,5},{4,2},{5,3},{6,0},{7,1},{8,14},{9,15},{10,... | collective-permute-start | bytes 1572872 | tf_op jit(solution)/shard_map/ppermute | solution.py:29
  74.4 1.2 collective-permute-start.14
  75.6 1.5 %collective-permute-start.16 = (bf16[128,2048]{1,0:T(8,128)(2,1)S(1)}, bf16[128,2048]{1,0:T(8,128)(2,1)S(1)}, u32[]{:S(2)}, u32[]{:S(2)}) collective-permute-start(bf16[128,2048]{1,0:T(8,128)(2,1)S(1)} %add_convert_fusion.1), channel_id=1, source_target_pairs={{0,16},{1,17},{2,18},{3,19},{4,20},{5,21},{6,22},{7,23},{8,24},{9,... | collective-permute-start | bytes 1572872 | tf_op jit(solution)/shard_map/ppermute | solution.py:29
  77.2 1.2 mix.1.mixed_ref
  78.4 0.1 add_convert_fusion
  78.5 0.1 collective-permute-start.1
  78.6 0.5 collective-permute-start.3
  79.1 7.9 %collective-permute-done.6.refs_6_ = bf16[128,2048]{1,0:T(8,128)(2,1)S(1)} collective-permute-done((bf16[128,2048]{1,0:T(8,128)(2,1)S(1)}, bf16[128,2048]{1,0:T(8,128)(2,1)S(1)}, u32[]{:S(2)}, u32[]{:S(2)}) %collective-permute-start.6) | collective-permute-done | bytes 524320 | tf_op jit(solution)/shard_map/ppermute | solution.py:29
  87.0 0.3 collective-permute-done.14
  87.3 0.2 collective-permute-start.7
  87.5 2.5 %collective-permute-start.20 = (bf16[128,2048]{1,0:T(8,128)(2,1)S(1)}, bf16[128,2048]{1,0:T(8,128)(2,1)S(1)}, u32[]{:S(2)}, u32[]{:S(2)}) collective-permute-start(bf16[128,2048]{1,0:T(8,128)(2,1)S(1)} %add_convert_fusion), channel_id=1, source_target_pairs={{0,24},{1,25},{2,26},{3,27},{4,28},{5,29},{6,30},{7,31},{8,16},{9,... | collective-permute-start | bytes 1572872 | tf_op jit(solution)/shard_map/ppermute | solution.py:29
  90.0 0.3 convert_add_fusion
  90.3 12.2 %collective-permute-done.20 = bf16[128,2048]{1,0:T(8,128)(2,1)S(1)} collective-permute-done((bf16[128,2048]{1,0:T(8,128)(2,1)S(1)}, bf16[128,2048]{1,0:T(8,128)(2,1)S(1)}, u32[]{:S(2)}, u32[]{:S(2)}) %collective-permute-start.20) | collective-permute-done | bytes 524320 | tf_op jit(solution)/shard_map/ppermute | solution.py:29
  102.6 0.1 spread.1
  102.7 0.0 copy-start.3
  102.7 11.5 %collective-permute-start.21 = (bf16[32,2048]{1,0:T(8,128)(2,1)S(1)}, bf16[32,2048]{1,0:T(8,128)(2,1)S(1)}, u32[]{:S(2)}, u32[]{:S(2)}) collective-permute-start(bf16[32,2048]{1,0:T(8,128)(2,1)S(1)} %get-tuple-element.29), channel_id=1, source_target_pairs={{0,2},{1,3},{2,0},{3,1},{4,6},{5,7},{6,4},{7,5},{8,10},{9,11},{10,... | collective-permute-start | bytes 393224 | tf_op jit(solution)/shard_map/ppermute | solution.py:29
  114.2 0.1 collective-permute-start.22
  114.2 2.4 %collective-permute-start.23 = (bf16[32,2048]{1,0:T(8,128)(2,1)S(1)}, bf16[32,2048]{1,0:T(8,128)(2,1)S(1)}, u32[]{:S(2)}, u32[]{:S(2)}) collective-permute-start(bf16[32,2048]{1,0:T(8,128)(2,1)S(1)} %get-tuple-element.31), channel_id=1, source_target_pairs={{0,6},{1,7},{2,4},{3,5},{4,2},{5,3},{6,0},{7,1},{8,14},{9,15},{10,... | collective-permute-start | bytes 393224 | tf_op jit(solution)/shard_map/ppermute | solution.py:29
  116.6 4.3 %project.1 = bf16[512,2048]{1,0:T(8,128)(2,1)} custom-call(bf16[512,1024]{1,0:T(8,128)(2,1)S(1)} %mix.1.mixed_ref, f32[1,2048]{1,0:T(1,128)S(1)} %bitcast.16, bf16[128,2048]{1,0:T(8,128)(2,1)S(1)} %copy-done.5, bf16[128,2048]{1,0:T(8,128)(2,1)S(1)} %collective-permute-done.1.refs_1_, bf16[128,2048]{1,0:T(8,128)(2,1)S(1)} %collective-permute-done.2.refs_2_, ...), custom_call_target="tpu_custom_call" | custom-call | flops 2147483648 | bytes 7340032 | tf_op jit(solution)/shard_map/project/pallas_call | solution.py:475
  120.9 4.7 %collective-permute-done.22.refs_1_ = bf16[32,2048]{1,0:T(8,128)(2,1)S(1)} collective-permute-done((bf16[32,2048]{1,0:T(8,128)(2,1)S(1)}, bf16[32,2048]{1,0:T(8,128)(2,1)S(1)}, u32[]{:S(2)}, u32[]{:S(2)}) %collective-permute-start.22) | collective-permute-done | bytes 131104 | tf_op jit(solution)/shard_map/ppermute | solution.py:29
  125.6 0.8 finish.1
  (27 shorter events, 0.1 us)
Async XLA Ops:
  1.7 16.5 %collective-permute-start.9 = (bf16[136,2048]{1,0:T(8,128)(2,1)S(1)}, bf16[136,2048]{1,0:T(8,128)(2,1)S(1)}, u32[]{:S(2)}, u32[]{:S(2)}) collective-permute-start(bf16[136,2048]{1,0:T(8,128)(2,1)S(1)} %pack.1.message_ref), channel_id=1, source_target_pairs={{0,8},{1,9},{2,10},{3,11},{4,12},{5,13},{6,14},{7,15},{8,0},{9,1},... | collective-permute-start | bytes 1671176 | tf_op jit(solution)/shard_map/ppermute | solution.py:29
  4.8 26.0 %collective-permute-start.11 = (bf16[136,2048]{1,0:T(8,128)(2,1)S(1)}, bf16[136,2048]{1,0:T(8,128)(2,1)S(1)}, u32[]{:S(2)}, u32[]{:S(2)}) collective-permute-start(bf16[136,2048]{1,0:T(8,128)(2,1)S(1)} %pack.1.message_ref), channel_id=1, source_target_pairs={{0,16},{1,17},{2,18},{3,19},{4,20},{5,21},{6,22},{7,23},{8,24},{9,... | collective-permute-start | bytes 1671176 | tf_op jit(solution)/shard_map/ppermute | solution.py:29
  6.3 31.4 %collective-permute-start.17 = (bf16[136,2048]{1,0:T(8,128)(2,1)S(1)}, bf16[136,2048]{1,0:T(8,128)(2,1)S(1)}, u32[]{:S(2)}, u32[]{:S(2)}) collective-permute-start(bf16[136,2048]{1,0:T(8,128)(2,1)S(1)} %pack.1.message_ref), channel_id=1, source_target_pairs={{0,24},{1,25},{2,26},{3,27},{4,28},{5,29},{6,30},{7,31},{8,16},{9,... | collective-permute-start | bytes 1671176 | tf_op jit(solution)/shard_map/ppermute | solution.py:29
  18.2 20.0 %collective-permute-start.10 = (bf16[136,2048]{1,0:T(8,128)(2,1)S(1)}, bf16[136,2048]{1,0:T(8,128)(2,1)S(1)}, u32[]{:S(2)}, u32[]{:S(2)}) collective-permute-start(bf16[136,2048]{1,0:T(8,128)(2,1)S(1)} %collective-permute-done.9.refs_4_), channel_id=1, source_target_pairs={{0,1},{1,0},{2,3},{3,2},{4,5},{5,4},{6,7},{7,6},{8,9},{9,8},{10,11... | collective-permute-start | bytes 1671176 | tf_op jit(solution)/shard_map/ppermute | solution.py:29
  30.8 7.5 %collective-permute-start.12 = (bf16[136,2048]{1,0:T(8,128)(2,1)S(1)}, bf16[136,2048]{1,0:T(8,128)(2,1)S(1)}, u32[]{:S(2)}, u32[]{:S(2)}) collective-permute-start(bf16[136,2048]{1,0:T(8,128)(2,1)S(1)} %collective-permute-done.11.refs_6_), channel_id=1, source_target_pairs={{0,1},{1,0},{2,3},{3,2},{4,5},{5,4},{6,7},{7,6},{8,9},{9,8},{10,11... | collective-permute-start | bytes 1671176 | tf_op jit(solution)/shard_map/ppermute | solution.py:29
  30.8 7.5 %copy-start.2 = (f32[2048]{0:T(1024)S(1)}, f32[2048]{0:T(1024)}, u32[]{:S(2)}) copy-start(f32[2048]{0:T(1024)} %param.21) | copy-start | bytes 24580
  37.6 13.0 %collective-permute-start.18 = (bf16[136,2048]{1,0:T(8,128)(2,1)S(1)}, bf16[136,2048]{1,0:T(8,128)(2,1)S(1)}, u32[]{:S(2)}, u32[]{:S(2)}) collective-permute-start(bf16[136,2048]{1,0:T(8,128)(2,1)S(1)} %collective-permute-done.17.refs_4_), channel_id=1, source_target_pairs={{0,1},{1,0},{2,3},{3,2},{4,5},{5,4},{6,7},{7,6},{8,9},{9,8},{10,11... | collective-permute-start | bytes 1671176 | tf_op jit(solution)/shard_map/ppermute | solution.py:29
  38.3 8.2 %copy-start.5 = (bf16[128,2048]{1,0:T(8,128)(2,1)S(1)}, bf16[128,2048]{1,0:T(8,128)(2,1)}, u32[]{:S(2)}) copy-start(bf16[128,2048]{1,0:T(8,128)(2,1)} %refs_0_.1) | copy-start | bytes 1572868
  38.3 12.4 %copy-start = (bf16[512,1024]{1,0:T(8,128)(2,1)S(1)}, bf16[512,1024]{1,0:T(8,128)(2,1)}, u32[]{:S(2)}) copy-start(bf16[512,1024]{1,0:T(8,128)(2,1)} %rows_ref.2) | copy-start | bytes 3145732
  46.3 9.4 %collective-permute-start.13 = (bf16[128,2048]{1,0:T(8,128)(2,1)S(1)}, bf16[128,2048]{1,0:T(8,128)(2,1)S(1)}, u32[]{:S(2)}, u32[]{:S(2)}) collective-permute-start(bf16[128,2048]{1,0:T(8,128)(2,1)S(1)} %get-tuple-element.23), channel_id=1, source_target_pairs={{0,1},{1,0},{2,3},{3,2},{4,5},{5,4},{6,7},{7,6},{8,9},{9,8},{10,11... | collective-permute-start | bytes 1572872 | tf_op jit(solution)/shard_map/ppermute | solution.py:29
  46.5 32.1 %collective-permute-start.2 = (bf16[128,2048]{1,0:T(8,128)(2,1)S(1)}, bf16[128,2048]{1,0:T(8,128)(2,1)S(1)}, u32[]{:S(2)}, u32[]{:S(2)}) collective-permute-start(bf16[128,2048]{1,0:T(8,128)(2,1)S(1)} %copy-done.5), channel_id=1, source_target_pairs={{0,2},{1,3},{2,0},{3,1},{4,6},{5,7},{6,4},{7,5},{8,10},{9,11},{10,... | collective-permute-start | bytes 1572872 | tf_op jit(solution)/shard_map/ppermute | solution.py:29
  48.1 30.6 %collective-permute-start.4 = (bf16[128,2048]{1,0:T(8,128)(2,1)S(1)}, bf16[128,2048]{1,0:T(8,128)(2,1)S(1)}, u32[]{:S(2)}, u32[]{:S(2)}) collective-permute-start(bf16[128,2048]{1,0:T(8,128)(2,1)S(1)} %copy-done.5), channel_id=1, source_target_pairs={{0,4},{1,5},{2,6},{3,7},{4,0},{5,1},{6,2},{7,3},{8,12},{9,13},{10,... | collective-permute-start | bytes 1572872 | tf_op jit(solution)/shard_map/ppermute | solution.py:29
  50.7 23.8 %collective-permute-start.8 = (bf16[128,2048]{1,0:T(8,128)(2,1)S(1)}, bf16[128,2048]{1,0:T(8,128)(2,1)S(1)}, u32[]{:S(2)}, u32[]{:S(2)}) collective-permute-start(bf16[128,2048]{1,0:T(8,128)(2,1)S(1)} %get-tuple-element.18), channel_id=1, source_target_pairs={{0,1},{1,0},{2,3},{3,2},{4,5},{5,4},{6,7},{7,6},{8,9},{9,8},{10,11... | collective-permute-start | bytes 1572872 | tf_op jit(solution)/shard_map/ppermute | solution.py:29
  50.7 26.5 %copy-start.1 = (bf16[4,256,256]{2,1,0:T(8,128)(2,1)S(1)}, bf16[4,256,256]{2,1,0:T(8,128)(2,1)}, u32[]{:S(2)}) copy-start(bf16[4,256,256]{2,1,0:T(8,128)(2,1)} %weight_ref.1) | copy-start | bytes 1572868
  50.7 26.5 %copy-start.4 = (f32[1024]{0:T(1024)S(1)}, f32[1024]{0:T(1024)}, u32[]{:S(2)}) copy-start(f32[1024]{0:T(1024)} %param.15) | copy-start | bytes 12292
  50.7 5.2 %collective-permute-start.15 = (bf16[128,2048]{1,0:T(8,128)(2,1)S(1)}, bf16[128,2048]{1,0:T(8,128)(2,1)S(1)}, u32[]{:S(2)}, u32[]{:S(2)}) collective-permute-start(bf16[128,2048]{1,0:T(8,128)(2,1)S(1)} %get-tuple-element.25), channel_id=1, source_target_pairs={{0,1},{1,0},{2,3},{3,2},{4,5},{5,4},{6,7},{7,6},{8,9},{9,8},{10,11... | collective-permute-start | bytes 1572872 | tf_op jit(solution)/shard_map/ppermute | solution.py:29
  55.7 19.9 %collective-permute-start.19 = (bf16[128,2048]{1,0:T(8,128)(2,1)S(1)}, bf16[128,2048]{1,0:T(8,128)(2,1)S(1)}, u32[]{:S(2)}, u32[]{:S(2)}) collective-permute-start(bf16[128,2048]{1,0:T(8,128)(2,1)S(1)} %get-tuple-element.27), channel_id=1, source_target_pairs={{0,1},{1,0},{2,3},{3,2},{4,5},{5,4},{6,7},{7,6},{8,9},{9,8},{10,11... | collective-permute-start | bytes 1572872 | tf_op jit(solution)/shard_map/ppermute | solution.py:29
  55.9 3.2 %collective-permute-start = (bf16[16,1024]{1,0:T(8,128)(2,1)S(1)}, bf16[16,1024]{1,0:T(8,128)(2,1)S(1)}, u32[]{:S(2)}, u32[]{:S(2)}) collective-permute-start(bf16[16,1024]{1,0:T(8,128)(2,1)S(1)} %slice.3), channel_id=1, source_target_pairs={{0,1},{1,2},{2,3},{3,4},{4,5},{5,6},{6,7},{7,8},{8,9},{9,10},{10,1... | collective-permute-start | bytes 98312 | tf_op jit(solution)/shard_map/ppermute | solution.py:19
  59.2 27.8 %collective-permute-start.6 = (bf16[128,2048]{1,0:T(8,128)(2,1)S(1)}, bf16[128,2048]{1,0:T(8,128)(2,1)S(1)}, u32[]{:S(2)}, u32[]{:S(2)}) collective-permute-start(bf16[128,2048]{1,0:T(8,128)(2,1)S(1)} %copy-done.5), channel_id=1, source_target_pairs={{0,6},{1,7},{2,4},{3,5},{4,2},{5,3},{6,0},{7,1},{8,14},{9,15},{10,... | collective-permute-start | bytes 1572872 | tf_op jit(solution)/shard_map/ppermute | solution.py:29
  74.4 12.9 %collective-permute-start.14 = (bf16[128,2048]{1,0:T(8,128)(2,1)S(1)}, bf16[128,2048]{1,0:T(8,128)(2,1)S(1)}, u32[]{:S(2)}, u32[]{:S(2)}) collective-permute-start(bf16[128,2048]{1,0:T(8,128)(2,1)S(1)} %add_convert_fusion.2), channel_id=1, source_target_pairs={{0,8},{1,9},{2,10},{3,11},{4,12},{5,13},{6,14},{7,15},{8,0},{9,1},... | collective-permute-start | bytes 1572872 | tf_op jit(solution)/shard_map/ppermute | solution.py:29
  75.6 11.9 %collective-permute-start.16 = (bf16[128,2048]{1,0:T(8,128)(2,1)S(1)}, bf16[128,2048]{1,0:T(8,128)(2,1)S(1)}, u32[]{:S(2)}, u32[]{:S(2)}) collective-permute-start(bf16[128,2048]{1,0:T(8,128)(2,1)S(1)} %add_convert_fusion.1), channel_id=1, source_target_pairs={{0,16},{1,17},{2,18},{3,19},{4,20},{5,21},{6,22},{7,23},{8,24},{9,... | collective-permute-start | bytes 1572872 | tf_op jit(solution)/shard_map/ppermute | solution.py:29
  77.2 39.5 %copy-start.6 = (f32[2048]{0:T(1024)S(1)}, f32[2048]{0:T(1024)}, u32[]{:S(2)}) copy-start(f32[2048]{0:T(1024)} %param.17) | copy-start | bytes 24580
  78.5 35.6 %collective-permute-start.1 = (bf16[128,2048]{1,0:T(8,128)(2,1)S(1)}, bf16[128,2048]{1,0:T(8,128)(2,1)S(1)}, u32[]{:S(2)}, u32[]{:S(2)}) collective-permute-start(bf16[128,2048]{1,0:T(8,128)(2,1)S(1)} %copy-done.5), channel_id=1, source_target_pairs={{0,1},{1,0},{2,3},{3,2},{4,5},{5,4},{6,7},{7,6},{8,9},{9,8},{10,11... | collective-permute-start | bytes 1572872 | tf_op jit(solution)/shard_map/ppermute | solution.py:29
  78.6 35.6 %collective-permute-start.3 = (bf16[128,2048]{1,0:T(8,128)(2,1)S(1)}, bf16[128,2048]{1,0:T(8,128)(2,1)S(1)}, u32[]{:S(2)}, u32[]{:S(2)}) collective-permute-start(bf16[128,2048]{1,0:T(8,128)(2,1)S(1)} %collective-permute-done.2.refs_2_), channel_id=1, source_target_pairs={{0,1},{1,0},{2,3},{3,2},{4,5},{5,4},{6,7},{7,6},{8,9},{9,8},{10,11... | collective-permute-start | bytes 1572872 | tf_op jit(solution)/shard_map/ppermute | solution.py:29
  87.0 29.6 %collective-permute-start.5 = (bf16[128,2048]{1,0:T(8,128)(2,1)S(1)}, bf16[128,2048]{1,0:T(8,128)(2,1)S(1)}, u32[]{:S(2)}, u32[]{:S(2)}) collective-permute-start(bf16[128,2048]{1,0:T(8,128)(2,1)S(1)} %collective-permute-done.4.refs_4_), channel_id=1, source_target_pairs={{0,1},{1,0},{2,3},{3,2},{4,5},{5,4},{6,7},{7,6},{8,9},{9,8},{10,11... | collective-permute-start | bytes 1572872 | tf_op jit(solution)/shard_map/ppermute | solution.py:29
  87.3 29.3 %collective-permute-start.7 = (bf16[128,2048]{1,0:T(8,128)(2,1)S(1)}, bf16[128,2048]{1,0:T(8,128)(2,1)S(1)}, u32[]{:S(2)}, u32[]{:S(2)}) collective-permute-start(bf16[128,2048]{1,0:T(8,128)(2,1)S(1)} %collective-permute-done.6.refs_6_), channel_id=1, source_target_pairs={{0,1},{1,0},{2,3},{3,2},{4,5},{5,4},{6,7},{7,6},{8,9},{9,8},{10,11... | collective-permute-start | bytes 1572872 | tf_op jit(solution)/shard_map/ppermute | solution.py:29
  87.5 15.0 %collective-permute-start.20 = (bf16[128,2048]{1,0:T(8,128)(2,1)S(1)}, bf16[128,2048]{1,0:T(8,128)(2,1)S(1)}, u32[]{:S(2)}, u32[]{:S(2)}) collective-permute-start(bf16[128,2048]{1,0:T(8,128)(2,1)S(1)} %add_convert_fusion), channel_id=1, source_target_pairs={{0,24},{1,25},{2,26},{3,27},{4,28},{5,29},{6,30},{7,31},{8,16},{9,... | collective-permute-start | bytes 1572872 | tf_op jit(solution)/shard_map/ppermute | solution.py:29
  102.7 23.0 %copy-start.3 = (f32[2048]{0:T(1024)S(1)}, f32[2048]{0:T(1024)}, u32[]{:S(2)}) copy-start(f32[2048]{0:T(1024)} %param.25) | copy-start | bytes 24580
  102.7 18.3 %collective-permute-start.21 = (bf16[32,2048]{1,0:T(8,128)(2,1)S(1)}, bf16[32,2048]{1,0:T(8,128)(2,1)S(1)}, u32[]{:S(2)}, u32[]{:S(2)}) collective-permute-start(bf16[32,2048]{1,0:T(8,128)(2,1)S(1)} %get-tuple-element.29), channel_id=1, source_target_pairs={{0,2},{1,3},{2,0},{3,1},{4,6},{5,7},{6,4},{7,5},{8,10},{9,11},{10,... | collective-permute-start | bytes 393224 | tf_op jit(solution)/shard_map/ppermute | solution.py:29
  114.2 11.4 %collective-permute-start.22 = (bf16[32,2048]{1,0:T(8,128)(2,1)S(1)}, bf16[32,2048]{1,0:T(8,128)(2,1)S(1)}, u32[]{:S(2)}, u32[]{:S(2)}) collective-permute-start(bf16[32,2048]{1,0:T(8,128)(2,1)S(1)} %get-tuple-element.30), channel_id=1, source_target_pairs={{0,4},{1,5},{2,6},{3,7},{4,0},{5,1},{6,2},{7,3},{8,12},{9,13},{10,... | collective-permute-start | bytes 393224 | tf_op jit(solution)/shard_map/ppermute | solution.py:29
  114.2 11.4 %collective-permute-start.23 = (bf16[32,2048]{1,0:T(8,128)(2,1)S(1)}, bf16[32,2048]{1,0:T(8,128)(2,1)S(1)}, u32[]{:S(2)}, u32[]{:S(2)}) collective-permute-start(bf16[32,2048]{1,0:T(8,128)(2,1)S(1)} %get-tuple-element.31), channel_id=1, source_target_pairs={{0,6},{1,7},{2,4},{3,5},{4,2},{5,3},{6,0},{7,1},{8,14},{9,15},{10,... | collective-permute-start | bytes 393224 | tf_op jit(solution)/shard_map/ppermute | solution.py:29

commit v3 on v2

--- a/solution.py
+++ b/solution.py
@@ -33,8 +33,9 @@
     return moved(block, lambda e, t: (e, t ^ 1))
 
 
-def to_group(block, mask):
-    return moved(block, lambda e, t: (e ^ mask, t))
+def to_group(block, turn):
+    masks = (1, 2) if turn == 0 else (2, 1)
+    return moved(block, lambda e, t: (e ^ masks[t % CORES], t))
 
 
 def paired(chips):
@@ -372,40 +373,43 @@
     )(gain.reshape(1, -1), own, *parts)
 
 
+def added(left, right):
+    return (left.astype(jnp.float32) + right.astype(jnp.float32)).astype(jnp.bfloat16)
+
+
 def dense_experts(
     expert_in, routes, route_weight, pre_gain, gate_weight, up_weight, down_weight, post_gain
 ):
     tokens, width = expert_in.shape
-    groups = lax.axis_size("ep")
     chips = lax.axis_size("tp") // CORES
     block = tokens // lax.axis_size("tp")
-    masks = range(1, groups)
     message = pack(expert_in, routes, route_weight)
-    mine_from = {}
-    for m in masks:
-        mine_from[m] = to_group(message, m)
+    from_a = to_group(message, 0)
+    from_b = to_group(message, 1)
     weights = (pre_gain, gate_weight, up_weight, down_weight.reshape(-1, width), block)
     kept, sent, *held = own_partial(expert_in, message, *weights)
     weights = (pre_gain, *held, block)
     early = kept.astype(jnp.float32) + to_core(sent).astype(jnp.float32)
-    near = [m for m in masks if m & (m - 1) == 0]
-    far = [m for m in masks if m & (m - 1) != 0]
-    returned = {}
-    for batch in (near, far):
-        chunks = []
-        for m in batch:
-            chunks.append((mine_from[m], to_core(mine_from[m])))
-        results = expert_partial(chunks, *weights)
-        for m, (kept, sent) in zip(batch, results):
-            partner = to_core(sent)
-            joined = (kept.astype(jnp.float32) + partner.astype(jnp.float32)).astype(jnp.bfloat16)
-            returned[m] = to_group(joined, m)
-    for m in masks[:-1]:
-        early = early + returned[m].astype(jnp.float32)
-    early = lax.optimization_barrier(early)
+    from_c = to_group(from_a, 1)
+    other_b = to_core(from_a)
+    other_a = to_core(from_b)
+    other_c = to_core(from_c)
+    near = expert_partial([(from_a, other_a), (from_b, other_b)], *weights)
+    (kept_a, sent_a), (kept_b, sent_b) = near
+    back_a = to_core(sent_b)
+    back_b = to_core(sent_a)
+    joined_a = added(kept_a, back_a)
+    joined_b = added(kept_b, back_b)
+    near_sum = to_group(joined_a, 0)
+    ((kept_c, sent_c),) = expert_partial([(from_c, other_c)], *weights)
+    back_c = to_core(sent_c)
+    joined_c = added(kept_c, back_c)
+    passing = to_group(joined_c, 0)
+    passed = added(joined_b, passing)
+    far_sum = to_group(passed, 1)
+    early = lax.optimization_barrier(early + near_sum.astype(jnp.float32))
     own, *pieces = spread(
-        early.reshape(chips, block, width),
-        returned[masks[-1]].reshape(chips, block, width),
+        early.reshape(chips, block, width), far_sum.reshape(chips, block, width)
     )
     parts = []
     for step in range(1, chips):
@@ -515,7 +519,7 @@
     block_tokens = tokens_here // tp_count
     capacity = 2 * block_tokens * choose // (gate_weight.shape[0] * ep_count)
     experts_in_all = gate_weight.shape[0] * ep_count
-    dense = capacity >= block_tokens and ep_count & (ep_count - 1) == 0
+    dense = capacity >= block_tokens and ep_count == 4
     dense = dense and experts_in_all * tokens_here <= expert_in.shape[1]
     experts = dense_experts if dense else routed_experts
     rim = shifted(pool_in[rows - 16 :], ("ep", "tp"), 1)

time: 127 us -> 135 us (1.063)
  starting transfers between devices: 47.8 us -> 71.5 us
  waiting for transfers between devices: 50.3 us -> 35 us
    ppermute x23, starting transfers between devices: 45.4 us -> 69.4 us  [moved(): return lax.ppermute(block, ('ep', 'tp'), route)]
    ppermute x23, waiting for transfers between devices: 49.6 us -> 34.2 us  [moved(): return lax.ppermute(block, ('ep', 'tp'), route)]
  transfers between devices with their start and end apart: 24 -> 24, of which waited for: 7 -> 8; matrix products, arithmetic and copies ran while one was open for 1% -> 1% of each run, Pallas kernels for 20% -> 18%
where the time goes in v3:
time: 135 us
  starting transfers between devices  71.5 us (53%)
  waiting for transfers between devices  35 us (26%)
  Pallas kernels  26.8 us (20%)
    ppermute x23, starting transfers between devices, moved(): return lax.ppermute(block, ('ep', 'tp'), route)  69.4 us
    ppermute x23, waiting for transfers between devices, moved(): return lax.ppermute(block, ('ep', 'tp'), route)  34.2 us
    pallas_call x2, Pallas kernels, expert_partial(): pl.pallas_call(lambda *refs: expert_kernel(*refs, groups=groups), in_spec...  12.4 us
    pallas_call x1, Pallas kernels, own_partial(): pl.pallas_call(own_kernel, in_specs=[HBM] * 5 + [VMEM], out_specs=[VMEM]...  6.83 us
    pallas_call x1, Pallas kernels, project(): pl.pallas_call(project_kernel, grid=(rows // tile,), in_specs=[pl.BlockSp...  4.27 us
  transfers between devices with their start and end apart: 24, of which 8 were waited for; matrix products, arithmetic and copies ran while one was open for 1% of the time, Pallas kernels for 18%

profile of v3, /device:TPU:0, one launch (start us, length us, event | category | flops | bytes accessed | tf_op | source)
XLA Modules:
  0.0 134.8 jit_solution(252523832647899974)
XLA Ops:
  0.6 1.1 pack.1.message_ref
  1.7 3.0 %collective-permute-start.9 = (bf16[136,2048]{1,0:T(8,128)(2,1)S(1)}, bf16[136,2048]{1,0:T(8,128)(2,1)S(1)}, u32[]{:S(2)}, u32[]{:S(2)}) collective-permute-start(bf16[136,2048]{1,0:T(8,128)(2,1)S(1)} %pack.1.message_ref), channel_id=1, source_target_pairs={{0,8},{1,17},{2,10},{3,19},{4,12},{5,21},{6,14},{7,23},{8,0},{9,25... | collective-permute-start | bytes 1671176 | tf_op jit(solution)/shard_map/ppermute | solution.py:29
  4.8 7.5 %collective-permute-done.9.refs_4_ = bf16[136,2048]{1,0:T(8,128)(2,1)S(1)} collective-permute-done((bf16[136,2048]{1,0:T(8,128)(2,1)S(1)}, bf16[136,2048]{1,0:T(8,128)(2,1)S(1)}, u32[]{:S(2)}, u32[]{:S(2)}) %collective-permute-start.9) | collective-permute-done | bytes 557088 | tf_op jit(solution)/shard_map/ppermute | solution.py:29
  12.3 2.0 %collective-permute-start.16 = (bf16[136,2048]{1,0:T(8,128)(2,1)S(1)}, bf16[136,2048]{1,0:T(8,128)(2,1)S(1)}, u32[]{:S(2)}, u32[]{:S(2)}) collective-permute-start(bf16[136,2048]{1,0:T(8,128)(2,1)S(1)} %collective-permute-done.9.refs_4_), channel_id=1, source_target_pairs={{0,16},{1,9},{2,18},{3,11},{4,20},{5,13},{6,22},{7,15},{8,24},{9,1... | collective-permute-start | bytes 1671176 | tf_op jit(solution)/shard_map/ppermute | solution.py:29
  14.3 0.0 collective-permute-start.10
  14.4 7.5 %collective-permute-done.16.refs_4_ = bf16[136,2048]{1,0:T(8,128)(2,1)S(1)} collective-permute-done((bf16[136,2048]{1,0:T(8,128)(2,1)S(1)}, bf16[136,2048]{1,0:T(8,128)(2,1)S(1)}, u32[]{:S(2)}, u32[]{:S(2)}) %collective-permute-start.16) | collective-permute-done | bytes 557088 | tf_op jit(solution)/shard_map/ppermute | solution.py:29
  21.8 0.0 collective-permute-start.17
  21.8 0.5 collective-permute-start.12
  22.4 5.5 %collective-permute-done.10.refs_6_ = bf16[136,2048]{1,0:T(8,128)(2,1)S(1)} collective-permute-done((bf16[136,2048]{1,0:T(8,128)(2,1)S(1)}, bf16[136,2048]{1,0:T(8,128)(2,1)S(1)}, u32[]{:S(2)}, u32[]{:S(2)}) %collective-permute-start.10) | collective-permute-done | bytes 557088 | tf_op jit(solution)/shard_map/ppermute | solution.py:29
  27.8 0.0 collective-permute-start.11
  27.8 6.8 %own.1 = (bf16[128,2048]{1,0:T(8,128)(2,1)S(1)}, bf16[128,2048]{1,0:T(8,128)(2,1)S(1)}, bf16[2,2048,512]{2,1,0:T(8,128)(2,1)S(1)}, bf16[2,2048,512]{2,1,0:T(8,128)(2,1)S(1)}, bf16[1024,2048]{1,0:T(8,128)(2,1)S(1)}) custom-call(f32[1,2048]{1,0:T(1,128)} %bitcast.11, bf16[256,2048]{1,0:T(8,128)(2,1)} %rows_in.1, bf16[2,2048,512]{2,1,0:T(8,128)(2,1)} %gate_in.1, ...), custom_call_target="tpu_custom_call" | custom-call | flops 3221225472 | bytes 14680064 | tf_op jit(solution)/shard_map/own/pallas_call | solution.py:263
  34.7 0.0 collective-permute-done.17.refs_5_
  34.7 4.2 %experts.3 = (bf16[128,2048]{1,0:T(8,128)(2,1)S(1)}, bf16[128,2048]{1,0:T(8,128)(2,1)S(1)}) custom-call(f32[1,2048]{1,0:T(1,128)S(1)} %bitcast.12, bf16[2,2048,512]{2,1,0:T(8,128)(2,1)S(1)} %get-tuple-element.19.refs_1_, bf16[2,2048,512]{2,1,0:T(8,128)(2,1)S(1)} %get-tuple-element.20.refs_2_, bf16[1024,2048]{1,0:T(8,128)(2,1)S(1)} %get-tuple-element.21.refs_3_, ...), custom_call_target="tpu_custom_call" | custom-call | flops 3221225472 | bytes 2097152 | tf_op jit(solution)/shard_map/experts/pallas_call | solution.py:310
  38.9 0.0 copy-start.5
  38.9 0.0 copy-start
  38.9 0.6 collective-permute-start.18
  39.6 8.2 %experts.2 = (bf16[128,2048]{1,0:T(8,128)(2,1)S(1)}, bf16[128,2048]{1,0:T(8,128)(2,1)S(1)}, bf16[128,2048]{1,0:T(8,128)(2,1)S(1)}, bf16[128,2048]{1,0:T(8,128)(2,1)S(1)}) custom-call(f32[1,2048]{1,0:T(1,128)S(1)} %bitcast.13, bf16[2,2048,512]{2,1,0:T(8,128)(2,1)S(1)} %get-tuple-element.19.refs_1_, bf16[2,2048,512]{2,1,0:T(8,128)(2,1)S(1)} %get-tuple-element.20.refs_2_, ...), custom_call_target="tpu_custom_call" | custom-call | flops 6442450944 | bytes 4194304 | tf_op jit(solution)/shard_map/experts/pallas_call | solution.py:310
  47.8 0.0 copy-start.1
  47.8 0.0 copy-start.4
  47.8 0.2 collective-permute-start.13
  48.0 0.4 collective-permute-start.15
  48.4 0.1 add_convert_fusion.1
  48.5 2.1 %collective-permute-start.19 = (bf16[128,2048]{1,0:T(8,128)(2,1)S(1)}, bf16[128,2048]{1,0:T(8,128)(2,1)S(1)}, u32[]{:S(2)}, u32[]{:S(2)}) collective-permute-start(bf16[128,2048]{1,0:T(8,128)(2,1)S(1)} %add_convert_fusion.1), channel_id=1, source_target_pairs={{0,8},{1,17},{2,10},{3,19},{4,12},{5,21},{6,14},{7,23},{8,0},{9,25... | collective-permute-start | bytes 1572872 | tf_op jit(solution)/shard_map/ppermute | solution.py:29
  50.6 1.6 %collective-permute-start.2 = (bf16[128,2048]{1,0:T(8,128)(2,1)S(1)}, bf16[128,2048]{1,0:T(8,128)(2,1)S(1)}, u32[]{:S(2)}, u32[]{:S(2)}) collective-permute-start(bf16[128,2048]{1,0:T(8,128)(2,1)S(1)} %copy-done.5), channel_id=1, source_target_pairs={{0,2},{1,3},{2,0},{3,1},{4,6},{5,7},{6,4},{7,5},{8,10},{9,11},{10,... | collective-permute-start | bytes 1572872 | tf_op jit(solution)/shard_map/ppermute | solution.py:29
  52.1 2.1 %collective-permute-start = (bf16[16,1024]{1,0:T(8,128)(2,1)S(1)}, bf16[16,1024]{1,0:T(8,128)(2,1)S(1)}, u32[]{:S(2)}, u32[]{:S(2)}) collective-permute-start(bf16[16,1024]{1,0:T(8,128)(2,1)S(1)} %slice.3), channel_id=1, source_target_pairs={{0,1},{1,2},{2,3},{3,4},{4,5},{5,6},{6,7},{7,8},{8,9},{9,10},{10,1... | collective-permute-start | bytes 98312 | tf_op jit(solution)/shard_map/ppermute | solution.py:19
  54.3 0.1 add_convert_fusion.3
  54.4 0.7 collective-permute-done.rim_ref
  55.1 4.9 %collective-permute-start.4 = (bf16[128,2048]{1,0:T(8,128)(2,1)S(1)}, bf16[128,2048]{1,0:T(8,128)(2,1)S(1)}, u32[]{:S(2)}, u32[]{:S(2)}) collective-permute-start(bf16[128,2048]{1,0:T(8,128)(2,1)S(1)} %copy-done.5), channel_id=1, source_target_pairs={{0,4},{1,5},{2,6},{3,7},{4,0},{5,1},{6,2},{7,3},{8,12},{9,13},{10,... | collective-permute-start | bytes 1572872 | tf_op jit(solution)/shard_map/ppermute | solution.py:29
  60.0 9.1 %collective-permute-start.6 = (bf16[128,2048]{1,0:T(8,128)(2,1)S(1)}, bf16[128,2048]{1,0:T(8,128)(2,1)S(1)}, u32[]{:S(2)}, u32[]{:S(2)}) collective-permute-start(bf16[128,2048]{1,0:T(8,128)(2,1)S(1)} %copy-done.5), channel_id=1, source_target_pairs={{0,6},{1,7},{2,4},{3,5},{4,2},{5,3},{6,0},{7,1},{8,14},{9,15},{10,... | collective-permute-start | bytes 1572872 | tf_op jit(solution)/shard_map/ppermute | solution.py:29
  69.1 0.4 collective-permute-start.14
  69.4 0.2 add_convert_fusion
  69.7 0.1 collective-permute-start.1
  69.8 1.2 collective-permute-done.2.refs_2_
  71.0 1.9 %collective-permute-done.4.refs_4_ = bf16[128,2048]{1,0:T(8,128)(2,1)S(1)} collective-permute-done((bf16[128,2048]{1,0:T(8,128)(2,1)S(1)}, bf16[128,2048]{1,0:T(8,128)(2,1)S(1)}, u32[]{:S(2)}, u32[]{:S(2)}) %collective-permute-start.4) | collective-permute-done | bytes 524320 | tf_op jit(solution)/shard_map/ppermute | solution.py:29
  72.9 28.2 %collective-permute-start.5 = (bf16[128,2048]{1,0:T(8,128)(2,1)S(1)}, bf16[128,2048]{1,0:T(8,128)(2,1)S(1)}, u32[]{:S(2)}, u32[]{:S(2)}) collective-permute-start(bf16[128,2048]{1,0:T(8,128)(2,1)S(1)} %collective-permute-done.4.refs_4_), channel_id=1, source_target_pairs={{0,1},{1,0},{2,3},{3,2},{4,5},{5,4},{6,7},{7,6},{8,9},{9,8},{10,11... | collective-permute-start | bytes 1572872 | tf_op jit(solution)/shard_map/ppermute | solution.py:29
  101.1 0.0 collective-permute-start.7
  101.1 2.4 %collective-permute-start.20 = (bf16[128,2048]{1,0:T(8,128)(2,1)S(1)}, bf16[128,2048]{1,0:T(8,128)(2,1)S(1)}, u32[]{:S(2)}, u32[]{:S(2)}) collective-permute-start(bf16[128,2048]{1,0:T(8,128)(2,1)S(1)} %add_convert_fusion), channel_id=1, source_target_pairs={{0,16},{1,9},{2,18},{3,11},{4,20},{5,13},{6,22},{7,15},{8,24},{9,1... | collective-permute-start | bytes 1572872 | tf_op jit(solution)/shard_map/ppermute | solution.py:29
  103.5 1.2 mix.1.mixed_ref
  104.8 0.2 convert_add_fusion
  105.0 5.7 %collective-permute-done.20 = bf16[128,2048]{1,0:T(8,128)(2,1)S(1)} collective-permute-done((bf16[128,2048]{1,0:T(8,128)(2,1)S(1)}, bf16[128,2048]{1,0:T(8,128)(2,1)S(1)}, u32[]{:S(2)}, u32[]{:S(2)}) %collective-permute-start.20) | collective-permute-done | bytes 524320 | tf_op jit(solution)/shard_map/ppermute | solution.py:29
  110.7 0.1 spread.1
  110.8 0.0 copy-start.3
  110.8 11.3 %collective-permute-start.21 = (bf16[32,2048]{1,0:T(8,128)(2,1)S(1)}, bf16[32,2048]{1,0:T(8,128)(2,1)S(1)}, u32[]{:S(2)}, u32[]{:S(2)}) collective-permute-start(bf16[32,2048]{1,0:T(8,128)(2,1)S(1)} %get-tuple-element.29), channel_id=1, source_target_pairs={{0,2},{1,3},{2,0},{3,1},{4,6},{5,7},{6,4},{7,5},{8,10},{9,11},{10,... | collective-permute-start | bytes 393224 | tf_op jit(solution)/shard_map/ppermute | solution.py:29
  122.0 1.3 collective-permute-start.22
  123.3 1.4 %collective-permute-start.23 = (bf16[32,2048]{1,0:T(8,128)(2,1)S(1)}, bf16[32,2048]{1,0:T(8,128)(2,1)S(1)}, u32[]{:S(2)}, u32[]{:S(2)}) collective-permute-start(bf16[32,2048]{1,0:T(8,128)(2,1)S(1)} %get-tuple-element.31), channel_id=1, source_target_pairs={{0,6},{1,7},{2,4},{3,5},{4,2},{5,3},{6,0},{7,1},{8,14},{9,15},{10,... | collective-permute-start | bytes 393224 | tf_op jit(solution)/shard_map/ppermute | solution.py:29
  124.8 4.3 %project.1 = bf16[512,2048]{1,0:T(8,128)(2,1)} custom-call(bf16[512,1024]{1,0:T(8,128)(2,1)S(1)} %mix.1.mixed_ref, f32[1,2048]{1,0:T(1,128)S(1)} %bitcast.16, bf16[128,2048]{1,0:T(8,128)(2,1)S(1)} %copy-done.5, bf16[128,2048]{1,0:T(8,128)(2,1)S(1)} %collective-permute-done.1.refs_1_, bf16[128,2048]{1,0:T(8,128)(2,1)S(1)} %collective-permute-done.2.refs_2_, ...), custom_call_target="tpu_custom_call" | custom-call | flops 2147483648 | bytes 7340032 | tf_op jit(solution)/shard_map/project/pallas_call | solution.py:479
  129.0 4.9 %collective-permute-done.22.refs_1_ = bf16[32,2048]{1,0:T(8,128)(2,1)S(1)} collective-permute-done((bf16[32,2048]{1,0:T(8,128)(2,1)S(1)}, bf16[32,2048]{1,0:T(8,128)(2,1)S(1)}, u32[]{:S(2)}, u32[]{:S(2)}) %collective-permute-start.22) | collective-permute-done | bytes 131104 | tf_op jit(solution)/shard_map/ppermute | solution.py:29
  134.0 0.8 finish.1
  (27 shorter events, 0.1 us)
Async XLA Ops:
  1.7 10.5 %collective-permute-start.9 = (bf16[136,2048]{1,0:T(8,128)(2,1)S(1)}, bf16[136,2048]{1,0:T(8,128)(2,1)S(1)}, u32[]{:S(2)}, u32[]{:S(2)}) collective-permute-start(bf16[136,2048]{1,0:T(8,128)(2,1)S(1)} %pack.1.message_ref), channel_id=1, source_target_pairs={{0,8},{1,17},{2,10},{3,19},{4,12},{5,21},{6,14},{7,23},{8,0},{9,25... | collective-permute-start | bytes 1671176 | tf_op jit(solution)/shard_map/ppermute | solution.py:29
  12.3 9.6 %collective-permute-start.16 = (bf16[136,2048]{1,0:T(8,128)(2,1)S(1)}, bf16[136,2048]{1,0:T(8,128)(2,1)S(1)}, u32[]{:S(2)}, u32[]{:S(2)}) collective-permute-start(bf16[136,2048]{1,0:T(8,128)(2,1)S(1)} %collective-permute-done.9.refs_4_), channel_id=1, source_target_pairs={{0,16},{1,9},{2,18},{3,11},{4,20},{5,13},{6,22},{7,15},{8,24},{9,1... | collective-permute-start | bytes 1671176 | tf_op jit(solution)/shard_map/ppermute | solution.py:29
  14.3 13.5 %collective-permute-start.10 = (bf16[136,2048]{1,0:T(8,128)(2,1)S(1)}, bf16[136,2048]{1,0:T(8,128)(2,1)S(1)}, u32[]{:S(2)}, u32[]{:S(2)}) collective-permute-start(bf16[136,2048]{1,0:T(8,128)(2,1)S(1)} %pack.1.message_ref), channel_id=1, source_target_pairs={{0,16},{1,9},{2,18},{3,11},{4,20},{5,13},{6,22},{7,15},{8,24},{9,1... | collective-permute-start | bytes 1671176 | tf_op jit(solution)/shard_map/ppermute | solution.py:29
  21.8 12.8 %collective-permute-start.17 = (bf16[136,2048]{1,0:T(8,128)(2,1)S(1)}, bf16[136,2048]{1,0:T(8,128)(2,1)S(1)}, u32[]{:S(2)}, u32[]{:S(2)}) collective-permute-start(bf16[136,2048]{1,0:T(8,128)(2,1)S(1)} %collective-permute-done.16.refs_4_), channel_id=1, source_target_pairs={{0,1},{1,0},{2,3},{3,2},{4,5},{5,4},{6,7},{7,6},{8,9},{9,8},{10,11... | collective-permute-start | bytes 1671176 | tf_op jit(solution)/shard_map/ppermute | solution.py:29
  21.8 17.7 %collective-permute-start.12 = (bf16[136,2048]{1,0:T(8,128)(2,1)S(1)}, bf16[136,2048]{1,0:T(8,128)(2,1)S(1)}, u32[]{:S(2)}, u32[]{:S(2)}) collective-permute-start(bf16[136,2048]{1,0:T(8,128)(2,1)S(1)} %collective-permute-done.9.refs_4_), channel_id=1, source_target_pairs={{0,1},{1,0},{2,3},{3,2},{4,5},{5,4},{6,7},{7,6},{8,9},{9,8},{10,11... | collective-permute-start | bytes 1671176 | tf_op jit(solution)/shard_map/ppermute | solution.py:29
  27.8 11.7 %collective-permute-start.11 = (bf16[136,2048]{1,0:T(8,128)(2,1)S(1)}, bf16[136,2048]{1,0:T(8,128)(2,1)S(1)}, u32[]{:S(2)}, u32[]{:S(2)}) collective-permute-start(bf16[136,2048]{1,0:T(8,128)(2,1)S(1)} %collective-permute-done.10.refs_6_), channel_id=1, source_target_pairs={{0,1},{1,0},{2,3},{3,2},{4,5},{5,4},{6,7},{7,6},{8,9},{9,8},{10,11... | collective-permute-start | bytes 1671176 | tf_op jit(solution)/shard_map/ppermute | solution.py:29
  27.8 6.9 %copy-start.2 = (f32[2048]{0:T(1024)S(1)}, f32[2048]{0:T(1024)}, u32[]{:S(2)}) copy-start(f32[2048]{0:T(1024)} %param.21) | copy-start | bytes 24580
  38.9 11.7 %copy-start.5 = (bf16[128,2048]{1,0:T(8,128)(2,1)S(1)}, bf16[128,2048]{1,0:T(8,128)(2,1)}, u32[]{:S(2)}) copy-start(bf16[128,2048]{1,0:T(8,128)(2,1)} %refs_0_.1) | copy-start | bytes 1572868
  38.9 13.2 %copy-start = (bf16[512,1024]{1,0:T(8,128)(2,1)S(1)}, bf16[512,1024]{1,0:T(8,128)(2,1)}, u32[]{:S(2)}) copy-start(bf16[512,1024]{1,0:T(8,128)(2,1)} %rows_ref.2) | copy-start | bytes 3145732
  38.9 9.4 %collective-permute-start.18 = (bf16[128,2048]{1,0:T(8,128)(2,1)S(1)}, bf16[128,2048]{1,0:T(8,128)(2,1)S(1)}, u32[]{:S(2)}, u32[]{:S(2)}) collective-permute-start(bf16[128,2048]{1,0:T(8,128)(2,1)S(1)} %get-tuple-element.27), channel_id=1, source_target_pairs={{0,1},{1,0},{2,3},{3,2},{4,5},{5,4},{6,7},{7,6},{8,9},{9,8},{10,11... | collective-permute-start | bytes 1572872 | tf_op jit(solution)/shard_map/ppermute | solution.py:29
  47.8 55.7 %copy-start.1 = (bf16[4,256,256]{2,1,0:T(8,128)(2,1)S(1)}, bf16[4,256,256]{2,1,0:T(8,128)(2,1)}, u32[]{:S(2)}) copy-start(bf16[4,256,256]{2,1,0:T(8,128)(2,1)} %weight_ref.1) | copy-start | bytes 1572868
  47.8 55.7 %copy-start.4 = (f32[1024]{0:T(1024)S(1)}, f32[1024]{0:T(1024)}, u32[]{:S(2)}) copy-start(f32[1024]{0:T(1024)} %param.15) | copy-start | bytes 12292
  47.8 4.3 %collective-permute-start.13 = (bf16[128,2048]{1,0:T(8,128)(2,1)S(1)}, bf16[128,2048]{1,0:T(8,128)(2,1)S(1)}, u32[]{:S(2)}, u32[]{:S(2)}) collective-permute-start(bf16[128,2048]{1,0:T(8,128)(2,1)S(1)} %get-tuple-element.23), channel_id=1, source_target_pairs={{0,1},{1,0},{2,3},{3,2},{4,5},{5,4},{6,7},{7,6},{8,9},{9,8},{10,11... | collective-permute-start | bytes 1572872 | tf_op jit(solution)/shard_map/ppermute | solution.py:29
  48.0 12.0 %collective-permute-start.15 = (bf16[128,2048]{1,0:T(8,128)(2,1)S(1)}, bf16[128,2048]{1,0:T(8,128)(2,1)S(1)}, u32[]{:S(2)}, u32[]{:S(2)}) collective-permute-start(bf16[128,2048]{1,0:T(8,128)(2,1)S(1)} %get-tuple-element.25), channel_id=1, source_target_pairs={{0,1},{1,0},{2,3},{3,2},{4,5},{5,4},{6,7},{7,6},{8,9},{9,8},{10,11... | collective-permute-start | bytes 1572872 | tf_op jit(solution)/shard_map/ppermute | solution.py:29
  48.5 20.6 %collective-permute-start.19 = (bf16[128,2048]{1,0:T(8,128)(2,1)S(1)}, bf16[128,2048]{1,0:T(8,128)(2,1)S(1)}, u32[]{:S(2)}, u32[]{:S(2)}) collective-permute-start(bf16[128,2048]{1,0:T(8,128)(2,1)S(1)} %add_convert_fusion.1), channel_id=1, source_target_pairs={{0,8},{1,17},{2,10},{3,19},{4,12},{5,21},{6,14},{7,23},{8,0},{9,25... | collective-permute-start | bytes 1572872 | tf_op jit(solution)/shard_map/ppermute | solution.py:29
  50.6 19.1 %collective-permute-start.8 = (bf16[128,2048]{1,0:T(8,128)(2,1)S(1)}, bf16[128,2048]{1,0:T(8,128)(2,1)S(1)}, u32[]{:S(2)}, u32[]{:S(2)}) collective-permute-start(bf16[128,2048]{1,0:T(8,128)(2,1)S(1)} %get-tuple-element.18), channel_id=1, source_target_pairs={{0,1},{1,0},{2,3},{3,2},{4,5},{5,4},{6,7},{7,6},{8,9},{9,8},{10,11... | collective-permute-start | bytes 1572872 | tf_op jit(solution)/shard_map/ppermute | solution.py:29
  50.6 20.4 %collective-permute-start.2 = (bf16[128,2048]{1,0:T(8,128)(2,1)S(1)}, bf16[128,2048]{1,0:T(8,128)(2,1)S(1)}, u32[]{:S(2)}, u32[]{:S(2)}) collective-permute-start(bf16[128,2048]{1,0:T(8,128)(2,1)S(1)} %copy-done.5), channel_id=1, source_target_pairs={{0,2},{1,3},{2,0},{3,1},{4,6},{5,7},{6,4},{7,5},{8,10},{9,11},{10,... | collective-permute-start | bytes 1572872 | tf_op jit(solution)/shard_map/ppermute | solution.py:29
  52.1 3.0 %collective-permute-start = (bf16[16,1024]{1,0:T(8,128)(2,1)S(1)}, bf16[16,1024]{1,0:T(8,128)(2,1)S(1)}, u32[]{:S(2)}, u32[]{:S(2)}) collective-permute-start(bf16[16,1024]{1,0:T(8,128)(2,1)S(1)} %slice.3), channel_id=1, source_target_pairs={{0,1},{1,2},{2,3},{3,4},{4,5},{5,6},{6,7},{7,8},{8,9},{9,10},{10,1... | collective-permute-start | bytes 98312 | tf_op jit(solution)/shard_map/ppermute | solution.py:19
  55.1 17.8 %collective-permute-start.4 = (bf16[128,2048]{1,0:T(8,128)(2,1)S(1)}, bf16[128,2048]{1,0:T(8,128)(2,1)S(1)}, u32[]{:S(2)}, u32[]{:S(2)}) collective-permute-start(bf16[128,2048]{1,0:T(8,128)(2,1)S(1)} %copy-done.5), channel_id=1, source_target_pairs={{0,4},{1,5},{2,6},{3,7},{4,0},{5,1},{6,2},{7,3},{8,12},{9,13},{10,... | collective-permute-start | bytes 1572872 | tf_op jit(solution)/shard_map/ppermute | solution.py:29
  60.0 41.1 %collective-permute-start.6 = (bf16[128,2048]{1,0:T(8,128)(2,1)S(1)}, bf16[128,2048]{1,0:T(8,128)(2,1)S(1)}, u32[]{:S(2)}, u32[]{:S(2)}) collective-permute-start(bf16[128,2048]{1,0:T(8,128)(2,1)S(1)} %copy-done.5), channel_id=1, source_target_pairs={{0,6},{1,7},{2,4},{3,5},{4,2},{5,3},{6,0},{7,1},{8,14},{9,15},{10,... | collective-permute-start | bytes 1572872 | tf_op jit(solution)/shard_map/ppermute | solution.py:29
  69.1 32.0 %collective-permute-start.14 = (bf16[128,2048]{1,0:T(8,128)(2,1)S(1)}, bf16[128,2048]{1,0:T(8,128)(2,1)S(1)}, u32[]{:S(2)}, u32[]{:S(2)}) collective-permute-start(bf16[128,2048]{1,0:T(8,128)(2,1)S(1)} %add_convert_fusion.3), channel_id=1, source_target_pairs={{0,8},{1,17},{2,10},{3,19},{4,12},{5,21},{6,14},{7,23},{8,0},{9,25... | collective-permute-start | bytes 1572872 | tf_op jit(solution)/shard_map/ppermute | solution.py:29
  69.4 55.3 %copy-start.6 = (f32[2048]{0:T(1024)S(1)}, f32[2048]{0:T(1024)}, u32[]{:S(2)}) copy-start(f32[2048]{0:T(1024)} %param.17) | copy-start | bytes 24580
  69.7 52.3 %collective-permute-start.1 = (bf16[128,2048]{1,0:T(8,128)(2,1)S(1)}, bf16[128,2048]{1,0:T(8,128)(2,1)S(1)}, u32[]{:S(2)}, u32[]{:S(2)}) collective-permute-start(bf16[128,2048]{1,0:T(8,128)(2,1)S(1)} %copy-done.5), channel_id=1, source_target_pairs={{0,1},{1,0},{2,3},{3,2},{4,5},{5,4},{6,7},{7,6},{8,9},{9,8},{10,11... | collective-permute-start | bytes 1572872 | tf_op jit(solution)/shard_map/ppermute | solution.py:29
  71.0 52.3 %collective-permute-start.3 = (bf16[128,2048]{1,0:T(8,128)(2,1)S(1)}, bf16[128,2048]{1,0:T(8,128)(2,1)S(1)}, u32[]{:S(2)}, u32[]{:S(2)}) collective-permute-start(bf16[128,2048]{1,0:T(8,128)(2,1)S(1)} %collective-permute-done.2.refs_2_), channel_id=1, source_target_pairs={{0,1},{1,0},{2,3},{3,2},{4,5},{5,4},{6,7},{7,6},{8,9},{9,8},{10,11... | collective-permute-start | bytes 1572872 | tf_op jit(solution)/shard_map/ppermute | solution.py:29
  72.9 51.8 %collective-permute-start.5 = (bf16[128,2048]{1,0:T(8,128)(2,1)S(1)}, bf16[128,2048]{1,0:T(8,128)(2,1)S(1)}, u32[]{:S(2)}, u32[]{:S(2)}) collective-permute-start(bf16[128,2048]{1,0:T(8,128)(2,1)S(1)} %collective-permute-done.4.refs_4_), channel_id=1, source_target_pairs={{0,1},{1,0},{2,3},{3,2},{4,5},{5,4},{6,7},{7,6},{8,9},{9,8},{10,11... | collective-permute-start | bytes 1572872 | tf_op jit(solution)/shard_map/ppermute | solution.py:29
  101.1 23.7 %collective-permute-start.7 = (bf16[128,2048]{1,0:T(8,128)(2,1)S(1)}, bf16[128,2048]{1,0:T(8,128)(2,1)S(1)}, u32[]{:S(2)}, u32[]{:S(2)}) collective-permute-start(bf16[128,2048]{1,0:T(8,128)(2,1)S(1)} %collective-permute-done.6.refs_6_), channel_id=1, source_target_pairs={{0,1},{1,0},{2,3},{3,2},{4,5},{5,4},{6,7},{7,6},{8,9},{9,8},{10,11... | collective-permute-start | bytes 1572872 | tf_op jit(solution)/shard_map/ppermute | solution.py:29
  101.1 9.6 %collective-permute-start.20 = (bf16[128,2048]{1,0:T(8,128)(2,1)S(1)}, bf16[128,2048]{1,0:T(8,128)(2,1)S(1)}, u32[]{:S(2)}, u32[]{:S(2)}) collective-permute-start(bf16[128,2048]{1,0:T(8,128)(2,1)S(1)} %add_convert_fusion), channel_id=1, source_target_pairs={{0,16},{1,9},{2,18},{3,11},{4,20},{5,13},{6,22},{7,15},{8,24},{9,1... | collective-permute-start | bytes 1572872 | tf_op jit(solution)/shard_map/ppermute | solution.py:29
  110.8 23.2 %copy-start.3 = (f32[2048]{0:T(1024)S(1)}, f32[2048]{0:T(1024)}, u32[]{:S(2)}) copy-start(f32[2048]{0:T(1024)} %param.25) | copy-start | bytes 24580
  110.8 18.3 %collective-permute-start.21 = (bf16[32,2048]{1,0:T(8,128)(2,1)S(1)}, bf16[32,2048]{1,0:T(8,128)(2,1)S(1)}, u32[]{:S(2)}, u32[]{:S(2)}) collective-permute-start(bf16[32,2048]{1,0:T(8,128)(2,1)S(1)} %get-tuple-element.29), channel_id=1, source_target_pairs={{0,2},{1,3},{2,0},{3,1},{4,6},{5,7},{6,4},{7,5},{8,10},{9,11},{10,... | collective-permute-start | bytes 393224 | tf_op jit(solution)/shard_map/ppermute | solution.py:29
  122.0 11.9 %collective-permute-start.22 = (bf16[32,2048]{1,0:T(8,128)(2,1)S(1)}, bf16[32,2048]{1,0:T(8,128)(2,1)S(1)}, u32[]{:S(2)}, u32[]{:S(2)}) collective-permute-start(bf16[32,2048]{1,0:T(8,128)(2,1)S(1)} %get-tuple-element.30), channel_id=1, source_target_pairs={{0,4},{1,5},{2,6},{3,7},{4,0},{5,1},{6,2},{7,3},{8,12},{9,13},{10,... | collective-permute-start | bytes 393224 | tf_op jit(solution)/shard_map/ppermute | solution.py:29
  123.3 10.7 %collective-permute-start.23 = (bf16[32,2048]{1,0:T(8,128)(2,1)S(1)}, bf16[32,2048]{1,0:T(8,128)(2,1)S(1)}, u32[]{:S(2)}, u32[]{:S(2)}) collective-permute-start(bf16[32,2048]{1,0:T(8,128)(2,1)S(1)} %get-tuple-element.31), channel_id=1, source_target_pairs={{0,6},{1,7},{2,4},{3,5},{4,2},{5,3},{6,0},{7,1},{8,14},{9,15},{10,... | collective-permute-start | bytes 393224 | tf_op jit(solution)/shard_map/ppermute | solution.py:29

commit v4 on v3

--- a/solution.py
+++ b/solution.py
@@ -11,12 +11,13 @@
 LIMIT = 7.0
 ALPHA = 1.702
 CORES = 2
-
-
-def shifted(block, axis, distance):
-    devices = range(lax.axis_size(axis))
-    route = [(i - distance, i) for i in devices if i - distance in devices]
-    return lax.ppermute(block, axis, route)
+PIECES = 2
+REACH = max(WINDOWS)
+
+
+def to_next(block):
+    eps, tps = lax.axis_size("ep"), lax.axis_size("tp")
+    return moved(block, lambda e, t: ((e + (t + 1) // tps) % eps, (t + 1) % tps))
 
 
 def moved(block, target):
@@ -181,7 +182,9 @@
     return [pltpu.with_memory_space_constraint(array, pltpu.HBM) for array in arrays]
 
 
-def pack_kernel(rows_ref, routes_in, weight_in, message_ref, routes_ref, weight_ref, sems):
+def pack_kernel(
+    rows_ref, routes_in, weight_in, pool_ref, message_ref, tail_ref, routes_ref, weight_ref, sems
+):
     half = rows_ref.shape[0] // CORES
     tokens = routes_ref.shape[1]
     experts = message_ref.shape[1] // tokens
@@ -191,6 +194,7 @@
             (routes_in, routes_ref),
             (weight_in, weight_ref),
             (rows_ref.at[pl.ds(start, half)], message_ref.at[pl.ds(0, half)]),
+            (pool_ref.at[pl.ds(pool_ref.shape[0] - REACH, REACH)], tail_ref),
         ],
         sems,
     )
@@ -206,24 +210,28 @@
         both = jnp.where(line == 0, coarse, jnp.where(line == 1, share - coarse, 0.0))
         message_ref[half:, expert * tokens : (expert + 1) * tokens] = both.astype(jnp.bfloat16)
     copies[2].wait()
-
-
-def pack(rows, routes, route_weight):
+    copies[3].wait()
+
+
+def pack(rows, routes, route_weight, pool_in):
     tokens, width = rows.shape
     choose = routes.shape[1]
     return pl.pallas_call(
         pack_kernel,
-        in_specs=[HBM] * 3,
-        out_specs=VMEM,
-        out_shape=jax.ShapeDtypeStruct((tokens // CORES + 8, width), rows.dtype),
+        in_specs=[HBM] * 4,
+        out_specs=[VMEM] * 2,
+        out_shape=[
+            jax.ShapeDtypeStruct((tokens // CORES + 8, width), rows.dtype),
+            jax.ShapeDtypeStruct((REACH, pool_in.shape[1]), pool_in.dtype),
+        ],
         scratch_shapes=[
             pltpu.VMEM((choose, tokens), jnp.int32),
             pltpu.VMEM((choose, tokens), jnp.float32),
-            pltpu.SemaphoreType.DMA((3,)),
+            pltpu.SemaphoreType.DMA((4,)),
         ],
         compiler_params=pltpu.CompilerParams(vmem_limit_bytes=2 << 20),
         name="pack",
-    )(*from_hbm(rows, routes.T, route_weight.T))
+    )(*from_hbm(rows, routes.T, route_weight.T, pool_in))
 
 
 def own_kernel(
@@ -328,62 +336,85 @@
     return [(outputs[2 * g], outputs[2 * g + 1]) for g in range(groups)]
 
 
-def spread_kernel(early_ref, late_ref, own_ref, *out_refs):
-    chips = early_ref.shape[0]
+def spread_kernel(early_ref, late_ref, own_ref, *out_refs, start):
+    chips, _, width = late_ref.shape
     for step in range(chips):
         at = chip_after(seat()[0], step, chips)
-        part = early_ref[at] + late_ref[at].astype(jnp.float32)
+        part = early_ref[at, :, start : start + width] + late_ref[at].astype(jnp.float32)
         if step:
             out_refs[step - 1][...] = part.astype(jnp.bfloat16)
         else:
             own_ref[...] = part
 
 
-def spread(early, late):
-    chips, block, width = early.shape
-    return pl.pallas_call(
-        spread_kernel,
+def spread(early, late, start):
+    chips, block, width = late.shape
+    return pl.pallas_call(
+        lambda *refs: spread_kernel(*refs, start=start),
         in_specs=[VMEM, VMEM],
         out_specs=[VMEM] * chips,
         out_shape=[jax.ShapeDtypeStruct((block, width), jnp.float32)]
         + [jax.ShapeDtypeStruct((block, width), jnp.bfloat16)] * (chips - 1),
         cost_estimate=pl.CostEstimate(
-            flops=early.size, bytes_accessed=8 * early.size, transcendentals=0
+            flops=late.size, bytes_accessed=8 * late.size, transcendentals=0
         ),
         compiler_params=pltpu.CompilerParams(vmem_limit_bytes=4 << 20),
         name="spread",
     )(early, late)
 
 
-def finish_kernel(gain_ref, own_ref, *refs):
-    total = own_ref[...]
-    for ref in refs[:-1]:
-        total = total + ref[...].astype(jnp.float32)
-    refs[-1][...] = rms_scale(total, gain_ref[...]).astype(jnp.bfloat16)
-
-
-def finish(gain, own, parts):
+def finish_kernel(gain_ref, *refs):
+    inputs, out_ref = refs[:-1], refs[-1]
+    each = len(inputs) // PIECES
+    totals = []
+    for piece in range(PIECES):
+        own, *parts = inputs[piece * each : (piece + 1) * each]
+        total = own[...]
+        for part in parts:
+            total = total + part[...].astype(jnp.float32)
+        totals.append(total)
+    total = jnp.concatenate(totals, axis=1)
+    out_ref[...] = rms_scale(total, gain_ref[...]).astype(jnp.bfloat16)
+
+
+def finish(gain, parts):
+    block, width = parts[0].shape
     return pl.pallas_call(
         finish_kernel,
-        in_specs=[VMEM] * (2 + len(parts)),
+        in_specs=[VMEM] * (1 + len(parts)),
         out_specs=VMEM,
-        out_shape=jax.ShapeDtypeStruct(own.shape, jnp.bfloat16),
+        out_shape=jax.ShapeDtypeStruct((block, width * PIECES), jnp.bfloat16),
         compiler_params=pltpu.CompilerParams(vmem_limit_bytes=4 << 20),
         name="finish",
-    )(gain.reshape(1, -1), own, *parts)
+    )(gain.reshape(1, -1), *parts)
 
 
 def added(left, right):
     return (left.astype(jnp.float32) + right.astype(jnp.float32)).astype(jnp.bfloat16)
 
 
+def pass_kernel(held_ref, passing_ref, out_ref, *, start):
+    held = held_ref[:, start : start + passing_ref.shape[1]]
+    out_ref[...] = added(held, passing_ref[...])
+
+
+def pass_on(held, passing, start):
+    return pl.pallas_call(
+        lambda *refs: pass_kernel(*refs, start=start),
+        in_specs=[VMEM, VMEM],
+        out_specs=VMEM,
+        out_shape=jax.ShapeDtypeStruct(passing.shape, passing.dtype),
+        compiler_params=pltpu.CompilerParams(vmem_limit_bytes=4 << 20),
+        name="pass_on",
+    )(held, passing)
+
+
 def dense_experts(
-    expert_in, routes, route_weight, pre_gain, gate_weight, up_weight, down_weight, post_gain
+    message, expert_in, pre_gain, gate_weight, up_weight, down_weight, post_gain
 ):
     tokens, width = expert_in.shape
     chips = lax.axis_size("tp") // CORES
     block = tokens // lax.axis_size("tp")
-    message = pack(expert_in, routes, route_weight)
     from_a = to_group(message, 0)
     from_b = to_group(message, 1)
     weights = (pre_gain, gate_weight, up_weight, down_weight.reshape(-1, width), block)
@@ -403,18 +434,24 @@
     near_sum = to_group(joined_a, 0)
     ((kept_c, sent_c),) = expert_partial([(from_c, other_c)], *weights)
     back_c = to_core(sent_c)
-    joined_c = added(kept_c, back_c)
-    passing = to_group(joined_c, 0)
-    passed = added(joined_b, passing)
-    far_sum = to_group(passed, 1)
+    span = width // PIECES
+    columns = [slice(piece * span, (piece + 1) * span) for piece in range(PIECES)]
+    joined_c = [added(kept_c[:, part], back_c[:, part]) for part in columns]
+    passed, late = [], []
+    for piece in range(PIECES):
+        passing = to_group(joined_c[piece], 0)
+        passed.append(pass_on(joined_b, passing, piece * span))
+    for piece in range(PIECES):
+        late.append(to_group(passed[piece], 1))
     early = lax.optimization_barrier(early + near_sum.astype(jnp.float32))
-    own, *pieces = spread(
-        early.reshape(chips, block, width), far_sum.reshape(chips, block, width)
-    )
+    early = early.reshape(chips, block, width)
     parts = []
-    for step in range(1, chips):
-        parts.append(to_chip(pieces[step - 1], step))
-    return finish(post_gain, own, parts)
+    for piece in range(PIECES):
+        own, *pieces = spread(early, late[piece].reshape(chips, block, span), piece * span)
+        parts.append(own)
+        for step in range(1, chips):
+            parts.append(to_chip(pieces[step - 1], step))
+    return finish(post_gain, parts)
 
 
 def mix_kernel(rim_ref, rows_ref, weight_ref, gain_ref, out_ref):
@@ -425,8 +462,8 @@
     position = device * rows + lax.broadcasted_iota(jnp.int32, (rows, 1), 0)
     for which, window in enumerate(WINDOWS):
         cols = slice(which * group, (which + 1) * group)
-        values = jnp.concatenate([rim_ref[:, cols], rows_ref[:, cols]], axis=0)
-        values = values.astype(jnp.float32)
+        rim = jnp.where(device == 0, 0.0, rim_ref[:, cols].astype(jnp.float32))
+        values = jnp.concatenate([rim, rows_ref[:, cols].astype(jnp.float32)], axis=0)
         running, reach = values, 1
         while reach < window:
             running = running + pltpu.roll(running, reach, 0)
@@ -455,46 +492,85 @@
     )(rim, rows, weight, gain.reshape(1, -1))
 
 
-def project_kernel(mixed_ref, gain_ref, *refs):
+def join_shards(joined, weights, far):
+    chip, core = seat()
+    chips = 2 * len(weights) // CORES
+    depth = weights[0].shape[0]
+    base = lax.div(chip, chips // 2)
+    base = (1 - base if far else base) * (chips // 2)
+    for k, weight in enumerate(weights):
+        step = k // CORES + (chips // 2 if far else 0)
+        shard = (chip_before(chip, step, chips) - base) * CORES
+        shard = shard + (core if k % CORES == 0 else 1 - core)
+        joined[pl.ds(pl.multiple_of(shard * depth, depth), depth), :] = weight[...]
+    return base * CORES * depth
+
+
+def near_kernel(mixed_ref, *refs):
     weights, out_ref, joined = refs[:-2], refs[-2], refs[-1]
+    span = joined.shape[0]
+    start = pl.multiple_of(join_shards(joined, weights, False), span)
+    out_ref[...] = jnp.dot(
+        mixed_ref[:, pl.ds(start, span)], joined[...], preferred_element_type=jnp.float32
+    )
+
+
+def near_project(mixed, weights):
+    rows, depth = mixed.shape
+    width = weights[0].shape[1]
+    return pl.pallas_call(
+        near_kernel,
+        in_specs=[VMEM] * (1 + len(weights)),
+        out_specs=VMEM,
+        out_shape=pltpu.VMEM((rows, width), jnp.float32),
+        scratch_shapes=[pltpu.VMEM((depth // 2, width), jnp.bfloat16)],
+        compiler_params=pltpu.CompilerParams(vmem_limit_bytes=8 << 20),
+        cost_estimate=pl.CostEstimate(
+            flops=rows * depth * width, bytes_accessed=4 * rows * width, transcendentals=0
+        ),
+        name="near",
+    )(mixed, *weights)
+
+
+def project_kernel(mixed_ref, near_ref, gain_ref, *refs):
+    weights, out_ref, joined = refs[:-2], refs[-2], refs[-1]
+    span, tile = joined.shape[0], out_ref.shape[0]
+    row = pl.multiple_of(pl.program_id(0) * tile, tile)
 
     @pl.when(pl.program_id(0) == 0)
     def _():
-        depth = weights[0].shape[0]
-        chip, core = seat()
-        chips = len(weights) // CORES
-        for k, weight in enumerate(weights):
-            source = chip_before(chip, k // CORES, chips) * CORES
-            shard = source + (core if k % CORES == 0 else 1 - core)
-            joined[pl.ds(pl.multiple_of(shard * depth, depth), depth), :] = weight[...]
-
-    total = jnp.dot(mixed_ref[...], joined[...], preferred_element_type=jnp.float32)
+        join_shards(joined, weights, True)
+
+    chip, _ = seat()
+    chips = 2 * len(weights) // CORES
+    start = pl.multiple_of((1 - lax.div(chip, chips // 2)) * span, span)
+    total = near_ref[pl.ds(row, tile), :] + jnp.dot(
+        mixed_ref[pl.ds(row, tile), pl.ds(start, span)],
+        joined[...],
+        preferred_element_type=jnp.float32,
+    )
     out_ref[...] = rms_scale(total, gain_ref[...]).astype(jnp.bfloat16)
 
 
-def project(mixed, gain, weights):
+def project(mixed, near, gain, weights):
     rows, depth = mixed.shape
     width = weights[0].shape[1]
     tile = min(256, rows)
     return pl.pallas_call(
         project_kernel,
         grid=(rows // tile,),
-        in_specs=[
-            pl.BlockSpec((tile, depth), lambda i: (i, 0)),
-            pl.BlockSpec((1, width), lambda i: (0, 0)),
-        ]
-        + [VMEM] * len(weights),
+        in_specs=[VMEM] * (3 + len(weights)),
         out_specs=pl.BlockSpec((tile, width), lambda i: (i, 0)),
         out_shape=jax.ShapeDtypeStruct((rows, width), jnp.bfloat16),
-        scratch_shapes=[pltpu.VMEM((depth, width), jnp.bfloat16)],
-        compiler_params=pltpu.CompilerParams(vmem_limit_bytes=18 << 20),
+        scratch_shapes=[pltpu.VMEM((depth // 2, width), jnp.bfloat16)],
+        compiler_params=pltpu.CompilerParams(vmem_limit_bytes=8 << 20),
         cost_estimate=pl.CostEstimate(
-            flops=2 * rows * depth * width,
-            bytes_accessed=2 * (rows * width + depth * (rows + width)),
+            flops=rows * depth * width,
+            bytes_accessed=6 * rows * width,
             transcendentals=0,
         ),
         name="project",
-    )(mixed, gain.reshape(1, width), *weights)
+    )(mixed, near, gain.reshape(1, width), *weights)
 
 
 def step(
@@ -521,17 +597,26 @@
     experts_in_all = gate_weight.shape[0] * ep_count
     dense = capacity >= block_tokens and ep_count == 4
     dense = dense and experts_in_all * tokens_here <= expert_in.shape[1]
-    experts = dense_experts if dense else routed_experts
-    rim = shifted(pool_in[rows - 16 :], ("ep", "tp"), 1)
-    expert_out = experts(
-        expert_in, routes, route_weight, pre_gain, gate_weight, up_weight, down_weight, post_gain
-    )
+    tail = pool_in[rows - REACH :]
+    if dense:
+        message, tail = pack(expert_in, routes, route_weight, pool_in)
+    rim = to_next(tail)
+    if dense:
+        expert_out = dense_experts(
+            message, expert_in, pre_gain, gate_weight, up_weight, down_weight, post_gain
+        )
+    else:
+        expert_out = routed_experts(
+            expert_in, routes, route_weight, pre_gain, gate_weight, up_weight, down_weight,
+            post_gain,
+        )
     shards = []
     for step in range(chips):
         shard = to_chip(out_weight, step) if step else out_weight
         shards += [shard, to_core(shard)]
     mixed = mix(rim, pool_in, pool_weight, pool_gain)
-    mix_out = project(mixed, mix_gain, shards)
+    half = len(shards) // 2
+    mix_out = project(mixed, near_project(mixed, shards[:half]), mix_gain, shards[half:])
     return (mix_out, expert_out)
 
 

time: 135 us -> 120 us (0.89)
  starting transfers between devices: 71.5 us -> 33.7 us
  waiting for transfers between devices: 35 us -> 57.6 us
    ppermute x23 -> x29, starting transfers between devices: 69.4 us -> 33.7 us  [moved(): return lax.ppermute(block, ('ep', 'tp'), route)]
    ppermute x23 -> x29, waiting for transfers between devices: 34.2 us -> 57.6 us  [moved(): return lax.ppermute(block, ('ep', 'tp'), route)]
    ppermute x1 -> x0, starting transfers between devices: 2.13 us -> none  [shifted(): return lax.ppermute(block, axis, route)]
    pallas_call x4 -> x8, Pallas kernels: 6.28 us -> 6.75 us  [the longest x1 3.15 us: project(): pl.pallas_call(project_kernel, grid=(rows // tile,), in_specs=[VMEM] * (3...]
  transfers between devices with their start and end apart: 24 -> 29, of which waited for: 8 -> 8; matrix products, arithmetic and copies ran while one was open for 1% -> 1% of each run, Pallas kernels for 18% -> 21%
where the time goes in v4:
time: 120 us
  waiting for transfers between devices  57.6 us (48%)
  starting transfers between devices  33.7 us (28%)
  Pallas kernels  27.2 us (23%)
    ppermute x29, waiting for transfers between devices, moved(): return lax.ppermute(block, ('ep', 'tp'), route)  57.6 us
    ppermute x29, starting transfers between devices, moved(): return lax.ppermute(block, ('ep', 'tp'), route)  33.7 us
    pallas_call x2, Pallas kernels, expert_partial(): pl.pallas_call(lambda *refs: expert_kernel(*refs, groups=groups), in_spec...  12.4 us
    pallas_call x1, Pallas kernels, own_partial(): pl.pallas_call(own_kernel, in_specs=[HBM] * 5 + [VMEM], out_specs=[VMEM]...  6.83 us
    pallas_call x1, Pallas kernels, project(): pl.pallas_call(project_kernel, grid=(rows // tile,), in_specs=[VMEM] * (3...  3.15 us
  transfers between devices with their start and end apart: 29, of which 8 were waited for; matrix products, arithmetic and copies ran while one was open for 1% of the time, Pallas kernels for 21%

profile of v4, /device:TPU:0, one launch (start us, length us, event | category | flops | bytes accessed | tf_op | source)
XLA Modules:
  0.0 120.1 jit_solution(13040148544885222786)
XLA Ops:
  0.6 1.1 pack.1
  1.8 3.0 %collective-permute-start.9 = (bf16[136,2048]{1,0:T(8,128)(2,1)S(1)}, bf16[136,2048]{1,0:T(8,128)(2,1)S(1)}, u32[]{:S(2)}, u32[]{:S(2)}) collective-permute-start(bf16[136,2048]{1,0:T(8,128)(2,1)S(1)} %get-tuple-element.24.message_ref), channel_id=1, source_target_pairs={{0,8},{1,17},{2,10},{3,19},{4,12},{5,21},{6,14},{7,23},{8,0},{9,25... | collective-permute-start | bytes 1671176 | tf_op jit(solution)/shard_map/ppermute | solution.py:30
  4.8 7.5 %collective-permute-done.9.refs_4_ = bf16[136,2048]{1,0:T(8,128)(2,1)S(1)} collective-permute-done((bf16[136,2048]{1,0:T(8,128)(2,1)S(1)}, bf16[136,2048]{1,0:T(8,128)(2,1)S(1)}, u32[]{:S(2)}, u32[]{:S(2)}) %collective-permute-start.9) | collective-permute-done | bytes 557088 | tf_op jit(solution)/shard_map/ppermute | solution.py:30
  12.3 2.0 %collective-permute-start.16 = (bf16[136,2048]{1,0:T(8,128)(2,1)S(1)}, bf16[136,2048]{1,0:T(8,128)(2,1)S(1)}, u32[]{:S(2)}, u32[]{:S(2)}) collective-permute-start(bf16[136,2048]{1,0:T(8,128)(2,1)S(1)} %collective-permute-done.9.refs_4_), channel_id=1, source_target_pairs={{0,16},{1,9},{2,18},{3,11},{4,20},{5,13},{6,22},{7,15},{8,24},{9,1... | collective-permute-start | bytes 1671176 | tf_op jit(solution)/shard_map/ppermute | solution.py:30
  14.3 0.0 collective-permute-start.10
  14.4 7.5 %collective-permute-done.16.refs_4_ = bf16[136,2048]{1,0:T(8,128)(2,1)S(1)} collective-permute-done((bf16[136,2048]{1,0:T(8,128)(2,1)S(1)}, bf16[136,2048]{1,0:T(8,128)(2,1)S(1)}, u32[]{:S(2)}, u32[]{:S(2)}) %collective-permute-start.16) | collective-permute-done | bytes 557088 | tf_op jit(solution)/shard_map/ppermute | solution.py:30
  21.9 0.5 collective-permute-start.12
  22.4 5.5 %collective-permute-done.10.refs_6_ = bf16[136,2048]{1,0:T(8,128)(2,1)S(1)} collective-permute-done((bf16[136,2048]{1,0:T(8,128)(2,1)S(1)}, bf16[136,2048]{1,0:T(8,128)(2,1)S(1)}, u32[]{:S(2)}, u32[]{:S(2)}) %collective-permute-start.10) | collective-permute-done | bytes 557088 | tf_op jit(solution)/shard_map/ppermute | solution.py:30
  27.8 6.8 %own.1 = (bf16[128,2048]{1,0:T(8,128)(2,1)S(1)}, bf16[128,2048]{1,0:T(8,128)(2,1)S(1)}, bf16[2,2048,512]{2,1,0:T(8,128)(2,1)S(1)}, bf16[2,2048,512]{2,1,0:T(8,128)(2,1)S(1)}, bf16[1024,2048]{1,0:T(8,128)(2,1)S(1)}) custom-call(f32[1,2048]{1,0:T(1,128)} %bitcast.14, bf16[256,2048]{1,0:T(8,128)(2,1)} %rows_in.1, bf16[2,2048,512]{2,1,0:T(8,128)(2,1)} %gate_in.1, ...), custom_call_target="tpu_custom_call" | custom-call | flops 3221225472 | bytes 14680064 | tf_op jit(solution)/shard_map/own/pallas_call | solution.py:271
  34.7 4.2 %experts.3 = (bf16[128,2048]{1,0:T(8,128)(2,1)S(1)}, bf16[128,2048]{1,0:T(8,128)(2,1)S(1)}) custom-call(f32[1,2048]{1,0:T(1,128)S(1)} %bitcast.15, bf16[2,2048,512]{2,1,0:T(8,128)(2,1)S(1)} %get-tuple-element.27.refs_1_, bf16[2,2048,512]{2,1,0:T(8,128)(2,1)S(1)} %get-tuple-element.28.refs_2_, bf16[1024,2048]{1,0:T(8,128)(2,1)S(1)} %get-tuple-element.29.refs_3_, ...), custom_call_target="tpu_custom_call" | custom-call | flops 3221225472 | bytes 2097152 | tf_op jit(solution)/shard_map/experts/pallas_call | solution.py:318
  38.9 0.6 collective-permute-start.18
  39.5 8.2 %experts.2 = (bf16[128,2048]{1,0:T(8,128)(2,1)S(1)}, bf16[128,2048]{1,0:T(8,128)(2,1)S(1)}, bf16[128,2048]{1,0:T(8,128)(2,1)S(1)}, bf16[128,2048]{1,0:T(8,128)(2,1)S(1)}) custom-call(f32[1,2048]{1,0:T(1,128)S(1)} %bitcast.16, bf16[2,2048,512]{2,1,0:T(8,128)(2,1)S(1)} %get-tuple-element.27.refs_1_, bf16[2,2048,512]{2,1,0:T(8,128)(2,1)S(1)} %get-tuple-element.28.refs_2_, ...), custom_call_target="tpu_custom_call" | custom-call | flops 6442450944 | bytes 4194304 | tf_op jit(solution)/shard_map/experts/pallas_call | solution.py:318
  47.8 0.2 collective-permute-start.13
  48.0 0.4 collective-permute-start.8
  48.4 0.1 collective-permute-start
  48.5 2.1 %collective-permute-start.2 = (bf16[128,2048]{1,0:T(8,128)(2,1)S(1)}, bf16[128,2048]{1,0:T(8,128)(2,1)S(1)}, u32[]{:S(2)}, u32[]{:S(2)}) collective-permute-start(bf16[128,2048]{1,0:T(8,128)(2,1)S(1)} %copy-done.1), channel_id=1, source_target_pairs={{0,2},{1,3},{2,0},{3,1},{4,6},{5,7},{6,4},{7,5},{8,10},{9,11},{10,... | collective-permute-start | bytes 1572872 | tf_op jit(solution)/shard_map/ppermute | solution.py:30
  50.6 1.3 %collective-permute-start.15 = (bf16[128,2048]{1,0:T(8,128)(2,1)S(1)}, bf16[128,2048]{1,0:T(8,128)(2,1)S(1)}, u32[]{:S(2)}, u32[]{:S(2)}) collective-permute-start(bf16[128,2048]{1,0:T(8,128)(2,1)S(1)} %get-tuple-element.33), channel_id=1, source_target_pairs={{0,1},{1,0},{2,3},{3,2},{4,5},{5,4},{6,7},{7,6},{8,9},{9,8},{10,11... | collective-permute-start | bytes 1572872 | tf_op jit(solution)/shard_map/ppermute | solution.py:30
  51.8 0.2 add_convert_fusion.2
  52.0 1.6 %collective-permute-start.24 = (bf16[128,1024]{1,0:T(8,128)(2,1)S(1)}, bf16[128,1024]{1,0:T(8,128)(2,1)S(1)}, u32[]{:S(2)}, u32[]{:S(2)}) collective-permute-start(bf16[128,1024]{1,0:T(8,128)(2,1)S(1)} %get-tuple-element.44), channel_id=1, source_target_pairs={{0,8},{1,17},{2,10},{3,19},{4,12},{5,21},{6,14},{7,23},{8,0},{9,25... | collective-permute-start | bytes 786440 | tf_op jit(solution)/shard_map/ppermute | solution.py:30
  53.6 0.1 add_convert_fusion.1
  53.7 2.1 %collective-permute-done.rim_ref = bf16[16,1024]{1,0:T(8,128)(2,1)S(1)} collective-permute-done((bf16[16,1024]{1,0:T(8,128)(2,1)S(1)}, bf16[16,1024]{1,0:T(8,128)(2,1)S(1)}, u32[]{:S(2)}, u32[]{:S(2)}) %collective-permute-start) | collective-permute-done | bytes 32800 | tf_op jit(solution)/shard_map/ppermute | solution.py:30
  55.8 0.2 collective-permute-start.4
  56.0 0.6 collective-permute-start.6
  56.6 1.0 collective-permute-start.14
  57.6 1.1 collective-permute-done.24.refs_1_
  58.8 1.2 %collective-permute-start.19 = (bf16[128,1024]{1,0:T(8,128)(2,1)S(1)}, bf16[128,1024]{1,0:T(8,128)(2,1)S(1)}, u32[]{:S(2)}, u32[]{:S(2)}) collective-permute-start(bf16[128,1024]{1,0:T(8,128)(2,1)S(1)} %get-tuple-element.45), channel_id=1, source_target_pairs={{0,8},{1,17},{2,10},{3,19},{4,12},{5,21},{6,14},{7,23},{8,0},{9,25... | collective-permute-start | bytes 786440 | tf_op jit(solution)/shard_map/ppermute | solution.py:30
  60.0 0.1 add_convert_fusion.refs_0_
  60.1 0.1 pass_on.3
  60.2 11.1 %collective-permute-done.2.refs_2_ = bf16[128,2048]{1,0:T(8,128)(2,1)S(1)} collective-permute-done((bf16[128,2048]{1,0:T(8,128)(2,1)S(1)}, bf16[128,2048]{1,0:T(8,128)(2,1)S(1)}, u32[]{:S(2)}, u32[]{:S(2)}) %collective-permute-start.2) | collective-permute-done | bytes 524320 | tf_op jit(solution)/shard_map/ppermute | solution.py:30
  71.3 2.2 %collective-permute-start.25 = (bf16[128,1024]{1,0:T(8,128)(2,1)S(1)}, bf16[128,1024]{1,0:T(8,128)(2,1)S(1)}, u32[]{:S(2)}, u32[]{:S(2)}) collective-permute-start(bf16[128,1024]{1,0:T(8,128)(2,1)S(1)} %pass_on.3), channel_id=1, source_target_pairs={{0,16},{1,9},{2,18},{3,11},{4,20},{5,13},{6,22},{7,15},{8,24},{9,1... | collective-permute-start | bytes 786440 | tf_op jit(solution)/shard_map/ppermute | solution.py:30
  73.5 20.4 %collective-permute-done.4.refs_0_ = bf16[128,2048]{1,0:T(8,128)(2,1)S(1)} collective-permute-done((bf16[128,2048]{1,0:T(8,128)(2,1)S(1)}, bf16[128,2048]{1,0:T(8,128)(2,1)S(1)}, u32[]{:S(2)}, u32[]{:S(2)}) %collective-permute-start.4) | collective-permute-done | bytes 524320 | tf_op jit(solution)/shard_map/ppermute | solution.py:30
  94.0 0.5 collective-permute-start.3
  94.5 1.2 mix.1.mixed_ref
  95.7 0.1 pass_on.2
  95.7 0.1 collective-permute-start.5
  95.8 0.5 collective-permute-start.7
  96.3 1.9 %collective-permute-start.20 = (bf16[128,1024]{1,0:T(8,128)(2,1)S(1)}, bf16[128,1024]{1,0:T(8,128)(2,1)S(1)}, u32[]{:S(2)}, u32[]{:S(2)}) collective-permute-start(bf16[128,1024]{1,0:T(8,128)(2,1)S(1)} %pass_on.2), channel_id=1, source_target_pairs={{0,16},{1,9},{2,18},{3,11},{4,20},{5,13},{6,22},{7,15},{8,24},{9,1... | collective-permute-start | bytes 786440 | tf_op jit(solution)/shard_map/ppermute | solution.py:30
  98.2 0.2 convert_add_fusion
  98.4 0.1 spread.3
  98.5 5.5 %collective-permute-start.26 = (bf16[32,1024]{1,0:T(8,128)(2,1)S(1)}, bf16[32,1024]{1,0:T(8,128)(2,1)S(1)}, u32[]{:S(2)}, u32[]{:S(2)}) collective-permute-start(bf16[32,1024]{1,0:T(8,128)(2,1)S(1)} %get-tuple-element.41), channel_id=1, source_target_pairs={{0,2},{1,3},{2,0},{3,1},{4,6},{5,7},{6,4},{7,5},{8,10},{9,11},{10,... | collective-permute-start | bytes 196616 | tf_op jit(solution)/shard_map/ppermute | solution.py:30
  104.0 1.4 %near.1.near_ref = f32[512,2048]{1,0:T(8,128)S(1)} custom-call(bf16[512,1024]{1,0:T(8,128)(2,1)S(1)} %mix.1.mixed_ref, bf16[128,2048]{1,0:T(8,128)(2,1)S(1)} %copy-done.1, bf16[128,2048]{1,0:T(8,128)(2,1)S(1)} %collective-permute-done.1.refs_1_, bf16[128,2048]{1,0:T(8,128)(2,1)S(1)} %collective-permute-done.2.refs_2_, ...), custom_call_target="tpu_custom_call" | custom-call | flops 1073741824 | bytes 4194304 | tf_op jit(solution)/shard_map/near/pallas_call | solution.py:521
  105.4 1.1 collective-permute-start.27
  106.5 1.5 %collective-permute-start.28 = (bf16[32,1024]{1,0:T(8,128)(2,1)S(1)}, bf16[32,1024]{1,0:T(8,128)(2,1)S(1)}, u32[]{:S(2)}, u32[]{:S(2)}) collective-permute-start(bf16[32,1024]{1,0:T(8,128)(2,1)S(1)} %get-tuple-element.43), channel_id=1, source_target_pairs={{0,6},{1,7},{2,4},{3,5},{4,2},{5,3},{6,0},{7,1},{8,14},{9,15},{10,... | collective-permute-start | bytes 196616 | tf_op jit(solution)/shard_map/ppermute | solution.py:30
  108.1 3.1 %collective-permute-start.21 = (bf16[32,1024]{1,0:T(8,128)(2,1)S(1)}, bf16[32,1024]{1,0:T(8,128)(2,1)S(1)}, u32[]{:S(2)}, u32[]{:S(2)}) collective-permute-start(bf16[32,1024]{1,0:T(8,128)(2,1)S(1)} %get-tuple-element.37), channel_id=1, source_target_pairs={{0,2},{1,3},{2,0},{3,1},{4,6},{5,7},{6,4},{7,5},{8,10},{9,11},{10,... | collective-permute-start | bytes 196616 | tf_op jit(solution)/shard_map/ppermute | solution.py:30
  111.2 2.4 %collective-permute-start.23 = (bf16[32,1024]{1,0:T(8,128)(2,1)S(1)}, bf16[32,1024]{1,0:T(8,128)(2,1)S(1)}, u32[]{:S(2)}, u32[]{:S(2)}) collective-permute-start(bf16[32,1024]{1,0:T(8,128)(2,1)S(1)} %get-tuple-element.39), channel_id=1, source_target_pairs={{0,6},{1,7},{2,4},{3,5},{4,2},{5,3},{6,0},{7,1},{8,14},{9,15},{10,... | collective-permute-start | bytes 196616 | tf_op jit(solution)/shard_map/ppermute | solution.py:30
  113.6 3.2 %project.1 = bf16[512,2048]{1,0:T(8,128)(2,1)} custom-call(bf16[512,1024]{1,0:T(8,128)(2,1)S(1)} %mix.1.mixed_ref, f32[512,2048]{1,0:T(8,128)S(1)} %near.1.near_ref, f32[1,2048]{1,0:T(1,128)S(1)} %bitcast.18, bf16[128,2048]{1,0:T(8,128)(2,1)S(1)} %collective-permute-done.4.refs_0_, bf16[128,2048]{1,0:T(8,128)(2,1)S(1)} %collective-permute-done.5.refs_1_, ...), custom_call_target="tpu_custom_call" | custom-call | flops 1073741824 | bytes 6291456 | tf_op jit(solution)/shard_map/project/pallas_call | solution.py:559
  116.8 2.4 %collective-permute-done.22.refs_2_ = bf16[32,1024]{1,0:T(8,128)(2,1)S(1)} collective-permute-done((bf16[32,1024]{1,0:T(8,128)(2,1)S(1)}, bf16[32,1024]{1,0:T(8,128)(2,1)S(1)}, u32[]{:S(2)}, u32[]{:S(2)}) %collective-permute-start.22) | collective-permute-done | bytes 65568 | tf_op jit(solution)/shard_map/ppermute | solution.py:30
  119.2 0.8 finish.1
  (40 shorter events, 0.2 us)
Async XLA Ops:
  1.8 10.5 %collective-permute-start.9 = (bf16[136,2048]{1,0:T(8,128)(2,1)S(1)}, bf16[136,2048]{1,0:T(8,128)(2,1)S(1)}, u32[]{:S(2)}, u32[]{:S(2)}) collective-permute-start(bf16[136,2048]{1,0:T(8,128)(2,1)S(1)} %get-tuple-element.24.message_ref), channel_id=1, source_target_pairs={{0,8},{1,17},{2,10},{3,19},{4,12},{5,21},{6,14},{7,23},{8,0},{9,25... | collective-permute-start | bytes 1671176 | tf_op jit(solution)/shard_map/ppermute | solution.py:30
  12.3 9.6 %collective-permute-start.16 = (bf16[136,2048]{1,0:T(8,128)(2,1)S(1)}, bf16[136,2048]{1,0:T(8,128)(2,1)S(1)}, u32[]{:S(2)}, u32[]{:S(2)}) collective-permute-start(bf16[136,2048]{1,0:T(8,128)(2,1)S(1)} %collective-permute-done.9.refs_4_), channel_id=1, source_target_pairs={{0,16},{1,9},{2,18},{3,11},{4,20},{5,13},{6,22},{7,15},{8,24},{9,1... | collective-permute-start | bytes 1671176 | tf_op jit(solution)/shard_map/ppermute | solution.py:30
  14.3 13.5 %collective-permute-start.10 = (bf16[136,2048]{1,0:T(8,128)(2,1)S(1)}, bf16[136,2048]{1,0:T(8,128)(2,1)S(1)}, u32[]{:S(2)}, u32[]{:S(2)}) collective-permute-start(bf16[136,2048]{1,0:T(8,128)(2,1)S(1)} %get-tuple-element.24.message_ref), channel_id=1, source_target_pairs={{0,16},{1,9},{2,18},{3,11},{4,20},{5,13},{6,22},{7,15},{8,24},{9,1... | collective-permute-start | bytes 1671176 | tf_op jit(solution)/shard_map/ppermute | solution.py:30
  21.9 12.8 %collective-permute-start.17 = (bf16[136,2048]{1,0:T(8,128)(2,1)S(1)}, bf16[136,2048]{1,0:T(8,128)(2,1)S(1)}, u32[]{:S(2)}, u32[]{:S(2)}) collective-permute-start(bf16[136,2048]{1,0:T(8,128)(2,1)S(1)} %collective-permute-done.16.refs_4_), channel_id=1, source_target_pairs={{0,1},{1,0},{2,3},{3,2},{4,5},{5,4},{6,7},{7,6},{8,9},{9,8},{10,11... | collective-permute-start | bytes 1671176 | tf_op jit(solution)/shard_map/ppermute | solution.py:30
  21.9 17.7 %collective-permute-start.12 = (bf16[136,2048]{1,0:T(8,128)(2,1)S(1)}, bf16[136,2048]{1,0:T(8,128)(2,1)S(1)}, u32[]{:S(2)}, u32[]{:S(2)}) collective-permute-start(bf16[136,2048]{1,0:T(8,128)(2,1)S(1)} %collective-permute-done.9.refs_4_), channel_id=1, source_target_pairs={{0,1},{1,0},{2,3},{3,2},{4,5},{5,4},{6,7},{7,6},{8,9},{9,8},{10,11... | collective-permute-start | bytes 1671176 | tf_op jit(solution)/shard_map/ppermute | solution.py:30
  27.8 11.7 %collective-permute-start.11 = (bf16[136,2048]{1,0:T(8,128)(2,1)S(1)}, bf16[136,2048]{1,0:T(8,128)(2,1)S(1)}, u32[]{:S(2)}, u32[]{:S(2)}) collective-permute-start(bf16[136,2048]{1,0:T(8,128)(2,1)S(1)} %collective-permute-done.10.refs_6_), channel_id=1, source_target_pairs={{0,1},{1,0},{2,3},{3,2},{4,5},{5,4},{6,7},{7,6},{8,9},{9,8},{10,11... | collective-permute-start | bytes 1671176 | tf_op jit(solution)/shard_map/ppermute | solution.py:30
  27.8 6.9 %copy-start.3 = (f32[2048]{0:T(1024)S(1)}, f32[2048]{0:T(1024)}, u32[]{:S(2)}) copy-start(f32[2048]{0:T(1024)} %param.21) | copy-start | bytes 24580
  38.9 9.6 %copy-start.1 = (bf16[128,2048]{1,0:T(8,128)(2,1)S(1)}, bf16[128,2048]{1,0:T(8,128)(2,1)}, u32[]{:S(2)}) copy-start(bf16[128,2048]{1,0:T(8,128)(2,1)} %refs_0_.1) | copy-start | bytes 1572868
  38.9 11.7 %collective-permute-start.18 = (bf16[128,2048]{1,0:T(8,128)(2,1)S(1)}, bf16[128,2048]{1,0:T(8,128)(2,1)S(1)}, u32[]{:S(2)}, u32[]{:S(2)}) collective-permute-start(bf16[128,2048]{1,0:T(8,128)(2,1)S(1)} %get-tuple-element.35), channel_id=1, source_target_pairs={{0,1},{1,0},{2,3},{3,2},{4,5},{5,4},{6,7},{7,6},{8,9},{9,8},{10,11... | collective-permute-start | bytes 1572872 | tf_op jit(solution)/shard_map/ppermute | solution.py:30
  47.7 46.7 %copy-start = (bf16[512,1024]{1,0:T(8,128)(2,1)S(1)}, bf16[512,1024]{1,0:T(8,128)(2,1)}, u32[]{:S(2)}) copy-start(bf16[512,1024]{1,0:T(8,128)(2,1)} %rows_ref.3) | copy-start | bytes 3145732
  47.8 46.7 %copy-start.2 = (bf16[4,256,256]{2,1,0:T(8,128)(2,1)S(1)}, bf16[4,256,256]{2,1,0:T(8,128)(2,1)}, u32[]{:S(2)}) copy-start(bf16[4,256,256]{2,1,0:T(8,128)(2,1)} %weight_ref.1) | copy-start | bytes 1572868
  47.8 46.7 %copy-start.6 = (f32[1024]{0:T(1024)S(1)}, f32[1024]{0:T(1024)}, u32[]{:S(2)}) copy-start(f32[1024]{0:T(1024)} %param.15) | copy-start | bytes 12292
  47.8 4.2 %collective-permute-start.13 = (bf16[128,2048]{1,0:T(8,128)(2,1)S(1)}, bf16[128,2048]{1,0:T(8,128)(2,1)S(1)}, u32[]{:S(2)}, u32[]{:S(2)}) collective-permute-start(bf16[128,2048]{1,0:T(8,128)(2,1)S(1)} %get-tuple-element.31), channel_id=1, source_target_pairs={{0,1},{1,0},{2,3},{3,2},{4,5},{5,4},{6,7},{7,6},{8,9},{9,8},{10,11... | collective-permute-start | bytes 1572872 | tf_op jit(solution)/shard_map/ppermute | solution.py:30
  48.0 8.0 %collective-permute-start.8 = (bf16[128,2048]{1,0:T(8,128)(2,1)S(1)}, bf16[128,2048]{1,0:T(8,128)(2,1)S(1)}, u32[]{:S(2)}, u32[]{:S(2)}) collective-permute-start(bf16[128,2048]{1,0:T(8,128)(2,1)S(1)} %get-tuple-element.26), channel_id=1, source_target_pairs={{0,1},{1,0},{2,3},{3,2},{4,5},{5,4},{6,7},{7,6},{8,9},{9,8},{10,11... | collective-permute-start | bytes 1572872 | tf_op jit(solution)/shard_map/ppermute | solution.py:30
  48.4 7.4 %collective-permute-start = (bf16[16,1024]{1,0:T(8,128)(2,1)S(1)}, bf16[16,1024]{1,0:T(8,128)(2,1)S(1)}, u32[]{:S(2)}, u32[]{:S(2)}) collective-permute-start(bf16[16,1024]{1,0:T(8,128)(2,1)S(1)} %get-tuple-element.23), channel_id=1, source_target_pairs={{0,1},{1,2},{2,3},{3,4},{4,5},{5,6},{6,7},{7,8},{8,9},{9,10},{10,1... | collective-permute-start | bytes 98312 | tf_op jit(solution)/shard_map/ppermute | solution.py:30
  48.5 22.8 %collective-permute-start.2 = (bf16[128,2048]{1,0:T(8,128)(2,1)S(1)}, bf16[128,2048]{1,0:T(8,128)(2,1)S(1)}, u32[]{:S(2)}, u32[]{:S(2)}) collective-permute-start(bf16[128,2048]{1,0:T(8,128)(2,1)S(1)} %copy-done.1), channel_id=1, source_target_pairs={{0,2},{1,3},{2,0},{3,1},{4,6},{5,7},{6,4},{7,5},{8,10},{9,11},{10,... | collective-permute-start | bytes 1572872 | tf_op jit(solution)/shard_map/ppermute | solution.py:30
  50.6 6.0 %collective-permute-start.15 = (bf16[128,2048]{1,0:T(8,128)(2,1)S(1)}, bf16[128,2048]{1,0:T(8,128)(2,1)S(1)}, u32[]{:S(2)}, u32[]{:S(2)}) collective-permute-start(bf16[128,2048]{1,0:T(8,128)(2,1)S(1)} %get-tuple-element.33), channel_id=1, source_target_pairs={{0,1},{1,0},{2,3},{3,2},{4,5},{5,4},{6,7},{7,6},{8,9},{9,8},{10,11... | collective-permute-start | bytes 1572872 | tf_op jit(solution)/shard_map/ppermute | solution.py:30
  52.0 6.7 %collective-permute-start.24 = (bf16[128,1024]{1,0:T(8,128)(2,1)S(1)}, bf16[128,1024]{1,0:T(8,128)(2,1)S(1)}, u32[]{:S(2)}, u32[]{:S(2)}) collective-permute-start(bf16[128,1024]{1,0:T(8,128)(2,1)S(1)} %get-tuple-element.44), channel_id=1, source_target_pairs={{0,8},{1,17},{2,10},{3,19},{4,12},{5,21},{6,14},{7,23},{8,0},{9,25... | collective-permute-start | bytes 786440 | tf_op jit(solution)/shard_map/ppermute | solution.py:30
  55.8 38.2 %collective-permute-start.4 = (bf16[128,2048]{1,0:T(8,128)(2,1)S(1)}, bf16[128,2048]{1,0:T(8,128)(2,1)S(1)}, u32[]{:S(2)}, u32[]{:S(2)}) collective-permute-start(bf16[128,2048]{1,0:T(8,128)(2,1)S(1)} %copy-done.1), channel_id=1, source_target_pairs={{0,4},{1,5},{2,6},{3,7},{4,0},{5,1},{6,2},{7,3},{8,12},{9,13},{10,... | collective-permute-start | bytes 1572872 | tf_op jit(solution)/shard_map/ppermute | solution.py:30
  56.0 39.8 %collective-permute-start.6 = (bf16[128,2048]{1,0:T(8,128)(2,1)S(1)}, bf16[128,2048]{1,0:T(8,128)(2,1)S(1)}, u32[]{:S(2)}, u32[]{:S(2)}) collective-permute-start(bf16[128,2048]{1,0:T(8,128)(2,1)S(1)} %copy-done.1), channel_id=1, source_target_pairs={{0,6},{1,7},{2,4},{3,5},{4,2},{5,3},{6,0},{7,1},{8,14},{9,15},{10,... | collective-permute-start | bytes 1572872 | tf_op jit(solution)/shard_map/ppermute | solution.py:30
  56.6 39.2 %collective-permute-start.14 = (bf16[128,2048]{1,0:T(8,128)(2,1)S(1)}, bf16[128,2048]{1,0:T(8,128)(2,1)S(1)}, u32[]{:S(2)}, u32[]{:S(2)}) collective-permute-start(bf16[128,2048]{1,0:T(8,128)(2,1)S(1)} %add_convert_fusion.1), channel_id=1, source_target_pairs={{0,8},{1,17},{2,10},{3,19},{4,12},{5,21},{6,14},{7,23},{8,0},{9,25... | collective-permute-start | bytes 1572872 | tf_op jit(solution)/shard_map/ppermute | solution.py:30
  58.8 35.2 %collective-permute-start.19 = (bf16[128,1024]{1,0:T(8,128)(2,1)S(1)}, bf16[128,1024]{1,0:T(8,128)(2,1)S(1)}, u32[]{:S(2)}, u32[]{:S(2)}) collective-permute-start(bf16[128,1024]{1,0:T(8,128)(2,1)S(1)} %get-tuple-element.45), channel_id=1, source_target_pairs={{0,8},{1,17},{2,10},{3,19},{4,12},{5,21},{6,14},{7,23},{8,0},{9,25... | collective-permute-start | bytes 786440 | tf_op jit(solution)/shard_map/ppermute | solution.py:30
  71.3 25.0 %collective-permute-start.25 = (bf16[128,1024]{1,0:T(8,128)(2,1)S(1)}, bf16[128,1024]{1,0:T(8,128)(2,1)S(1)}, u32[]{:S(2)}, u32[]{:S(2)}) collective-permute-start(bf16[128,1024]{1,0:T(8,128)(2,1)S(1)} %pass_on.3), channel_id=1, source_target_pairs={{0,16},{1,9},{2,18},{3,11},{4,20},{5,13},{6,22},{7,15},{8,24},{9,1... | collective-permute-start | bytes 786440 | tf_op jit(solution)/shard_map/ppermute | solution.py:30
  93.9 4.5 %collective-permute-start.1 = (bf16[128,2048]{1,0:T(8,128)(2,1)S(1)}, bf16[128,2048]{1,0:T(8,128)(2,1)S(1)}, u32[]{:S(2)}, u32[]{:S(2)}) collective-permute-start(bf16[128,2048]{1,0:T(8,128)(2,1)S(1)} %copy-done.1), channel_id=1, source_target_pairs={{0,1},{1,0},{2,3},{3,2},{4,5},{5,4},{6,7},{7,6},{8,9},{9,8},{10,11... | collective-permute-start | bytes 1572872 | tf_op jit(solution)/shard_map/ppermute | solution.py:30
  94.0 10.1 %collective-permute-start.3 = (bf16[128,2048]{1,0:T(8,128)(2,1)S(1)}, bf16[128,2048]{1,0:T(8,128)(2,1)S(1)}, u32[]{:S(2)}, u32[]{:S(2)}) collective-permute-start(bf16[128,2048]{1,0:T(8,128)(2,1)S(1)} %collective-permute-done.2.refs_2_), channel_id=1, source_target_pairs={{0,1},{1,0},{2,3},{3,2},{4,5},{5,4},{6,7},{7,6},{8,9},{9,8},{10,11... | collective-permute-start | bytes 1572872 | tf_op jit(solution)/shard_map/ppermute | solution.py:30
  95.7 12.4 %collective-permute-start.5 = (bf16[128,2048]{1,0:T(8,128)(2,1)S(1)}, bf16[128,2048]{1,0:T(8,128)(2,1)S(1)}, u32[]{:S(2)}, u32[]{:S(2)}) collective-permute-start(bf16[128,2048]{1,0:T(8,128)(2,1)S(1)} %collective-permute-done.4.refs_0_), channel_id=1, source_target_pairs={{0,1},{1,0},{2,3},{3,2},{4,5},{5,4},{6,7},{7,6},{8,9},{9,8},{10,11... | collective-permute-start | bytes 1572872 | tf_op jit(solution)/shard_map/ppermute | solution.py:30
  95.8 15.4 %collective-permute-start.7 = (bf16[128,2048]{1,0:T(8,128)(2,1)S(1)}, bf16[128,2048]{1,0:T(8,128)(2,1)S(1)}, u32[]{:S(2)}, u32[]{:S(2)}) collective-permute-start(bf16[128,2048]{1,0:T(8,128)(2,1)S(1)} %collective-permute-done.6.refs_2_), channel_id=1, source_target_pairs={{0,1},{1,0},{2,3},{3,2},{4,5},{5,4},{6,7},{7,6},{8,9},{9,8},{10,11... | collective-permute-start | bytes 1572872 | tf_op jit(solution)/shard_map/ppermute | solution.py:30
  96.3 10.2 %collective-permute-start.20 = (bf16[128,1024]{1,0:T(8,128)(2,1)S(1)}, bf16[128,1024]{1,0:T(8,128)(2,1)S(1)}, u32[]{:S(2)}, u32[]{:S(2)}) collective-permute-start(bf16[128,1024]{1,0:T(8,128)(2,1)S(1)} %pass_on.2), channel_id=1, source_target_pairs={{0,16},{1,9},{2,18},{3,11},{4,20},{5,13},{6,22},{7,15},{8,24},{9,1... | collective-permute-start | bytes 786440 | tf_op jit(solution)/shard_map/ppermute | solution.py:30
  98.5 15.1 %copy-start.5 = (f32[2048]{0:T(1024)S(1)}, f32[2048]{0:T(1024)}, u32[]{:S(2)}) copy-start(f32[2048]{0:T(1024)} %param.17) | copy-start | bytes 24580
  98.5 12.7 %collective-permute-start.26 = (bf16[32,1024]{1,0:T(8,128)(2,1)S(1)}, bf16[32,1024]{1,0:T(8,128)(2,1)S(1)}, u32[]{:S(2)}, u32[]{:S(2)}) collective-permute-start(bf16[32,1024]{1,0:T(8,128)(2,1)S(1)} %get-tuple-element.41), channel_id=1, source_target_pairs={{0,2},{1,3},{2,0},{3,1},{4,6},{5,7},{6,4},{7,5},{8,10},{9,11},{10,... | collective-permute-start | bytes 196616 | tf_op jit(solution)/shard_map/ppermute | solution.py:30
  105.4 11.4 %collective-permute-start.27 = (bf16[32,1024]{1,0:T(8,128)(2,1)S(1)}, bf16[32,1024]{1,0:T(8,128)(2,1)S(1)}, u32[]{:S(2)}, u32[]{:S(2)}) collective-permute-start(bf16[32,1024]{1,0:T(8,128)(2,1)S(1)} %get-tuple-element.42), channel_id=1, source_target_pairs={{0,4},{1,5},{2,6},{3,7},{4,0},{5,1},{6,2},{7,3},{8,12},{9,13},{10,... | collective-permute-start | bytes 196616 | tf_op jit(solution)/shard_map/ppermute | solution.py:30
  106.5 10.3 %collective-permute-start.28 = (bf16[32,1024]{1,0:T(8,128)(2,1)S(1)}, bf16[32,1024]{1,0:T(8,128)(2,1)S(1)}, u32[]{:S(2)}, u32[]{:S(2)}) collective-permute-start(bf16[32,1024]{1,0:T(8,128)(2,1)S(1)} %get-tuple-element.43), channel_id=1, source_target_pairs={{0,6},{1,7},{2,4},{3,5},{4,2},{5,3},{6,0},{7,1},{8,14},{9,15},{10,... | collective-permute-start | bytes 196616 | tf_op jit(solution)/shard_map/ppermute | solution.py:30
  108.1 8.7 %collective-permute-start.21 = (bf16[32,1024]{1,0:T(8,128)(2,1)S(1)}, bf16[32,1024]{1,0:T(8,128)(2,1)S(1)}, u32[]{:S(2)}, u32[]{:S(2)}) collective-permute-start(bf16[32,1024]{1,0:T(8,128)(2,1)S(1)} %get-tuple-element.37), channel_id=1, source_target_pairs={{0,2},{1,3},{2,0},{3,1},{4,6},{5,7},{6,4},{7,5},{8,10},{9,11},{10,... | collective-permute-start | bytes 196616 | tf_op jit(solution)/shard_map/ppermute | solution.py:30
  111.2 8.0 %collective-permute-start.22 = (bf16[32,1024]{1,0:T(8,128)(2,1)S(1)}, bf16[32,1024]{1,0:T(8,128)(2,1)S(1)}, u32[]{:S(2)}, u32[]{:S(2)}) collective-permute-start(bf16[32,1024]{1,0:T(8,128)(2,1)S(1)} %get-tuple-element.38), channel_id=1, source_target_pairs={{0,4},{1,5},{2,6},{3,7},{4,0},{5,1},{6,2},{7,3},{8,12},{9,13},{10,... | collective-permute-start | bytes 196616 | tf_op jit(solution)/shard_map/ppermute | solution.py:30
  111.2 8.0 %collective-permute-start.23 = (bf16[32,1024]{1,0:T(8,128)(2,1)S(1)}, bf16[32,1024]{1,0:T(8,128)(2,1)S(1)}, u32[]{:S(2)}, u32[]{:S(2)}) collective-permute-start(bf16[32,1024]{1,0:T(8,128)(2,1)S(1)} %get-tuple-element.39), channel_id=1, source_target_pairs={{0,6},{1,7},{2,4},{3,5},{4,2},{5,3},{6,0},{7,1},{8,14},{9,15},{10,... | collective-permute-start | bytes 196616 | tf_op jit(solution)/shard_map/ppermute | solution.py:30
  113.6 5.6 %copy-start.4 = (f32[2048]{0:T(1024)S(1)}, f32[2048]{0:T(1024)}, u32[]{:S(2)}) copy-start(f32[2048]{0:T(1024)} %param.25) | copy-start | bytes 24580

commit v5 on v4

--- a/solution.py
+++ b/solution.py
@@ -183,9 +183,10 @@
 
 
 def pack_kernel(
-    rows_ref, routes_in, weight_in, pool_ref, message_ref, tail_ref, routes_ref, weight_ref, sems
+    rows_in, gain_in, routes_in, weight_in, pool_in,
+    message_ref, tail_ref, rows_ref, gain_ref, routes_ref, weight_ref, sems,
 ):
-    half = rows_ref.shape[0] // CORES
+    half = rows_ref.shape[0]
     tokens = routes_ref.shape[1]
     experts = message_ref.shape[1] // tokens
     start = pl.multiple_of(seat()[1] * half, half)
@@ -193,8 +194,9 @@
         [
             (routes_in, routes_ref),
             (weight_in, weight_ref),
-            (rows_ref.at[pl.ds(start, half)], message_ref.at[pl.ds(0, half)]),
-            (pool_ref.at[pl.ds(pool_ref.shape[0] - REACH, REACH)], tail_ref),
+            (gain_in, gain_ref),
+            (rows_in.at[pl.ds(start, half)], rows_ref),
+            (pool_in.at[pl.ds(pool_in.shape[0] - REACH, REACH)], tail_ref),
         ],
         sems,
     )
@@ -211,27 +213,31 @@
         message_ref[half:, expert * tokens : (expert + 1) * tokens] = both.astype(jnp.bfloat16)
     copies[2].wait()
     copies[3].wait()
-
-
-def pack(rows, routes, route_weight, pool_in):
+    message_ref[:half, :] = normed_rows(rows_ref, gain_ref)
+    copies[4].wait()
+
+
+def pack(rows, gain, routes, route_weight, pool_in):
     tokens, width = rows.shape
     choose = routes.shape[1]
     return pl.pallas_call(
         pack_kernel,
-        in_specs=[HBM] * 4,
+        in_specs=[HBM] * 5,
         out_specs=[VMEM] * 2,
         out_shape=[
             jax.ShapeDtypeStruct((tokens // CORES + 8, width), rows.dtype),
             jax.ShapeDtypeStruct((REACH, pool_in.shape[1]), pool_in.dtype),
         ],
         scratch_shapes=[
+            pltpu.VMEM((tokens // CORES, width), rows.dtype),
+            pltpu.VMEM((1, width), jnp.float32),
             pltpu.VMEM((choose, tokens), jnp.int32),
             pltpu.VMEM((choose, tokens), jnp.float32),
-            pltpu.SemaphoreType.DMA((4,)),
+            pltpu.SemaphoreType.DMA((5,)),
         ],
-        compiler_params=pltpu.CompilerParams(vmem_limit_bytes=2 << 20),
+        compiler_params=pltpu.CompilerParams(vmem_limit_bytes=3 << 20),
         name="pack",
-    )(*from_hbm(rows, routes.T, route_weight.T, pool_in))
+    )(*from_hbm(rows, gain.reshape(1, width), routes.T, route_weight.T, pool_in))
 
 
 def own_kernel(
@@ -291,7 +297,7 @@
     )(*from_hbm(gain.reshape(1, width), rows, gate_weight, up_weight, down_weight), message)
 
 
-def expert_kernel(gain_ref, gate_ref, up_ref, down_ref, *refs, groups):
+def expert_kernel(gate_ref, up_ref, down_ref, *refs, groups):
     inputs, outputs = refs[: 2 * groups], refs[2 * groups : 4 * groups]
     normed, hidden, total = refs[4 * groups :]
     first, core = lax.axis_index("ep") * gate_ref.shape[0], seat()[1]
@@ -300,7 +306,7 @@
         mine_ref, other_ref = inputs[2 * group : 2 * group + 2]
         for source, which in ((mine_ref, core), (other_ref, 1 - core)):
             start = pl.multiple_of((2 * group + which) * half, half)
-            normed[pl.ds(start, half), :] = normed_rows(source.at[:half], gain_ref)
+            normed[pl.ds(start, half), :] = source[:half, :]
     for expert in range(gate_ref.shape[0]):
         shares = [share_of(ref, first + expert, 2 * half) for ref in inputs[::2]]
         scale = jnp.concatenate(shares, axis=0)
@@ -308,7 +314,7 @@
     store_halves(hidden, down_ref, total, core, outputs)
 
 
-def expert_partial(chunks, gain, gate_weight, up_weight, down_weight, block):
+def expert_partial(chunks, gate_weight, up_weight, down_weight, block):
     groups = len(chunks)
     half, width = chunks[0][0].shape
     half -= 8
@@ -317,7 +323,7 @@
     inputs = [array for chunk in chunks for array in chunk]
     outputs = pl.pallas_call(
         lambda *refs: expert_kernel(*refs, groups=groups),
-        in_specs=[VMEM] * (4 + len(inputs)),
+        in_specs=[VMEM] * (3 + len(inputs)),
         out_specs=[VMEM] * (2 * groups),
         out_shape=[jax.ShapeDtypeStruct((half, width), jnp.bfloat16)] * (2 * groups),
         scratch_shapes=[
@@ -332,8 +338,75 @@
             transcendentals=rows * local * units,
         ),
         name="experts",
-    )(gain.reshape(1, width), gate_weight, up_weight, down_weight, *inputs)
+    )(gate_weight, up_weight, down_weight, *inputs)
     return [(outputs[2 * g], outputs[2 * g + 1]) for g in range(groups)]
+
+
+def half_kernel(gate_ref, up_ref, down_ref, *refs, rest):
+    inputs, (kept_ref, sent_ref, normed, hidden, total) = refs[:-5], refs[-5:]
+    core = seat()[1]
+    first = lax.axis_index("ep") * gate_ref.shape[0]
+    half = normed.shape[0] // len(inputs)
+    side = 1 - core if rest else core
+    for group, source in enumerate(inputs):
+        normed[group * half : (group + 1) * half, :] = source[:half, :]
+    for expert in range(gate_ref.shape[0]):
+        shares = [share_of(ref, first + expert, 2 * half) for ref in inputs]
+        shares = [jnp.where(side == 0, share[:half], share[half:]) for share in shares]
+        scale = jnp.concatenate(shares, axis=0)
+        fill_hidden(hidden, expert, scale, normed, gate_ref.at[expert], up_ref.at[expert])
+    result = jnp.dot(hidden[...], down_ref[...], preferred_element_type=jnp.float32)
+    total[...] = result.astype(jnp.bfloat16).reshape(total.shape)
+    blocks, block, _ = total.shape
+    for k in range(blocks // CORES):
+        rows_of = slice(k * block, (k + 1) * block)
+        kept_ref[rows_of, :] = total[CORES * k + core]
+        sent_ref[rows_of, :] = total[CORES * k + 1 - core]
+
+
+def half_partial(inputs, gate_weight, up_weight, down_weight, block, rest):
+    half, width = inputs[0].shape
+    half -= 8
+    rows = len(inputs) * half
+    local, _, units = gate_weight.shape
+    return pl.pallas_call(
+        lambda *refs: half_kernel(*refs, rest=rest),
+        in_specs=[VMEM] * (3 + len(inputs)),
+        out_specs=[VMEM] * 2,
+        out_shape=[jax.ShapeDtypeStruct((rows // CORES, width), jnp.bfloat16)] * 2,
+        scratch_shapes=[
+            pltpu.VMEM((rows, width), jnp.bfloat16),
+            pltpu.VMEM((rows, local * units), jnp.bfloat16),
+            pltpu.VMEM((rows // block, block, width), jnp.bfloat16),
+        ],
+        compiler_params=pltpu.CompilerParams(vmem_limit_bytes=12 << 20),
+        cost_estimate=pl.CostEstimate(
+            flops=6 * rows * width * local * units,
+            bytes_accessed=4 * rows * width,
+            transcendentals=rows * local * units,
+        ),
+        name="halves",
+    )(gate_weight, up_weight, down_weight, *inputs)
+
+
+def join_kernel(kept_mine, kept_rest, back_mine, back_rest, out_ref, *, group):
+    half = out_ref.shape[0] // 2
+    core = seat()[1]
+    here, there = (slice(g * half, (g + 1) * half) for g in (group, 1 - group))
+    for kept, back, side in ((kept_mine, back_rest, core), (kept_rest, back_mine, 1 - core)):
+        rows_of = pl.ds(pl.multiple_of(side * half, half), half)
+        out_ref[rows_of, :] = added(kept[here, :], back[there, :])
+
+
+def join_halves(kept_mine, kept_rest, back_mine, back_rest, group):
+    return pl.pallas_call(
+        lambda *refs: join_kernel(*refs, group=group),
+        in_specs=[VMEM] * 4,
+        out_specs=VMEM,
+        out_shape=jax.ShapeDtypeStruct(kept_mine.shape, kept_mine.dtype),
+        compiler_params=pltpu.CompilerParams(vmem_limit_bytes=4 << 20),
+        name="join",
+    )(kept_mine, kept_rest, back_mine, back_rest)
 
 
 def spread_kernel(early_ref, late_ref, own_ref, *out_refs, start):
@@ -378,12 +451,12 @@
 
 
 def finish(gain, parts):
-    block, width = parts[0].shape
+    block = parts[0].shape[0]
     return pl.pallas_call(
         finish_kernel,
         in_specs=[VMEM] * (1 + len(parts)),
         out_specs=VMEM,
-        out_shape=jax.ShapeDtypeStruct((block, width * PIECES), jnp.bfloat16),
+        out_shape=jax.ShapeDtypeStruct((block, gain.shape[0]), jnp.bfloat16),
         compiler_params=pltpu.CompilerParams(vmem_limit_bytes=4 << 20),
         name="finish",
     )(gain.reshape(1, -1), *parts)
@@ -419,35 +492,36 @@
     from_b = to_group(message, 1)
     weights = (pre_gain, gate_weight, up_weight, down_weight.reshape(-1, width), block)
     kept, sent, *held = own_partial(expert_in, message, *weights)
-    weights = (pre_gain, *held, block)
+    weights = (*held, block)
     early = kept.astype(jnp.float32) + to_core(sent).astype(jnp.float32)
     from_c = to_group(from_a, 1)
     other_b = to_core(from_a)
     other_a = to_core(from_b)
     other_c = to_core(from_c)
-    near = expert_partial([(from_a, other_a), (from_b, other_b)], *weights)
-    (kept_a, sent_a), (kept_b, sent_b) = near
-    back_a = to_core(sent_b)
-    back_b = to_core(sent_a)
-    joined_a = added(kept_a, back_a)
-    joined_b = added(kept_b, back_b)
+    kept_mine, sent = half_partial((from_a, from_b), *weights, rest=False)
+    back_mine = to_core(sent)
+    kept_rest, sent = half_partial((other_a, other_b), *weights, rest=True)
+    back_rest = to_core(sent)
+    halves = (kept_mine, kept_rest, back_mine, back_rest)
+    joined_a = join_halves(*halves, 0)
+    joined_b = join_halves(*halves, 1)
     near_sum = to_group(joined_a, 0)
     ((kept_c, sent_c),) = expert_partial([(from_c, other_c)], *weights)
     back_c = to_core(sent_c)
-    span = width // PIECES
-    columns = [slice(piece * span, (piece + 1) * span) for piece in range(PIECES)]
+    cut = width * 8 // 16
+    columns = [slice(0, cut), slice(cut, width)]
     joined_c = [added(kept_c[:, part], back_c[:, part]) for part in columns]
     passed, late = [], []
     for piece in range(PIECES):
         passing = to_group(joined_c[piece], 0)
-        passed.append(pass_on(joined_b, passing, piece * span))
+        passed.append(pass_on(joined_b, passing, columns[piece].start))
     for piece in range(PIECES):
         late.append(to_group(passed[piece], 1))
     early = lax.optimization_barrier(early + near_sum.astype(jnp.float32))
     early = early.reshape(chips, block, width)
     parts = []
     for piece in range(PIECES):
-        own, *pieces = spread(early, late[piece].reshape(chips, block, span), piece * span)
+        own, *pieces = spread(early, late[piece].reshape(chips, block, -1), columns[piece].start)
         parts.append(own)
         for step in range(1, chips):
             parts.append(to_chip(pieces[step - 1], step))
@@ -599,7 +673,9 @@
     dense = dense and experts_in_all * tokens_here <= expert_in.shape[1]
     tail = pool_in[rows - REACH :]
     if dense:
-        message, tail = pack(expert_in, routes, route_weight, pool_in)
+        message, tail = pack(
+            expert_in, pre_gain, routes, route_weight, pool_in
+        )
     rim = to_next(tail)
     if dense:
         expert_out = dense_experts(
@@ -610,9 +686,11 @@
             expert_in, routes, route_weight, pre_gain, gate_weight, up_weight, down_weight,
             post_gain,
         )
-    shards = []
-    for step in range(chips):
-        shard = to_chip(out_weight, step) if step else out_weight
+    shards, held = [], [out_weight]
+    for step in range(1, chips):
+        longer = step & (step - 1) if paired(chips) else 0
+        held.append(to_chip(held[longer], step ^ longer))
+    for shard in held:
         shards += [shard, to_core(shard)]
     mixed = mix(rim, pool_in, pool_weight, pool_gain)
     half = len(shards) // 2

time: 120 us -> 90.6 us (0.76)
  waiting for transfers between devices: 57.6 us -> 32 us
  starting transfers between devices: 33.7 us -> 30.1 us
    ppermute x29, waiting for transfers between devices: 57.6 us -> 32 us  [moved(): return lax.ppermute(block, ('ep', 'tp'), route)]
    pallas_call x2 -> x1, Pallas kernels: 12.4 us -> 3.86 us  [expert_partial(): pl.pallas_call(lambda *refs: expert_kernel(*refs, groups=groups), in_spec...]
    pallas_call x1 -> x5, Pallas kernels: 1.11 us -> 9.46 us  [the longest x2 7.85 us: half_partial(): pl.pallas_call(lambda *refs: half_kernel(*refs, rest=rest), in_specs=[VME...]
    ppermute x29, starting transfers between devices: 33.7 us -> 30.1 us  [moved(): return lax.ppermute(block, ('ep', 'tp'), route)]
  transfers between devices with their start and end apart: 29 -> 29, of which waited for: 8 -> 8; matrix products, arithmetic and copies ran while one was open for 1% -> 0% of each run, Pallas kernels for 21% -> 27%
where the time goes in v5:
time: 90.6 us; the launch traced here: 90.4 us
  waiting for transfers between devices  32 us (35%)
  starting transfers between devices  30.1 us (33%)
  Pallas kernels  27 us (30%)
    ppermute x29, waiting for transfers between devices, moved(): return lax.ppermute(block, ('ep', 'tp'), route)  32 us
    ppermute x29, starting transfers between devices, moved(): return lax.ppermute(block, ('ep', 'tp'), route)  30.1 us
    pallas_call x2, Pallas kernels, half_partial(): pl.pallas_call(lambda *refs: half_kernel(*refs, rest=rest), in_specs=[VME...  7.85 us
    pallas_call x1, Pallas kernels, own_partial(): pl.pallas_call(own_kernel, in_specs=[HBM] * 5 + [VMEM], out_specs=[VMEM]...  6.82 us
    pallas_call x1, Pallas kernels, expert_partial(): pl.pallas_call(lambda *refs: expert_kernel(*refs, groups=groups), in_spec...  3.86 us
    pallas_call x1, Pallas kernels, project(): pl.pallas_call(project_kernel, grid=(rows // tile,), in_specs=[VMEM] * (3...  3.15 us
  transfers between devices with their start and end apart: 29, of which 8 were waited for; matrix products, arithmetic and copies ran while one was open for 0% of the time, Pallas kernels for 27%

profile of v5, /device:TPU:0, one launch (start us, length us, event | category | flops | bytes accessed | tf_op | source)
XLA Modules:
  0.0 90.4 jit_solution(10039738327938161000)
XLA Ops:
  0.6 1.4 %pack.1 = (bf16[136,2048]{1,0:T(8,128)(2,1)S(1)}, bf16[16,1024]{1,0:T(8,128)(2,1)S(1)}) custom-call(bf16[256,2048]{1,0:T(8,128)(2,1)} %rows_in.3, f32[1,2048]{1,0:T(1,128)} %bitcast.18, s32[4,256]{1,0:T(4,128)} %bitcast.20, f32[4,256]{1,0:T(4,128)} %bitcast.21, bf16[512,1024]{1,0:T(8,128)(2,1)} %rows_ref.1), custom_call_target="tpu_custom_call" | custom-call | tf_op jit(solution)/shard_map/pack/pallas_call | solution.py:223
  2.0 3.0 %collective-permute-start.9 = (bf16[136,2048]{1,0:T(8,128)(2,1)S(1)}, bf16[136,2048]{1,0:T(8,128)(2,1)S(1)}, u32[]{:S(2)}, u32[]{:S(2)}) collective-permute-start(bf16[136,2048]{1,0:T(8,128)(2,1)S(1)} %get-tuple-element.24.message_ref), channel_id=1, source_target_pairs={{0,8},{1,17},{2,10},{3,19},{4,12},{5,21},{6,14},{7,23},{8,0},{9,25... | collective-permute-start | bytes 1671176 | tf_op jit(solution)/shard_map/ppermute | solution.py:30
  5.0 7.5 %collective-permute-done.9.refs_3_ = bf16[136,2048]{1,0:T(8,128)(2,1)S(1)} collective-permute-done((bf16[136,2048]{1,0:T(8,128)(2,1)S(1)}, bf16[136,2048]{1,0:T(8,128)(2,1)S(1)}, u32[]{:S(2)}, u32[]{:S(2)}) %collective-permute-start.9) | collective-permute-done | bytes 557088 | tf_op jit(solution)/shard_map/ppermute | solution.py:30
  12.5 2.0 %collective-permute-start.16 = (bf16[136,2048]{1,0:T(8,128)(2,1)S(1)}, bf16[136,2048]{1,0:T(8,128)(2,1)S(1)}, u32[]{:S(2)}, u32[]{:S(2)}) collective-permute-start(bf16[136,2048]{1,0:T(8,128)(2,1)S(1)} %collective-permute-done.9.refs_3_), channel_id=1, source_target_pairs={{0,16},{1,9},{2,18},{3,11},{4,20},{5,13},{6,22},{7,15},{8,24},{9,1... | collective-permute-start | bytes 1671176 | tf_op jit(solution)/shard_map/ppermute | solution.py:30
  14.6 3.1 %collective-permute-start.4 = (bf16[128,2048]{1,0:T(8,128)(2,1)}, bf16[128,2048]{1,0:T(8,128)(2,1)S(1)}, u32[]{:S(2)}, u32[]{:S(2)}) collective-permute-start(bf16[128,2048]{1,0:T(8,128)(2,1)} %refs_0_.1), channel_id=1, source_target_pairs={{0,4},{1,5},{2,6},{3,7},{4,0},{5,1},{6,2},{7,3},{8,12},{9,13},{10,... | collective-permute-start | bytes 1572872 | tf_op jit(solution)/shard_map/ppermute | solution.py:30
  17.7 4.4 %collective-permute-done.16.refs_3_ = bf16[136,2048]{1,0:T(8,128)(2,1)S(1)} collective-permute-done((bf16[136,2048]{1,0:T(8,128)(2,1)S(1)}, bf16[136,2048]{1,0:T(8,128)(2,1)S(1)}, u32[]{:S(2)}, u32[]{:S(2)}) %collective-permute-start.16) | collective-permute-done | bytes 557088 | tf_op jit(solution)/shard_map/ppermute | solution.py:30
  22.1 6.8 %own.1 = (bf16[128,2048]{1,0:T(8,128)(2,1)S(1)}, bf16[128,2048]{1,0:T(8,128)(2,1)S(1)}, bf16[2,2048,512]{2,1,0:T(8,128)(2,1)S(1)}, bf16[2,2048,512]{2,1,0:T(8,128)(2,1)S(1)}, bf16[1024,2048]{1,0:T(8,128)(2,1)S(1)}) custom-call(f32[1,2048]{1,0:T(1,128)} %bitcast.19, bf16[256,2048]{1,0:T(8,128)(2,1)} %rows_in.3, bf16[2,2048,512]{2,1,0:T(8,128)(2,1)} %gate_in.1, ...), custom_call_target="tpu_custom_call" | custom-call | flops 3221225472 | bytes 14680064 | tf_op jit(solution)/shard_map/own/pallas_call | solution.py:277
  28.9 0.6 collective-permute-start.12
  29.5 0.1 collective-permute-start.11
  29.6 3.8 %halves.2 = (bf16[128,2048]{1,0:T(8,128)(2,1)S(1)}, bf16[128,2048]{1,0:T(8,128)(2,1)S(1)}) custom-call(bf16[2,2048,512]{2,1,0:T(8,128)(2,1)S(1)} %get-tuple-element.27.refs_0_, bf16[2,2048,512]{2,1,0:T(8,128)(2,1)S(1)} %get-tuple-element.28.refs_1_, bf16[1024,2048]{1,0:T(8,128)(2,1)S(1)} %get-tuple-element.29.refs_2_, ...), custom_call_target="tpu_custom_call" | custom-call | flops 3221225472 | bytes 2097152 | tf_op jit(solution)/shard_map/halves/pallas_call | solution.py:372
  33.4 0.5 collective-permute-start.13
  33.9 3.9 %experts.1 = (bf16[128,2048]{1,0:T(8,128)(2,1)S(1)}, bf16[128,2048]{1,0:T(8,128)(2,1)S(1)}) custom-call(bf16[2,2048,512]{2,1,0:T(8,128)(2,1)S(1)} %get-tuple-element.27.refs_0_, bf16[2,2048,512]{2,1,0:T(8,128)(2,1)S(1)} %get-tuple-element.28.refs_1_, bf16[1024,2048]{1,0:T(8,128)(2,1)S(1)} %get-tuple-element.29.refs_2_, ...), custom_call_target="tpu_custom_call" | custom-call | flops 3221225472 | bytes 2097152 | tf_op jit(solution)/shard_map/experts/pallas_call | solution.py:324
  37.8 0.1 collective-permute-start.18
  37.9 4.1 %halves.3 = (bf16[128,2048]{1,0:T(8,128)(2,1)S(1)}, bf16[128,2048]{1,0:T(8,128)(2,1)S(1)}) custom-call(bf16[2,2048,512]{2,1,0:T(8,128)(2,1)S(1)} %get-tuple-element.27.refs_0_, bf16[2,2048,512]{2,1,0:T(8,128)(2,1)S(1)} %get-tuple-element.28.refs_1_, bf16[1024,2048]{1,0:T(8,128)(2,1)S(1)} %get-tuple-element.29.refs_2_, ...), custom_call_target="tpu_custom_call" | custom-call | flops 3221225472 | bytes 2097152 | tf_op jit(solution)/shard_map/halves/pallas_call | solution.py:372
  42.0 0.5 collective-permute-start.14
  42.5 0.1 collective-permute-start.8
  42.6 0.4 collective-permute-start
  43.1 0.2 add_convert_fusion
  43.3 2.1 %collective-permute-start.24 = (bf16[128,1024]{1,0:T(8,128)(2,1)S(1)}, bf16[128,1024]{1,0:T(8,128)(2,1)S(1)}, u32[]{:S(2)}, u32[]{:S(2)}) collective-permute-start(bf16[128,1024]{1,0:T(8,128)(2,1)S(1)} %get-tuple-element.44), channel_id=1, source_target_pairs={{0,8},{1,17},{2,10},{3,19},{4,12},{5,21},{6,14},{7,23},{8,0},{9,25... | collective-permute-start | bytes 786440 | tf_op jit(solution)/shard_map/ppermute | solution.py:30
  45.3 1.6 %collective-permute-start.2 = (bf16[128,2048]{1,0:T(8,128)(2,1)S(1)}, bf16[128,2048]{1,0:T(8,128)(2,1)S(1)}, u32[]{:S(2)}, u32[]{:S(2)}) collective-permute-start(bf16[128,2048]{1,0:T(8,128)(2,1)S(1)} %copy-done.1), channel_id=1, source_target_pairs={{0,2},{1,3},{2,0},{3,1},{4,6},{5,7},{6,4},{7,5},{8,10},{9,11},{10,... | collective-permute-start | bytes 1572872 | tf_op jit(solution)/shard_map/ppermute | solution.py:30
  46.9 0.4 collective-permute-start.6
  47.4 0.1 join.2
  47.5 2.9 %collective-permute-done.rim_ref = bf16[16,1024]{1,0:T(8,128)(2,1)S(1)} collective-permute-done((bf16[16,1024]{1,0:T(8,128)(2,1)S(1)}, bf16[16,1024]{1,0:T(8,128)(2,1)S(1)}, u32[]{:S(2)}, u32[]{:S(2)}) %collective-permute-start) | collective-permute-done | bytes 32800 | tf_op jit(solution)/shard_map/ppermute | solution.py:30
  50.4 0.4 collective-permute-start.15
  50.8 1.6 %collective-permute-start.19 = (bf16[128,1024]{1,0:T(8,128)(2,1)S(1)}, bf16[128,1024]{1,0:T(8,128)(2,1)S(1)}, u32[]{:S(2)}, u32[]{:S(2)}) collective-permute-start(bf16[128,1024]{1,0:T(8,128)(2,1)S(1)} %get-tuple-element.45), channel_id=1, source_target_pairs={{0,8},{1,17},{2,10},{3,19},{4,12},{5,21},{6,14},{7,23},{8,0},{9,25... | collective-permute-start | bytes 786440 | tf_op jit(solution)/shard_map/ppermute | solution.py:30
  52.4 0.1 join.3.refs_0_
  52.6 1.4 %collective-permute-start.25 = (bf16[128,1024]{1,0:T(8,128)(2,1)S(1)}, bf16[128,1024]{1,0:T(8,128)(2,1)S(1)}, u32[]{:S(2)}, u32[]{:S(2)}) collective-permute-start(bf16[128,1024]{1,0:T(8,128)(2,1)S(1)} %pass_on.3), channel_id=1, source_target_pairs={{0,16},{1,9},{2,18},{3,11},{4,20},{5,13},{6,22},{7,15},{8,24},{9,1... | collective-permute-start | bytes 786440 | tf_op jit(solution)/shard_map/ppermute | solution.py:30
  54.0 6.4 %collective-permute-done.2.refs_2_ = bf16[128,2048]{1,0:T(8,128)(2,1)S(1)} collective-permute-done((bf16[128,2048]{1,0:T(8,128)(2,1)S(1)}, bf16[128,2048]{1,0:T(8,128)(2,1)S(1)}, u32[]{:S(2)}, u32[]{:S(2)}) %collective-permute-start.2) | collective-permute-done | bytes 524320 | tf_op jit(solution)/shard_map/ppermute | solution.py:30
  60.4 0.1 collective-permute-start.1
  60.5 4.6 %collective-permute-done.19.refs_1_ = bf16[128,1024]{1,0:T(8,128)(2,1)S(1)} collective-permute-done((bf16[128,1024]{1,0:T(8,128)(2,1)S(1)}, bf16[128,1024]{1,0:T(8,128)(2,1)S(1)}, u32[]{:S(2)}, u32[]{:S(2)}) %collective-permute-start.19) | collective-permute-done | bytes 262176 | tf_op jit(solution)/shard_map/ppermute | solution.py:30
  65.2 1.2 %mix.1.mixed_ref = bf16[512,1024]{1,0:T(8,128)(2,1)S(1)} custom-call(bf16[16,1024]{1,0:T(8,128)(2,1)S(1)} %collective-permute-done.rim_ref, bf16[512,1024]{1,0:T(8,128)(2,1)S(1)} %copy-done, bf16[4,256,256]{2,1,0:T(8,128)(2,1)S(1)} %copy-done.2, f32[1,1024]{1,0:T(1,128)S(1)} %bitcast.16), custom_call_target="tpu_custom_call" | custom-call | flops 268435456 | bytes 2097152 | tf_op jit(solution)/shard_map/mix/pallas_call | solution.py:554
  66.4 5.2 %collective-permute-done.6.refs_2_ = bf16[128,2048]{1,0:T(8,128)(2,1)S(1)} collective-permute-done((bf16[128,2048]{1,0:T(8,128)(2,1)S(1)}, bf16[128,2048]{1,0:T(8,128)(2,1)S(1)}, u32[]{:S(2)}, u32[]{:S(2)}) %collective-permute-start.6) | collective-permute-done | bytes 524320 | tf_op jit(solution)/shard_map/ppermute | solution.py:30
  71.7 0.1 collective-permute-start.5
  71.8 0.4 collective-permute-start.7
  72.2 0.6 collective-permute-start.20
  72.8 0.2 convert_add_fusion
  73.0 0.1 spread.3
  73.1 1.3 %collective-permute-start.26 = (bf16[32,1024]{1,0:T(8,128)(2,1)S(1)}, bf16[32,1024]{1,0:T(8,128)(2,1)S(1)}, u32[]{:S(2)}, u32[]{:S(2)}) collective-permute-start(bf16[32,1024]{1,0:T(8,128)(2,1)S(1)} %get-tuple-element.41), channel_id=1, source_target_pairs={{0,2},{1,3},{2,0},{3,1},{4,6},{5,7},{6,4},{7,5},{8,10},{9,11},{10,... | collective-permute-start | bytes 196616 | tf_op jit(solution)/shard_map/ppermute | solution.py:30
  74.4 1.4 %near.1.near_ref = f32[512,2048]{1,0:T(8,128)S(1)} custom-call(bf16[512,1024]{1,0:T(8,128)(2,1)S(1)} %mix.1.mixed_ref, bf16[128,2048]{1,0:T(8,128)(2,1)S(1)} %copy-done.1, bf16[128,2048]{1,0:T(8,128)(2,1)S(1)} %collective-permute-done.1.refs_1_, bf16[128,2048]{1,0:T(8,128)(2,1)S(1)} %collective-permute-done.2.refs_2_, ...), custom_call_target="tpu_custom_call" | custom-call | flops 1073741824 | bytes 4194304 | tf_op jit(solution)/shard_map/near/pallas_call | solution.py:595
  75.8 2.2 %collective-permute-start.27 = (bf16[32,1024]{1,0:T(8,128)(2,1)S(1)}, bf16[32,1024]{1,0:T(8,128)(2,1)S(1)}, u32[]{:S(2)}, u32[]{:S(2)}) collective-permute-start(bf16[32,1024]{1,0:T(8,128)(2,1)S(1)} %get-tuple-element.42), channel_id=1, source_target_pairs={{0,4},{1,5},{2,6},{3,7},{4,0},{5,1},{6,2},{7,3},{8,12},{9,13},{10,... | collective-permute-start | bytes 196616 | tf_op jit(solution)/shard_map/ppermute | solution.py:30
  78.0 0.5 collective-permute-done.20
  78.6 2.9 %collective-permute-start.28 = (bf16[32,1024]{1,0:T(8,128)(2,1)S(1)}, bf16[32,1024]{1,0:T(8,128)(2,1)S(1)}, u32[]{:S(2)}, u32[]{:S(2)}) collective-permute-start(bf16[32,1024]{1,0:T(8,128)(2,1)S(1)} %get-tuple-element.43), channel_id=1, source_target_pairs={{0,6},{1,7},{2,4},{3,5},{4,2},{5,3},{6,0},{7,1},{8,14},{9,15},{10,... | collective-permute-start | bytes 196616 | tf_op jit(solution)/shard_map/ppermute | solution.py:30
  81.6 0.1 collective-permute-start.21
  81.6 1.4 %collective-permute-start.22 = (bf16[32,1024]{1,0:T(8,128)(2,1)S(1)}, bf16[32,1024]{1,0:T(8,128)(2,1)S(1)}, u32[]{:S(2)}, u32[]{:S(2)}) collective-permute-start(bf16[32,1024]{1,0:T(8,128)(2,1)S(1)} %get-tuple-element.38), channel_id=1, source_target_pairs={{0,4},{1,5},{2,6},{3,7},{4,0},{5,1},{6,2},{7,3},{8,12},{9,13},{10,... | collective-permute-start | bytes 196616 | tf_op jit(solution)/shard_map/ppermute | solution.py:30
  83.1 2.9 %collective-permute-start.23 = (bf16[32,1024]{1,0:T(8,128)(2,1)S(1)}, bf16[32,1024]{1,0:T(8,128)(2,1)S(1)}, u32[]{:S(2)}, u32[]{:S(2)}) collective-permute-start(bf16[32,1024]{1,0:T(8,128)(2,1)S(1)} %get-tuple-element.39), channel_id=1, source_target_pairs={{0,6},{1,7},{2,4},{3,5},{4,2},{5,3},{6,0},{7,1},{8,14},{9,15},{10,... | collective-permute-start | bytes 196616 | tf_op jit(solution)/shard_map/ppermute | solution.py:30
  86.0 3.2 %project.1 = bf16[512,2048]{1,0:T(8,128)(2,1)} custom-call(bf16[512,1024]{1,0:T(8,128)(2,1)S(1)} %mix.1.mixed_ref, f32[512,2048]{1,0:T(8,128)S(1)} %near.1.near_ref, f32[1,2048]{1,0:T(1,128)S(1)} %bitcast.15, bf16[128,2048]{1,0:T(8,128)(2,1)S(1)} %collective-permute-done.4.refs_0_, bf16[128,2048]{1,0:T(8,128)(2,1)S(1)} %collective-permute-done.5.refs_1_, ...), custom_call_target="tpu_custom_call" | custom-call | flops 1073741824 | bytes 6291456 | tf_op jit(solution)/shard_map/project/pallas_call | solution.py:633
  89.2 0.4 collective-permute-done.22.refs_2_
  89.5 0.8 finish.1
  (39 shorter events, 0.3 us)
Async XLA Ops:
  2.0 10.5 %collective-permute-start.9 = (bf16[136,2048]{1,0:T(8,128)(2,1)S(1)}, bf16[136,2048]{1,0:T(8,128)(2,1)S(1)}, u32[]{:S(2)}, u32[]{:S(2)}) collective-permute-start(bf16[136,2048]{1,0:T(8,128)(2,1)S(1)} %get-tuple-element.24.message_ref), channel_id=1, source_target_pairs={{0,8},{1,17},{2,10},{3,19},{4,12},{5,21},{6,14},{7,23},{8,0},{9,25... | collective-permute-start | bytes 1671176 | tf_op jit(solution)/shard_map/ppermute | solution.py:30
  12.5 9.6 %collective-permute-start.16 = (bf16[136,2048]{1,0:T(8,128)(2,1)S(1)}, bf16[136,2048]{1,0:T(8,128)(2,1)S(1)}, u32[]{:S(2)}, u32[]{:S(2)}) collective-permute-start(bf16[136,2048]{1,0:T(8,128)(2,1)S(1)} %collective-permute-done.9.refs_3_), channel_id=1, source_target_pairs={{0,16},{1,9},{2,18},{3,11},{4,20},{5,13},{6,22},{7,15},{8,24},{9,1... | collective-permute-start | bytes 1671176 | tf_op jit(solution)/shard_map/ppermute | solution.py:30
  14.6 14.9 %collective-permute-start.10 = (bf16[136,2048]{1,0:T(8,128)(2,1)S(1)}, bf16[136,2048]{1,0:T(8,128)(2,1)S(1)}, u32[]{:S(2)}, u32[]{:S(2)}) collective-permute-start(bf16[136,2048]{1,0:T(8,128)(2,1)S(1)} %get-tuple-element.24.message_ref), channel_id=1, source_target_pairs={{0,16},{1,9},{2,18},{3,11},{4,20},{5,13},{6,22},{7,15},{8,24},{9,1... | collective-permute-start | bytes 1671176 | tf_op jit(solution)/shard_map/ppermute | solution.py:30
  14.6 28.6 %collective-permute-start.4 = (bf16[128,2048]{1,0:T(8,128)(2,1)}, bf16[128,2048]{1,0:T(8,128)(2,1)S(1)}, u32[]{:S(2)}, u32[]{:S(2)}) collective-permute-start(bf16[128,2048]{1,0:T(8,128)(2,1)} %refs_0_.1), channel_id=1, source_target_pairs={{0,4},{1,5},{2,6},{3,7},{4,0},{5,1},{6,2},{7,3},{8,12},{9,13},{10,... | collective-permute-start | bytes 1572872 | tf_op jit(solution)/shard_map/ppermute | solution.py:30
  22.1 11.8 %collective-permute-start.17 = (bf16[136,2048]{1,0:T(8,128)(2,1)S(1)}, bf16[136,2048]{1,0:T(8,128)(2,1)S(1)}, u32[]{:S(2)}, u32[]{:S(2)}) collective-permute-start(bf16[136,2048]{1,0:T(8,128)(2,1)S(1)} %collective-permute-done.16.refs_3_), channel_id=1, source_target_pairs={{0,1},{1,0},{2,3},{3,2},{4,5},{5,4},{6,7},{7,6},{8,9},{9,8},{10,11... | collective-permute-start | bytes 1671176 | tf_op jit(solution)/shard_map/ppermute | solution.py:30
  28.9 9.0 %collective-permute-start.12 = (bf16[136,2048]{1,0:T(8,128)(2,1)S(1)}, bf16[136,2048]{1,0:T(8,128)(2,1)S(1)}, u32[]{:S(2)}, u32[]{:S(2)}) collective-permute-start(bf16[136,2048]{1,0:T(8,128)(2,1)S(1)} %collective-permute-done.9.refs_3_), channel_id=1, source_target_pairs={{0,1},{1,0},{2,3},{3,2},{4,5},{5,4},{6,7},{7,6},{8,9},{9,8},{10,11... | collective-permute-start | bytes 1671176 | tf_op jit(solution)/shard_map/ppermute | solution.py:30
  29.5 8.4 %collective-permute-start.11 = (bf16[136,2048]{1,0:T(8,128)(2,1)S(1)}, bf16[136,2048]{1,0:T(8,128)(2,1)S(1)}, u32[]{:S(2)}, u32[]{:S(2)}) collective-permute-start(bf16[136,2048]{1,0:T(8,128)(2,1)S(1)} %collective-permute-done.10.refs_4_), channel_id=1, source_target_pairs={{0,1},{1,0},{2,3},{3,2},{4,5},{5,4},{6,7},{7,6},{8,9},{9,8},{10,11... | collective-permute-start | bytes 1671176 | tf_op jit(solution)/shard_map/ppermute | solution.py:30
  33.4 12.0 %collective-permute-start.13 = (bf16[128,2048]{1,0:T(8,128)(2,1)S(1)}, bf16[128,2048]{1,0:T(8,128)(2,1)S(1)}, u32[]{:S(2)}, u32[]{:S(2)}) collective-permute-start(bf16[128,2048]{1,0:T(8,128)(2,1)S(1)} %get-tuple-element.32), channel_id=1, source_target_pairs={{0,1},{1,0},{2,3},{3,2},{4,5},{5,4},{6,7},{7,6},{8,9},{9,8},{10,11... | collective-permute-start | bytes 1572872 | tf_op jit(solution)/shard_map/ppermute | solution.py:30
  37.8 7.6 %copy-start.1 = (bf16[128,2048]{1,0:T(8,128)(2,1)S(1)}, bf16[128,2048]{1,0:T(8,128)(2,1)}, u32[]{:S(2)}) copy-start(bf16[128,2048]{1,0:T(8,128)(2,1)} %refs_0_.1) | copy-start | bytes 1572868
  37.8 4.9 %collective-permute-start.18 = (bf16[128,2048]{1,0:T(8,128)(2,1)S(1)}, bf16[128,2048]{1,0:T(8,128)(2,1)S(1)}, u32[]{:S(2)}, u32[]{:S(2)}) collective-permute-start(bf16[128,2048]{1,0:T(8,128)(2,1)S(1)} %get-tuple-element.35), channel_id=1, source_target_pairs={{0,1},{1,0},{2,3},{3,2},{4,5},{5,4},{6,7},{7,6},{8,9},{9,8},{10,11... | collective-permute-start | bytes 1572872 | tf_op jit(solution)/shard_map/ppermute | solution.py:30
  42.0 23.2 %copy-start = (bf16[512,1024]{1,0:T(8,128)(2,1)S(1)}, bf16[512,1024]{1,0:T(8,128)(2,1)}, u32[]{:S(2)}) copy-start(bf16[512,1024]{1,0:T(8,128)(2,1)} %rows_ref.1) | copy-start | bytes 3145732
  42.0 23.2 %copy-start.2 = (bf16[4,256,256]{2,1,0:T(8,128)(2,1)S(1)}, bf16[4,256,256]{2,1,0:T(8,128)(2,1)}, u32[]{:S(2)}) copy-start(bf16[4,256,256]{2,1,0:T(8,128)(2,1)} %weight_ref.1) | copy-start | bytes 1572868
  42.0 23.1 %copy-start.5 = (f32[1024]{0:T(1024)S(1)}, f32[1024]{0:T(1024)}, u32[]{:S(2)}) copy-start(f32[1024]{0:T(1024)} %param.15) | copy-start | bytes 12292
  42.0 4.9 %collective-permute-start.14 = (bf16[128,2048]{1,0:T(8,128)(2,1)S(1)}, bf16[128,2048]{1,0:T(8,128)(2,1)S(1)}, u32[]{:S(2)}, u32[]{:S(2)}) collective-permute-start(bf16[128,2048]{1,0:T(8,128)(2,1)S(1)} %get-tuple-element.33), channel_id=1, source_target_pairs={{0,1},{1,0},{2,3},{3,2},{4,5},{5,4},{6,7},{7,6},{8,9},{9,8},{10,11... | collective-permute-start | bytes 1572872 | tf_op jit(solution)/shard_map/ppermute | solution.py:30
  42.5 10.0 %collective-permute-start.8 = (bf16[128,2048]{1,0:T(8,128)(2,1)S(1)}, bf16[128,2048]{1,0:T(8,128)(2,1)S(1)}, u32[]{:S(2)}, u32[]{:S(2)}) collective-permute-start(bf16[128,2048]{1,0:T(8,128)(2,1)S(1)} %get-tuple-element.26), channel_id=1, source_target_pairs={{0,1},{1,0},{2,3},{3,2},{4,5},{5,4},{6,7},{7,6},{8,9},{9,8},{10,11... | collective-permute-start | bytes 1572872 | tf_op jit(solution)/shard_map/ppermute | solution.py:30
  42.6 7.7 %collective-permute-start = (bf16[16,1024]{1,0:T(8,128)(2,1)S(1)}, bf16[16,1024]{1,0:T(8,128)(2,1)S(1)}, u32[]{:S(2)}, u32[]{:S(2)}) collective-permute-start(bf16[16,1024]{1,0:T(8,128)(2,1)S(1)} %get-tuple-element.23), channel_id=1, source_target_pairs={{0,1},{1,2},{2,3},{3,4},{4,5},{5,6},{6,7},{7,8},{8,9},{9,10},{10,1... | collective-permute-start | bytes 98312 | tf_op jit(solution)/shard_map/ppermute | solution.py:30
  43.3 7.5 %collective-permute-start.24 = (bf16[128,1024]{1,0:T(8,128)(2,1)S(1)}, bf16[128,1024]{1,0:T(8,128)(2,1)S(1)}, u32[]{:S(2)}, u32[]{:S(2)}) collective-permute-start(bf16[128,1024]{1,0:T(8,128)(2,1)S(1)} %get-tuple-element.44), channel_id=1, source_target_pairs={{0,8},{1,17},{2,10},{3,19},{4,12},{5,21},{6,14},{7,23},{8,0},{9,25... | collective-permute-start | bytes 786440 | tf_op jit(solution)/shard_map/ppermute | solution.py:30
  45.3 15.1 %collective-permute-start.2 = (bf16[128,2048]{1,0:T(8,128)(2,1)S(1)}, bf16[128,2048]{1,0:T(8,128)(2,1)S(1)}, u32[]{:S(2)}, u32[]{:S(2)}) collective-permute-start(bf16[128,2048]{1,0:T(8,128)(2,1)S(1)} %copy-done.1), channel_id=1, source_target_pairs={{0,2},{1,3},{2,0},{3,1},{4,6},{5,7},{6,4},{7,5},{8,10},{9,11},{10,... | collective-permute-start | bytes 1572872 | tf_op jit(solution)/shard_map/ppermute | solution.py:30
  46.9 24.7 %collective-permute-start.6 = (bf16[128,2048]{1,0:T(8,128)(2,1)S(1)}, bf16[128,2048]{1,0:T(8,128)(2,1)S(1)}, u32[]{:S(2)}, u32[]{:S(2)}) collective-permute-start(bf16[128,2048]{1,0:T(8,128)(2,1)S(1)} %collective-permute-done.4.refs_0_), channel_id=1, source_target_pairs={{0,2},{1,3},{2,0},{3,1},{4,6},{5,7},{6,4},{7,5},{8,10},{9,11},{10,... | collective-permute-start | bytes 1572872 | tf_op jit(solution)/shard_map/ppermute | solution.py:30
  50.4 21.4 %collective-permute-start.15 = (bf16[128,2048]{1,0:T(8,128)(2,1)S(1)}, bf16[128,2048]{1,0:T(8,128)(2,1)S(1)}, u32[]{:S(2)}, u32[]{:S(2)}) collective-permute-start(bf16[128,2048]{1,0:T(8,128)(2,1)S(1)} %join.2), channel_id=1, source_target_pairs={{0,8},{1,17},{2,10},{3,19},{4,12},{5,21},{6,14},{7,23},{8,0},{9,25... | collective-permute-start | bytes 1572872 | tf_op jit(solution)/shard_map/ppermute | solution.py:30
  50.8 14.4 %collective-permute-start.19 = (bf16[128,1024]{1,0:T(8,128)(2,1)S(1)}, bf16[128,1024]{1,0:T(8,128)(2,1)S(1)}, u32[]{:S(2)}, u32[]{:S(2)}) collective-permute-start(bf16[128,1024]{1,0:T(8,128)(2,1)S(1)} %get-tuple-element.45), channel_id=1, source_target_pairs={{0,8},{1,17},{2,10},{3,19},{4,12},{5,21},{6,14},{7,23},{8,0},{9,25... | collective-permute-start | bytes 786440 | tf_op jit(solution)/shard_map/ppermute | solution.py:30
  52.6 19.6 %collective-permute-start.25 = (bf16[128,1024]{1,0:T(8,128)(2,1)S(1)}, bf16[128,1024]{1,0:T(8,128)(2,1)S(1)}, u32[]{:S(2)}, u32[]{:S(2)}) collective-permute-start(bf16[128,1024]{1,0:T(8,128)(2,1)S(1)} %pass_on.3), channel_id=1, source_target_pairs={{0,16},{1,9},{2,18},{3,11},{4,20},{5,13},{6,22},{7,15},{8,24},{9,1... | collective-permute-start | bytes 786440 | tf_op jit(solution)/shard_map/ppermute | solution.py:30
  60.4 12.7 %collective-permute-start.1 = (bf16[128,2048]{1,0:T(8,128)(2,1)S(1)}, bf16[128,2048]{1,0:T(8,128)(2,1)S(1)}, u32[]{:S(2)}, u32[]{:S(2)}) collective-permute-start(bf16[128,2048]{1,0:T(8,128)(2,1)S(1)} %copy-done.1), channel_id=1, source_target_pairs={{0,1},{1,0},{2,3},{3,2},{4,5},{5,4},{6,7},{7,6},{8,9},{9,8},{10,11... | collective-permute-start | bytes 1572872 | tf_op jit(solution)/shard_map/ppermute | solution.py:30
  65.2 9.2 %collective-permute-start.3 = (bf16[128,2048]{1,0:T(8,128)(2,1)S(1)}, bf16[128,2048]{1,0:T(8,128)(2,1)S(1)}, u32[]{:S(2)}, u32[]{:S(2)}) collective-permute-start(bf16[128,2048]{1,0:T(8,128)(2,1)S(1)} %collective-permute-done.2.refs_2_), channel_id=1, source_target_pairs={{0,1},{1,0},{2,3},{3,2},{4,5},{5,4},{6,7},{7,6},{8,9},{9,8},{10,11... | collective-permute-start | bytes 1572872 | tf_op jit(solution)/shard_map/ppermute | solution.py:30
  71.7 9.9 %collective-permute-start.5 = (bf16[128,2048]{1,0:T(8,128)(2,1)S(1)}, bf16[128,2048]{1,0:T(8,128)(2,1)S(1)}, u32[]{:S(2)}, u32[]{:S(2)}) collective-permute-start(bf16[128,2048]{1,0:T(8,128)(2,1)S(1)} %collective-permute-done.4.refs_0_), channel_id=1, source_target_pairs={{0,1},{1,0},{2,3},{3,2},{4,5},{5,4},{6,7},{7,6},{8,9},{9,8},{10,11... | collective-permute-start | bytes 1572872 | tf_op jit(solution)/shard_map/ppermute | solution.py:30
  71.8 9.8 %collective-permute-start.7 = (bf16[128,2048]{1,0:T(8,128)(2,1)S(1)}, bf16[128,2048]{1,0:T(8,128)(2,1)S(1)}, u32[]{:S(2)}, u32[]{:S(2)}) collective-permute-start(bf16[128,2048]{1,0:T(8,128)(2,1)S(1)} %collective-permute-done.6.refs_2_), channel_id=1, source_target_pairs={{0,1},{1,0},{2,3},{3,2},{4,5},{5,4},{6,7},{7,6},{8,9},{9,8},{10,11... | collective-permute-start | bytes 1572872 | tf_op jit(solution)/shard_map/ppermute | solution.py:30
  72.2 6.4 %collective-permute-start.20 = (bf16[128,1024]{1,0:T(8,128)(2,1)S(1)}, bf16[128,1024]{1,0:T(8,128)(2,1)S(1)}, u32[]{:S(2)}, u32[]{:S(2)}) collective-permute-start(bf16[128,1024]{1,0:T(8,128)(2,1)S(1)} %pass_on.2), channel_id=1, source_target_pairs={{0,16},{1,9},{2,18},{3,11},{4,20},{5,13},{6,22},{7,15},{8,24},{9,1... | collective-permute-start | bytes 786440 | tf_op jit(solution)/shard_map/ppermute | solution.py:30
  73.1 12.9 %copy-start.4 = (f32[2048]{0:T(1024)S(1)}, f32[2048]{0:T(1024)}, u32[]{:S(2)}) copy-start(f32[2048]{0:T(1024)} %param.17) | copy-start | bytes 24580
  73.1 10.0 %collective-permute-start.26 = (bf16[32,1024]{1,0:T(8,128)(2,1)S(1)}, bf16[32,1024]{1,0:T(8,128)(2,1)S(1)}, u32[]{:S(2)}, u32[]{:S(2)}) collective-permute-start(bf16[32,1024]{1,0:T(8,128)(2,1)S(1)} %get-tuple-element.41), channel_id=1, source_target_pairs={{0,2},{1,3},{2,0},{3,1},{4,6},{5,7},{6,4},{7,5},{8,10},{9,11},{10,... | collective-permute-start | bytes 196616 | tf_op jit(solution)/shard_map/ppermute | solution.py:30
  75.8 13.4 %collective-permute-start.27 = (bf16[32,1024]{1,0:T(8,128)(2,1)S(1)}, bf16[32,1024]{1,0:T(8,128)(2,1)S(1)}, u32[]{:S(2)}, u32[]{:S(2)}) collective-permute-start(bf16[32,1024]{1,0:T(8,128)(2,1)S(1)} %get-tuple-element.42), channel_id=1, source_target_pairs={{0,4},{1,5},{2,6},{3,7},{4,0},{5,1},{6,2},{7,3},{8,12},{9,13},{10,... | collective-permute-start | bytes 196616 | tf_op jit(solution)/shard_map/ppermute | solution.py:30
  78.6 10.6 %collective-permute-start.28 = (bf16[32,1024]{1,0:T(8,128)(2,1)S(1)}, bf16[32,1024]{1,0:T(8,128)(2,1)S(1)}, u32[]{:S(2)}, u32[]{:S(2)}) collective-permute-start(bf16[32,1024]{1,0:T(8,128)(2,1)S(1)} %get-tuple-element.43), channel_id=1, source_target_pairs={{0,6},{1,7},{2,4},{3,5},{4,2},{5,3},{6,0},{7,1},{8,14},{9,15},{10,... | collective-permute-start | bytes 196616 | tf_op jit(solution)/shard_map/ppermute | solution.py:30
  81.6 7.6 %collective-permute-start.21 = (bf16[32,1024]{1,0:T(8,128)(2,1)S(1)}, bf16[32,1024]{1,0:T(8,128)(2,1)S(1)}, u32[]{:S(2)}, u32[]{:S(2)}) collective-permute-start(bf16[32,1024]{1,0:T(8,128)(2,1)S(1)} %get-tuple-element.37), channel_id=1, source_target_pairs={{0,2},{1,3},{2,0},{3,1},{4,6},{5,7},{6,4},{7,5},{8,10},{9,11},{10,... | collective-permute-start | bytes 196616 | tf_op jit(solution)/shard_map/ppermute | solution.py:30
  81.6 7.9 %collective-permute-start.22 = (bf16[32,1024]{1,0:T(8,128)(2,1)S(1)}, bf16[32,1024]{1,0:T(8,128)(2,1)S(1)}, u32[]{:S(2)}, u32[]{:S(2)}) collective-permute-start(bf16[32,1024]{1,0:T(8,128)(2,1)S(1)} %get-tuple-element.38), channel_id=1, source_target_pairs={{0,4},{1,5},{2,6},{3,7},{4,0},{5,1},{6,2},{7,3},{8,12},{9,13},{10,... | collective-permute-start | bytes 196616 | tf_op jit(solution)/shard_map/ppermute | solution.py:30
  83.1 6.4 %collective-permute-start.23 = (bf16[32,1024]{1,0:T(8,128)(2,1)S(1)}, bf16[32,1024]{1,0:T(8,128)(2,1)S(1)}, u32[]{:S(2)}, u32[]{:S(2)}) collective-permute-start(bf16[32,1024]{1,0:T(8,128)(2,1)S(1)} %get-tuple-element.39), channel_id=1, source_target_pairs={{0,6},{1,7},{2,4},{3,5},{4,2},{5,3},{6,0},{7,1},{8,14},{9,15},{10,... | collective-permute-start | bytes 196616 | tf_op jit(solution)/shard_map/ppermute | solution.py:30
  86.0 3.5 %copy-start.3 = (f32[2048]{0:T(1024)S(1)}, f32[2048]{0:T(1024)}, u32[]{:S(2)}) copy-start(f32[2048]{0:T(1024)} %param.25) | copy-start | bytes 24580

commit v6 on v5

--- a/solution.py
+++ b/solution.py
@@ -154,8 +154,8 @@
     )
 
 
-def store_halves(hidden, down_weight, total, core, outputs):
-    result = jnp.dot(hidden[...], down_weight[...], preferred_element_type=jnp.float32)
+def store_halves(hidden, down_weight, total, core, outputs, cols=slice(None)):
+    result = jnp.dot(hidden[...], down_weight[:, cols], preferred_element_type=jnp.float32)
     total[...] = result.astype(jnp.bfloat16).reshape(total.shape)
     groups = len(outputs) // 2
     chips = total.shape[0] // (CORES * groups)
@@ -297,49 +297,67 @@
     )(*from_hbm(gain.reshape(1, width), rows, gate_weight, up_weight, down_weight), message)
 
 
-def expert_kernel(gate_ref, up_ref, down_ref, *refs, groups):
-    inputs, outputs = refs[: 2 * groups], refs[2 * groups : 4 * groups]
-    normed, hidden, total = refs[4 * groups :]
+def far_kernel(
+    gate_ref, up_ref, down_ref, mine_ref, other_ref, hidden_ref, kept_ref, sent_ref, normed, total,
+    *, cols,
+):
     first, core = lax.axis_index("ep") * gate_ref.shape[0], seat()[1]
-    half = normed.shape[0] // (2 * groups)
-    for group in range(groups):
-        mine_ref, other_ref = inputs[2 * group : 2 * group + 2]
-        for source, which in ((mine_ref, core), (other_ref, 1 - core)):
-            start = pl.multiple_of((2 * group + which) * half, half)
-            normed[pl.ds(start, half), :] = source[:half, :]
+    half = normed.shape[0] // 2
+    for source, which in ((mine_ref, core), (other_ref, 1 - core)):
+        start = pl.multiple_of(which * half, half)
+        normed[pl.ds(start, half), :] = source[:half, :]
     for expert in range(gate_ref.shape[0]):
-        shares = [share_of(ref, first + expert, 2 * half) for ref in inputs[::2]]
-        scale = jnp.concatenate(shares, axis=0)
-        fill_hidden(hidden, expert, scale, normed, gate_ref.at[expert], up_ref.at[expert])
-    store_halves(hidden, down_ref, total, core, outputs)
-
-
-def expert_partial(chunks, gate_weight, up_weight, down_weight, block):
-    groups = len(chunks)
-    half, width = chunks[0][0].shape
+        scale = share_of(mine_ref, first + expert, 2 * half)
+        fill_hidden(hidden_ref, expert, scale, normed, gate_ref.at[expert], up_ref.at[expert])
+    store_halves(hidden_ref, down_ref, total, core, (kept_ref, sent_ref), cols)
+
+
+def far_partial(mine, other, gate_weight, up_weight, down_weight, block, cols):
+    half, width = mine.shape
     half -= 8
-    rows = 2 * half * groups
+    rows, span = 2 * half, cols.stop - cols.start
     local, _, units = gate_weight.shape
-    inputs = [array for chunk in chunks for array in chunk]
-    outputs = pl.pallas_call(
-        lambda *refs: expert_kernel(*refs, groups=groups),
-        in_specs=[VMEM] * (3 + len(inputs)),
-        out_specs=[VMEM] * (2 * groups),
-        out_shape=[jax.ShapeDtypeStruct((half, width), jnp.bfloat16)] * (2 * groups),
+    part = jax.ShapeDtypeStruct((half, span), jnp.bfloat16)
+    return pl.pallas_call(
+        lambda *refs: far_kernel(*refs, cols=cols),
+        in_specs=[VMEM] * 5,
+        out_specs=[VMEM] * 3,
+        out_shape=[pltpu.VMEM((rows, local * units), jnp.bfloat16), part, part],
         scratch_shapes=[
             pltpu.VMEM((rows, width), jnp.bfloat16),
-            pltpu.VMEM((rows, local * units), jnp.bfloat16),
-            pltpu.VMEM((rows // block, block, width), jnp.bfloat16),
+            pltpu.VMEM((rows // block, block, span), jnp.bfloat16),
         ],
-        compiler_params=pltpu.CompilerParams(vmem_limit_bytes=16 << 20),
+        compiler_params=pltpu.CompilerParams(vmem_limit_bytes=12 << 20),
         cost_estimate=pl.CostEstimate(
-            flops=6 * rows * width * local * units,
+            flops=5 * rows * width * local * units,
             bytes_accessed=4 * rows * width,
             transcendentals=rows * local * units,
         ),
-        name="experts",
-    )(gate_weight, up_weight, down_weight, *inputs)
-    return [(outputs[2 * g], outputs[2 * g + 1]) for g in range(groups)]
+        name="far",
+    )(gate_weight, up_weight, down_weight, mine, other)
+
+
+def down_kernel(hidden_ref, down_ref, kept_ref, sent_ref, total, *, cols):
+    store_halves(hidden_ref, down_ref, total, seat()[1], (kept_ref, sent_ref), cols)
+
+
+def down_partial(hidden, down_weight, block, cols):
+    rows, span = hidden.shape[0], cols.stop - cols.start
+    part = jax.ShapeDtypeStruct((rows // 2, span), jnp.bfloat16)
+    return pl.pallas_call(
+        lambda *refs: down_kernel(*refs, cols=cols),
+        in_specs=[VMEM] * 2,
+        out_specs=[VMEM] * 2,
+        out_shape=[part, part],
+        scratch_shapes=[pltpu.VMEM((rows // block, block, span), jnp.bfloat16)],
+        compiler_params=pltpu.CompilerParams(vmem_limit_bytes=8 << 20),
+        cost_estimate=pl.CostEstimate(
+            flops=2 * rows * span * hidden.shape[1],
+            bytes_accessed=4 * rows * span,
+            transcendentals=0,
+        ),
+        name="down",
+    )(hidden, down_weight)
 
 
 def half_kernel(gate_ref, up_ref, down_ref, *refs, rest):
@@ -506,11 +524,14 @@
     joined_a = join_halves(*halves, 0)
     joined_b = join_halves(*halves, 1)
     near_sum = to_group(joined_a, 0)
-    ((kept_c, sent_c),) = expert_partial([(from_c, other_c)], *weights)
-    back_c = to_core(sent_c)
-    cut = width * 8 // 16
+    cut = width // 2
     columns = [slice(0, cut), slice(cut, width)]
-    joined_c = [added(kept_c[:, part], back_c[:, part]) for part in columns]
+    hidden, *first_half = far_partial(from_c, other_c, *weights, columns[0])
+    second_half = down_partial(hidden, weights[2], block, columns[1])
+    joined_c = []
+    for kept_c, sent_c in (first_half, second_half):
+        back_c = to_core(sent_c)
+        joined_c.append(pass_on(kept_c, back_c, 0))
     passed, late = [], []
     for piece in range(PIECES):
         passing = to_group(joined_c[piece], 0)

time: 90.6 us -> 94.1 us (1.039)
  waiting for transfers between devices: 32 us -> 40.3 us
  starting transfers between devices: 30.1 us -> 25.2 us
    ppermute x29 -> x30, waiting for transfers between devices: 32 us -> 40.3 us  [moved(): return lax.ppermute(block, ('ep', 'tp'), route)]
    ppermute x29 -> x30, starting transfers between devices: 30.1 us -> 25.2 us  [moved(): return lax.ppermute(block, ('ep', 'tp'), route)]
    pallas_call x1 -> x2, Pallas kernels: 3.86 us -> 4.23 us  [the longest x1 3.4 us: far_partial(): pl.pallas_call(lambda *refs: far_kernel(*refs, cols=cols), in_specs=[VMEM...]
  transfers between devices with their start and end apart: 29 -> 30, of which waited for: 8 -> 9; matrix products, arithmetic and copies ran while one was open for 0% -> 0% of each run, Pallas kernels for 27% -> 27%
where the time goes in v6:
time: 94.1 us; the launch traced here: 93.9 us
  waiting for transfers between devices  40.3 us (43%)
  Pallas kernels  27.3 us (29%)
  starting transfers between devices  25.2 us (27%)
    ppermute x30, waiting for transfers between devices, moved(): return lax.ppermute(block, ('ep', 'tp'), route)  40.3 us
    ppermute x30, starting transfers between devices, moved(): return lax.ppermute(block, ('ep', 'tp'), route)  25.2 us
    pallas_call x2, Pallas kernels, half_partial(): pl.pallas_call(lambda *refs: half_kernel(*refs, rest=rest), in_specs=[VME...  7.65 us
    pallas_call x1, Pallas kernels, own_partial(): pl.pallas_call(own_kernel, in_specs=[HBM] * 5 + [VMEM], out_specs=[VMEM]...  6.81 us
    pallas_call x1, Pallas kernels, far_partial(): pl.pallas_call(lambda *refs: far_kernel(*refs, cols=cols), in_specs=[VMEM...  3.4 us
    pallas_call x1, Pallas kernels, project(): pl.pallas_call(project_kernel, grid=(rows // tile,), in_specs=[VMEM] * (3...  3.16 us
  transfers between devices with their start and end apart: 30, of which 9 were waited for; matrix products, arithmetic and copies ran while one was open for 0% of the time, Pallas kernels for 27%

profile of v6, /device:TPU:0, one launch (start us, length us, event | category | flops | bytes accessed | tf_op | source)
XLA Modules:
  0.0 93.9 jit_solution(2754589221226741275)
XLA Ops:
  0.6 1.4 %pack.1 = (bf16[136,2048]{1,0:T(8,128)(2,1)S(1)}, bf16[16,1024]{1,0:T(8,128)(2,1)S(1)}) custom-call(bf16[256,2048]{1,0:T(8,128)(2,1)} %rows_in.3, f32[1,2048]{1,0:T(1,128)} %bitcast.18, s32[4,256]{1,0:T(4,128)} %bitcast.20, f32[4,256]{1,0:T(4,128)} %bitcast.21, bf16[512,1024]{1,0:T(8,128)(2,1)} %rows_ref.1), custom_call_target="tpu_custom_call" | custom-call | tf_op jit(solution)/shard_map/pack/pallas_call | solution.py:223
  2.0 3.0 %collective-permute-start.9 = (bf16[136,2048]{1,0:T(8,128)(2,1)S(1)}, bf16[136,2048]{1,0:T(8,128)(2,1)S(1)}, u32[]{:S(2)}, u32[]{:S(2)}) collective-permute-start(bf16[136,2048]{1,0:T(8,128)(2,1)S(1)} %get-tuple-element.27.message_ref), channel_id=1, source_target_pairs={{0,8},{1,17},{2,10},{3,19},{4,12},{5,21},{6,14},{7,23},{8,0},{9,25... | collective-permute-start | bytes 1671176 | tf_op jit(solution)/shard_map/ppermute | solution.py:30
  5.0 1.5 %collective-permute-start.10 = (bf16[136,2048]{1,0:T(8,128)(2,1)S(1)}, bf16[136,2048]{1,0:T(8,128)(2,1)S(1)}, u32[]{:S(2)}, u32[]{:S(2)}) collective-permute-start(bf16[136,2048]{1,0:T(8,128)(2,1)S(1)} %get-tuple-element.27.message_ref), channel_id=1, source_target_pairs={{0,16},{1,9},{2,18},{3,11},{4,20},{5,13},{6,22},{7,15},{8,24},{9,1... | collective-permute-start | bytes 1671176 | tf_op jit(solution)/shard_map/ppermute | solution.py:30
  6.6 11.4 %collective-permute-done.9.refs_3_ = bf16[136,2048]{1,0:T(8,128)(2,1)S(1)} collective-permute-done((bf16[136,2048]{1,0:T(8,128)(2,1)S(1)}, bf16[136,2048]{1,0:T(8,128)(2,1)S(1)}, u32[]{:S(2)}, u32[]{:S(2)}) %collective-permute-start.9) | collective-permute-done | bytes 557088 | tf_op jit(solution)/shard_map/ppermute | solution.py:30
  17.9 1.6 %collective-permute-start.16 = (bf16[136,2048]{1,0:T(8,128)(2,1)S(1)}, bf16[136,2048]{1,0:T(8,128)(2,1)S(1)}, u32[]{:S(2)}, u32[]{:S(2)}) collective-permute-start(bf16[136,2048]{1,0:T(8,128)(2,1)S(1)} %collective-permute-done.9.refs_3_), channel_id=1, source_target_pairs={{0,16},{1,9},{2,18},{3,11},{4,20},{5,13},{6,22},{7,15},{8,24},{9,1... | collective-permute-start | bytes 1671176 | tf_op jit(solution)/shard_map/ppermute | solution.py:30
  19.5 2.7 %collective-permute-start.4 = (bf16[128,2048]{1,0:T(8,128)(2,1)}, bf16[128,2048]{1,0:T(8,128)(2,1)S(1)}, u32[]{:S(2)}, u32[]{:S(2)}) collective-permute-start(bf16[128,2048]{1,0:T(8,128)(2,1)} %refs_0_.1), channel_id=1, source_target_pairs={{0,4},{1,5},{2,6},{3,7},{4,0},{5,1},{6,2},{7,3},{8,12},{9,13},{10,... | collective-permute-start | bytes 1572872 | tf_op jit(solution)/shard_map/ppermute | solution.py:30
  22.2 0.5 collective-permute-start.11
  22.8 6.8 %own.1 = (bf16[128,2048]{1,0:T(8,128)(2,1)S(1)}, bf16[128,2048]{1,0:T(8,128)(2,1)S(1)}, bf16[2,2048,512]{2,1,0:T(8,128)(2,1)S(1)}, bf16[2,2048,512]{2,1,0:T(8,128)(2,1)S(1)}, bf16[1024,2048]{1,0:T(8,128)(2,1)S(1)}) custom-call(f32[1,2048]{1,0:T(1,128)} %bitcast.19, bf16[256,2048]{1,0:T(8,128)(2,1)} %rows_in.3, bf16[2,2048,512]{2,1,0:T(8,128)(2,1)} %gate_in.1, ...), custom_call_target="tpu_custom_call" | custom-call | flops 3221225472 | bytes 14680064 | tf_op jit(solution)/shard_map/own/pallas_call | solution.py:277
  29.6 0.1 collective-permute-start.17
  29.7 3.8 %halves.2 = (bf16[128,2048]{1,0:T(8,128)(2,1)S(1)}, bf16[128,2048]{1,0:T(8,128)(2,1)S(1)}) custom-call(bf16[2,2048,512]{2,1,0:T(8,128)(2,1)S(1)} %get-tuple-element.30.refs_0_, bf16[2,2048,512]{2,1,0:T(8,128)(2,1)S(1)} %get-tuple-element.31.refs_1_, bf16[1024,2048]{1,0:T(8,128)(2,1)S(1)} %get-tuple-element.32.refs_2_.refs_1_, ...), custom_call_target="tpu_custom_call" | custom-call | flops 3221225472 | bytes 2097152 | tf_op jit(solution)/shard_map/halves/pallas_call | solution.py:390
  33.4 0.6 collective-permute-start.13
  34.0 3.9 %halves.3 = (bf16[128,2048]{1,0:T(8,128)(2,1)S(1)}, bf16[128,2048]{1,0:T(8,128)(2,1)S(1)}) custom-call(bf16[2,2048,512]{2,1,0:T(8,128)(2,1)S(1)} %get-tuple-element.30.refs_0_, bf16[2,2048,512]{2,1,0:T(8,128)(2,1)S(1)} %get-tuple-element.31.refs_1_, bf16[1024,2048]{1,0:T(8,128)(2,1)S(1)} %get-tuple-element.32.refs_2_.refs_1_, ...), custom_call_target="tpu_custom_call" | custom-call | flops 3221225472 | bytes 2097152 | tf_op jit(solution)/shard_map/halves/pallas_call | solution.py:390
  37.9 0.1 collective-permute-start.14
  38.0 3.4 %far.1 = (bf16[256,1024]{1,0:T(8,128)(2,1)S(1)}, bf16[128,1024]{1,0:T(8,128)(2,1)S(1)}, bf16[128,1024]{1,0:T(8,128)(2,1)S(1)}) custom-call(bf16[2,2048,512]{2,1,0:T(8,128)(2,1)S(1)} %get-tuple-element.30.refs_0_, bf16[2,2048,512]{2,1,0:T(8,128)(2,1)S(1)} %get-tuple-element.31.refs_1_, bf16[1024,2048]{1,0:T(8,128)(2,1)S(1)} %get-tuple-element.32.refs_2_.refs_1_, ...), custom_call_target="tpu_custom_call" | custom-call | flops 2684354560 | bytes 2097152 | tf_op jit(solution)/shard_map/far/pallas_call | solution.py:321
  41.4 0.8 down.1
  42.3 0.5 collective-permute-start.24
  42.9 0.1 collective-permute-start
  42.9 6.9 %collective-permute-done.rim_ref = bf16[16,1024]{1,0:T(8,128)(2,1)S(1)} collective-permute-done((bf16[16,1024]{1,0:T(8,128)(2,1)S(1)}, bf16[16,1024]{1,0:T(8,128)(2,1)S(1)}, u32[]{:S(2)}, u32[]{:S(2)}) %collective-permute-start) | collective-permute-done | bytes 32800 | tf_op jit(solution)/shard_map/ppermute | solution.py:30
  49.8 0.5 collective-permute-start.8
  50.4 0.1 collective-permute-start.2
  50.5 0.6 collective-permute-start.25
  51.1 0.1 join.2
  51.3 2.0 %collective-permute-start.6 = (bf16[128,2048]{1,0:T(8,128)(2,1)S(1)}, bf16[128,2048]{1,0:T(8,128)(2,1)S(1)}, u32[]{:S(2)}, u32[]{:S(2)}) collective-permute-start(bf16[128,2048]{1,0:T(8,128)(2,1)S(1)} %collective-permute-done.4.refs_0_), channel_id=1, source_target_pairs={{0,2},{1,3},{2,0},{3,1},{4,6},{5,7},{6,4},{7,5},{8,10},{9,11},{10,... | collective-permute-start | bytes 1572872 | tf_op jit(solution)/shard_map/ppermute | solution.py:30
  53.3 1.4 %collective-permute-start.15 = (bf16[128,2048]{1,0:T(8,128)(2,1)S(1)}, bf16[128,2048]{1,0:T(8,128)(2,1)S(1)}, u32[]{:S(2)}, u32[]{:S(2)}) collective-permute-start(bf16[128,2048]{1,0:T(8,128)(2,1)S(1)} %join.2), channel_id=1, source_target_pairs={{0,8},{1,17},{2,10},{3,19},{4,12},{5,21},{6,14},{7,23},{8,0},{9,25... | collective-permute-start | bytes 1572872 | tf_op jit(solution)/shard_map/ppermute | solution.py:30
  54.8 2.1 %collective-permute-done.25.refs_1_ = bf16[128,1024]{1,0:T(8,128)(2,1)S(1)} collective-permute-done((bf16[128,1024]{1,0:T(8,128)(2,1)S(1)}, bf16[128,1024]{1,0:T(8,128)(2,1)S(1)}, u32[]{:S(2)}, u32[]{:S(2)}) %collective-permute-start.25) | collective-permute-done | bytes 262176 | tf_op jit(solution)/shard_map/ppermute | solution.py:30
  56.9 0.6 collective-permute-start.19
  57.5 0.1 join.3.refs_0_
  57.7 1.4 %collective-permute-start.26 = (bf16[128,1024]{1,0:T(8,128)(2,1)S(1)}, bf16[128,1024]{1,0:T(8,128)(2,1)S(1)}, u32[]{:S(2)}, u32[]{:S(2)}) collective-permute-start(bf16[128,1024]{1,0:T(8,128)(2,1)S(1)} %pass_on.7), channel_id=1, source_target_pairs={{0,16},{1,9},{2,18},{3,11},{4,20},{5,13},{6,22},{7,15},{8,24},{9,1... | collective-permute-start | bytes 786440 | tf_op jit(solution)/shard_map/ppermute | solution.py:30
  59.1 6.2 %collective-permute-done.2.refs_2_ = bf16[128,2048]{1,0:T(8,128)(2,1)S(1)} collective-permute-done((bf16[128,2048]{1,0:T(8,128)(2,1)S(1)}, bf16[128,2048]{1,0:T(8,128)(2,1)S(1)}, u32[]{:S(2)}, u32[]{:S(2)}) %collective-permute-start.2) | collective-permute-done | bytes 524320 | tf_op jit(solution)/shard_map/ppermute | solution.py:30
  65.3 2.9 %collective-permute-done.19.refs_1_ = bf16[128,1024]{1,0:T(8,128)(2,1)S(1)} collective-permute-done((bf16[128,1024]{1,0:T(8,128)(2,1)S(1)}, bf16[128,1024]{1,0:T(8,128)(2,1)S(1)}, u32[]{:S(2)}, u32[]{:S(2)}) %collective-permute-start.19) | collective-permute-done | bytes 262176 | tf_op jit(solution)/shard_map/ppermute | solution.py:30
  68.2 1.2 %mix.1.mixed_ref = bf16[512,1024]{1,0:T(8,128)(2,1)S(1)} custom-call(bf16[16,1024]{1,0:T(8,128)(2,1)S(1)} %collective-permute-done.rim_ref, bf16[512,1024]{1,0:T(8,128)(2,1)S(1)} %copy-done, bf16[4,256,256]{2,1,0:T(8,128)(2,1)S(1)} %copy-done.2, f32[1,1024]{1,0:T(1,128)S(1)} %bitcast.16), custom_call_target="tpu_custom_call" | custom-call | flops 268435456 | bytes 2097152 | tf_op jit(solution)/shard_map/mix/pallas_call | solution.py:575
  69.4 0.1 pass_on.5
  69.5 6.1 %collective-permute-done.6.refs_2_ = bf16[128,2048]{1,0:T(8,128)(2,1)S(1)} collective-permute-done((bf16[128,2048]{1,0:T(8,128)(2,1)S(1)}, bf16[128,2048]{1,0:T(8,128)(2,1)S(1)}, u32[]{:S(2)}, u32[]{:S(2)}) %collective-permute-start.6) | collective-permute-done | bytes 524320 | tf_op jit(solution)/shard_map/ppermute | solution.py:30
  75.5 0.5 collective-permute-start.7
  76.0 1.3 %collective-permute-start.20 = (bf16[128,1024]{1,0:T(8,128)(2,1)S(1)}, bf16[128,1024]{1,0:T(8,128)(2,1)S(1)}, u32[]{:S(2)}, u32[]{:S(2)}) collective-permute-start(bf16[128,1024]{1,0:T(8,128)(2,1)S(1)} %pass_on.5), channel_id=1, source_target_pairs={{0,16},{1,9},{2,18},{3,11},{4,20},{5,13},{6,22},{7,15},{8,24},{9,1... | collective-permute-start | bytes 786440 | tf_op jit(solution)/shard_map/ppermute | solution.py:30
  77.4 0.2 convert_add_fusion
  77.7 0.4 collective-permute-start.27
  78.0 1.4 %near.1.near_ref = f32[512,2048]{1,0:T(8,128)S(1)} custom-call(bf16[512,1024]{1,0:T(8,128)(2,1)S(1)} %mix.1.mixed_ref, bf16[128,2048]{1,0:T(8,128)(2,1)S(1)} %copy-done.1, bf16[128,2048]{1,0:T(8,128)(2,1)S(1)} %collective-permute-done.1.refs_1_, bf16[128,2048]{1,0:T(8,128)(2,1)S(1)} %collective-permute-done.2.refs_2_, ...), custom_call_target="tpu_custom_call" | custom-call | flops 1073741824 | bytes 4194304 | tf_op jit(solution)/shard_map/near/pallas_call | solution.py:616
  79.4 0.1 collective-permute-start.28
  79.5 2.9 %collective-permute-done.20 = bf16[128,1024]{1,0:T(8,128)(2,1)S(1)} collective-permute-done((bf16[128,1024]{1,0:T(8,128)(2,1)S(1)}, bf16[128,1024]{1,0:T(8,128)(2,1)S(1)}, u32[]{:S(2)}, u32[]{:S(2)}) %collective-permute-start.20) | collective-permute-done | bytes 262176 | tf_op jit(solution)/shard_map/ppermute | solution.py:30
  82.4 1.2 %collective-permute-start.29 = (bf16[32,1024]{1,0:T(8,128)(2,1)S(1)}, bf16[32,1024]{1,0:T(8,128)(2,1)S(1)}, u32[]{:S(2)}, u32[]{:S(2)}) collective-permute-start(bf16[32,1024]{1,0:T(8,128)(2,1)S(1)} %get-tuple-element.49), channel_id=1, source_target_pairs={{0,6},{1,7},{2,4},{3,5},{4,2},{5,3},{6,0},{7,1},{8,14},{9,15},{10,... | collective-permute-start | bytes 196616 | tf_op jit(solution)/shard_map/ppermute | solution.py:30
  83.7 0.1 collective-permute-start.21
  83.7 3.2 %collective-permute-start.22 = (bf16[32,1024]{1,0:T(8,128)(2,1)S(1)}, bf16[32,1024]{1,0:T(8,128)(2,1)S(1)}, u32[]{:S(2)}, u32[]{:S(2)}) collective-permute-start(bf16[32,1024]{1,0:T(8,128)(2,1)S(1)} %get-tuple-element.41), channel_id=1, source_target_pairs={{0,4},{1,5},{2,6},{3,7},{4,0},{5,1},{6,2},{7,3},{8,12},{9,13},{10,... | collective-permute-start | bytes 196616 | tf_op jit(solution)/shard_map/ppermute | solution.py:30
  86.9 1.2 %collective-permute-start.23 = (bf16[32,1024]{1,0:T(8,128)(2,1)S(1)}, bf16[32,1024]{1,0:T(8,128)(2,1)S(1)}, u32[]{:S(2)}, u32[]{:S(2)}) collective-permute-start(bf16[32,1024]{1,0:T(8,128)(2,1)S(1)} %get-tuple-element.42), channel_id=1, source_target_pairs={{0,6},{1,7},{2,4},{3,5},{4,2},{5,3},{6,0},{7,1},{8,14},{9,15},{10,... | collective-permute-start | bytes 196616 | tf_op jit(solution)/shard_map/ppermute | solution.py:30
  88.1 3.2 %project.1 = bf16[512,2048]{1,0:T(8,128)(2,1)} custom-call(bf16[512,1024]{1,0:T(8,128)(2,1)S(1)} %mix.1.mixed_ref, f32[512,2048]{1,0:T(8,128)S(1)} %near.1.near_ref, f32[1,2048]{1,0:T(1,128)S(1)} %bitcast.15, bf16[128,2048]{1,0:T(8,128)(2,1)S(1)} %collective-permute-done.4.refs_0_, bf16[128,2048]{1,0:T(8,128)(2,1)S(1)} %collective-permute-done.5.refs_1_, ...), custom_call_target="tpu_custom_call" | custom-call | flops 1073741824 | bytes 6291456 | tf_op jit(solution)/shard_map/project/pallas_call | solution.py:654
  91.3 1.1 %collective-permute-done.22.refs_2_ = bf16[32,1024]{1,0:T(8,128)(2,1)S(1)} collective-permute-done((bf16[32,1024]{1,0:T(8,128)(2,1)S(1)}, bf16[32,1024]{1,0:T(8,128)(2,1)S(1)}, u32[]{:S(2)}, u32[]{:S(2)}) %collective-permute-start.22) | collective-permute-done | bytes 65568 | tf_op jit(solution)/shard_map/ppermute | solution.py:30
  92.4 0.7 collective-permute-done.23.refs_3_
  93.1 0.8 finish.1
  (43 shorter events, 0.4 us)
Async XLA Ops:
  2.0 15.9 %collective-permute-start.9 = (bf16[136,2048]{1,0:T(8,128)(2,1)S(1)}, bf16[136,2048]{1,0:T(8,128)(2,1)S(1)}, u32[]{:S(2)}, u32[]{:S(2)}) collective-permute-start(bf16[136,2048]{1,0:T(8,128)(2,1)S(1)} %get-tuple-element.27.message_ref), channel_id=1, source_target_pairs={{0,8},{1,17},{2,10},{3,19},{4,12},{5,21},{6,14},{7,23},{8,0},{9,25... | collective-permute-start | bytes 1671176 | tf_op jit(solution)/shard_map/ppermute | solution.py:30
  5.0 17.2 %collective-permute-start.10 = (bf16[136,2048]{1,0:T(8,128)(2,1)S(1)}, bf16[136,2048]{1,0:T(8,128)(2,1)S(1)}, u32[]{:S(2)}, u32[]{:S(2)}) collective-permute-start(bf16[136,2048]{1,0:T(8,128)(2,1)S(1)} %get-tuple-element.27.message_ref), channel_id=1, source_target_pairs={{0,16},{1,9},{2,18},{3,11},{4,20},{5,13},{6,22},{7,15},{8,24},{9,1... | collective-permute-start | bytes 1671176 | tf_op jit(solution)/shard_map/ppermute | solution.py:30
  17.9 11.6 %collective-permute-start.16 = (bf16[136,2048]{1,0:T(8,128)(2,1)S(1)}, bf16[136,2048]{1,0:T(8,128)(2,1)S(1)}, u32[]{:S(2)}, u32[]{:S(2)}) collective-permute-start(bf16[136,2048]{1,0:T(8,128)(2,1)S(1)} %collective-permute-done.9.refs_3_), channel_id=1, source_target_pairs={{0,16},{1,9},{2,18},{3,11},{4,20},{5,13},{6,22},{7,15},{8,24},{9,1... | collective-permute-start | bytes 1671176 | tf_op jit(solution)/shard_map/ppermute | solution.py:30
  19.5 31.7 %collective-permute-start.4 = (bf16[128,2048]{1,0:T(8,128)(2,1)}, bf16[128,2048]{1,0:T(8,128)(2,1)S(1)}, u32[]{:S(2)}, u32[]{:S(2)}) collective-permute-start(bf16[128,2048]{1,0:T(8,128)(2,1)} %refs_0_.1), channel_id=1, source_target_pairs={{0,4},{1,5},{2,6},{3,7},{4,0},{5,1},{6,2},{7,3},{8,12},{9,13},{10,... | collective-permute-start | bytes 1572872 | tf_op jit(solution)/shard_map/ppermute | solution.py:30
  22.2 11.8 %collective-permute-start.12 = (bf16[136,2048]{1,0:T(8,128)(2,1)S(1)}, bf16[136,2048]{1,0:T(8,128)(2,1)S(1)}, u32[]{:S(2)}, u32[]{:S(2)}) collective-permute-start(bf16[136,2048]{1,0:T(8,128)(2,1)S(1)} %collective-permute-done.9.refs_3_), channel_id=1, source_target_pairs={{0,1},{1,0},{2,3},{3,2},{4,5},{5,4},{6,7},{7,6},{8,9},{9,8},{10,11... | collective-permute-start | bytes 1671176 | tf_op jit(solution)/shard_map/ppermute | solution.py:30
  22.2 11.8 %collective-permute-start.11 = (bf16[136,2048]{1,0:T(8,128)(2,1)S(1)}, bf16[136,2048]{1,0:T(8,128)(2,1)S(1)}, u32[]{:S(2)}, u32[]{:S(2)}) collective-permute-start(bf16[136,2048]{1,0:T(8,128)(2,1)S(1)} %collective-permute-done.10.refs_4_), channel_id=1, source_target_pairs={{0,1},{1,0},{2,3},{3,2},{4,5},{5,4},{6,7},{7,6},{8,9},{9,8},{10,11... | collective-permute-start | bytes 1671176 | tf_op jit(solution)/shard_map/ppermute | solution.py:30
  29.6 8.4 %collective-permute-start.17 = (bf16[136,2048]{1,0:T(8,128)(2,1)S(1)}, bf16[136,2048]{1,0:T(8,128)(2,1)S(1)}, u32[]{:S(2)}, u32[]{:S(2)}) collective-permute-start(bf16[136,2048]{1,0:T(8,128)(2,1)S(1)} %collective-permute-done.16.refs_3_), channel_id=1, source_target_pairs={{0,1},{1,0},{2,3},{3,2},{4,5},{5,4},{6,7},{7,6},{8,9},{9,8},{10,11... | collective-permute-start | bytes 1671176 | tf_op jit(solution)/shard_map/ppermute | solution.py:30
  33.4 16.9 %collective-permute-start.13 = (bf16[128,2048]{1,0:T(8,128)(2,1)S(1)}, bf16[128,2048]{1,0:T(8,128)(2,1)S(1)}, u32[]{:S(2)}, u32[]{:S(2)}) collective-permute-start(bf16[128,2048]{1,0:T(8,128)(2,1)S(1)} %get-tuple-element.35), channel_id=1, source_target_pairs={{0,1},{1,0},{2,3},{3,2},{4,5},{5,4},{6,7},{7,6},{8,9},{9,8},{10,11... | collective-permute-start | bytes 1572872 | tf_op jit(solution)/shard_map/ppermute | solution.py:30
  37.9 12.6 %collective-permute-start.14 = (bf16[128,2048]{1,0:T(8,128)(2,1)S(1)}, bf16[128,2048]{1,0:T(8,128)(2,1)S(1)}, u32[]{:S(2)}, u32[]{:S(2)}) collective-permute-start(bf16[128,2048]{1,0:T(8,128)(2,1)S(1)} %get-tuple-element.36), channel_id=1, source_target_pairs={{0,1},{1,0},{2,3},{3,2},{4,5},{5,4},{6,7},{7,6},{8,9},{9,8},{10,11... | collective-permute-start | bytes 1572872 | tf_op jit(solution)/shard_map/ppermute | solution.py:30
  41.4 9.0 %copy-start.1 = (bf16[128,2048]{1,0:T(8,128)(2,1)S(1)}, bf16[128,2048]{1,0:T(8,128)(2,1)}, u32[]{:S(2)}) copy-start(bf16[128,2048]{1,0:T(8,128)(2,1)} %refs_0_.1) | copy-start | bytes 1572868
  42.3 25.9 %copy-start = (bf16[512,1024]{1,0:T(8,128)(2,1)S(1)}, bf16[512,1024]{1,0:T(8,128)(2,1)}, u32[]{:S(2)}) copy-start(bf16[512,1024]{1,0:T(8,128)(2,1)} %rows_ref.1) | copy-start | bytes 3145732
  42.3 25.9 %copy-start.2 = (bf16[4,256,256]{2,1,0:T(8,128)(2,1)S(1)}, bf16[4,256,256]{2,1,0:T(8,128)(2,1)}, u32[]{:S(2)}) copy-start(bf16[4,256,256]{2,1,0:T(8,128)(2,1)} %weight_ref.1) | copy-start | bytes 1572868
  42.3 25.9 %copy-start.5 = (f32[1024]{0:T(1024)S(1)}, f32[1024]{0:T(1024)}, u32[]{:S(2)}) copy-start(f32[1024]{0:T(1024)} %param.15) | copy-start | bytes 12292
  42.3 7.5 %collective-permute-start.24 = (bf16[128,1024]{1,0:T(8,128)(2,1)S(1)}, bf16[128,1024]{1,0:T(8,128)(2,1)S(1)}, u32[]{:S(2)}, u32[]{:S(2)}) collective-permute-start(bf16[128,1024]{1,0:T(8,128)(2,1)S(1)} %get-tuple-element.45), channel_id=1, source_target_pairs={{0,1},{1,0},{2,3},{3,2},{4,5},{5,4},{6,7},{7,6},{8,9},{9,8},{10,11... | collective-permute-start | bytes 786440 | tf_op jit(solution)/shard_map/ppermute | solution.py:30
  42.9 6.9 %collective-permute-start = (bf16[16,1024]{1,0:T(8,128)(2,1)S(1)}, bf16[16,1024]{1,0:T(8,128)(2,1)S(1)}, u32[]{:S(2)}, u32[]{:S(2)}) collective-permute-start(bf16[16,1024]{1,0:T(8,128)(2,1)S(1)} %get-tuple-element.26), channel_id=1, source_target_pairs={{0,1},{1,2},{2,3},{3,4},{4,5},{5,6},{6,7},{7,8},{8,9},{9,10},{10,1... | collective-permute-start | bytes 98312 | tf_op jit(solution)/shard_map/ppermute | solution.py:30
  49.8 3.5 %collective-permute-start.18 = (bf16[128,1024]{1,0:T(8,128)(2,1)S(1)}, bf16[128,1024]{1,0:T(8,128)(2,1)S(1)}, u32[]{:S(2)}, u32[]{:S(2)}) collective-permute-start(bf16[128,1024]{1,0:T(8,128)(2,1)S(1)} %get-tuple-element.38), channel_id=1, source_target_pairs={{0,1},{1,0},{2,3},{3,2},{4,5},{5,4},{6,7},{7,6},{8,9},{9,8},{10,11... | collective-permute-start | bytes 786440 | tf_op jit(solution)/shard_map/ppermute | solution.py:30
  49.8 7.9 %collective-permute-start.8 = (bf16[128,2048]{1,0:T(8,128)(2,1)S(1)}, bf16[128,2048]{1,0:T(8,128)(2,1)S(1)}, u32[]{:S(2)}, u32[]{:S(2)}) collective-permute-start(bf16[128,2048]{1,0:T(8,128)(2,1)S(1)} %get-tuple-element.29), channel_id=1, source_target_pairs={{0,1},{1,0},{2,3},{3,2},{4,5},{5,4},{6,7},{7,6},{8,9},{9,8},{10,11... | collective-permute-start | bytes 1572872 | tf_op jit(solution)/shard_map/ppermute | solution.py:30
  50.4 14.9 %collective-permute-start.2 = (bf16[128,2048]{1,0:T(8,128)(2,1)S(1)}, bf16[128,2048]{1,0:T(8,128)(2,1)S(1)}, u32[]{:S(2)}, u32[]{:S(2)}) collective-permute-start(bf16[128,2048]{1,0:T(8,128)(2,1)S(1)} %copy-done.1), channel_id=1, source_target_pairs={{0,2},{1,3},{2,0},{3,1},{4,6},{5,7},{6,4},{7,5},{8,10},{9,11},{10,... | collective-permute-start | bytes 1572872 | tf_op jit(solution)/shard_map/ppermute | solution.py:30
  50.5 6.4 %collective-permute-start.25 = (bf16[128,1024]{1,0:T(8,128)(2,1)S(1)}, bf16[128,1024]{1,0:T(8,128)(2,1)S(1)}, u32[]{:S(2)}, u32[]{:S(2)}) collective-permute-start(bf16[128,1024]{1,0:T(8,128)(2,1)S(1)} %pass_on.6), channel_id=1, source_target_pairs={{0,8},{1,17},{2,10},{3,19},{4,12},{5,21},{6,14},{7,23},{8,0},{9,25... | collective-permute-start | bytes 786440 | tf_op jit(solution)/shard_map/ppermute | solution.py:30
  51.3 24.3 %collective-permute-start.6 = (bf16[128,2048]{1,0:T(8,128)(2,1)S(1)}, bf16[128,2048]{1,0:T(8,128)(2,1)S(1)}, u32[]{:S(2)}, u32[]{:S(2)}) collective-permute-start(bf16[128,2048]{1,0:T(8,128)(2,1)S(1)} %collective-permute-done.4.refs_0_), channel_id=1, source_target_pairs={{0,2},{1,3},{2,0},{3,1},{4,6},{5,7},{6,4},{7,5},{8,10},{9,11},{10,... | collective-permute-start | bytes 1572872 | tf_op jit(solution)/shard_map/ppermute | solution.py:30
  53.3 22.3 %collective-permute-start.15 = (bf16[128,2048]{1,0:T(8,128)(2,1)S(1)}, bf16[128,2048]{1,0:T(8,128)(2,1)S(1)}, u32[]{:S(2)}, u32[]{:S(2)}) collective-permute-start(bf16[128,2048]{1,0:T(8,128)(2,1)S(1)} %join.2), channel_id=1, source_target_pairs={{0,8},{1,17},{2,10},{3,19},{4,12},{5,21},{6,14},{7,23},{8,0},{9,25... | collective-permute-start | bytes 1572872 | tf_op jit(solution)/shard_map/ppermute | solution.py:30
  56.9 11.2 %collective-permute-start.19 = (bf16[128,1024]{1,0:T(8,128)(2,1)S(1)}, bf16[128,1024]{1,0:T(8,128)(2,1)S(1)}, u32[]{:S(2)}, u32[]{:S(2)}) collective-permute-start(bf16[128,1024]{1,0:T(8,128)(2,1)S(1)} %pass_on.4), channel_id=1, source_target_pairs={{0,8},{1,17},{2,10},{3,19},{4,12},{5,21},{6,14},{7,23},{8,0},{9,25... | collective-permute-start | bytes 786440 | tf_op jit(solution)/shard_map/ppermute | solution.py:30
  57.7 18.3 %collective-permute-start.26 = (bf16[128,1024]{1,0:T(8,128)(2,1)S(1)}, bf16[128,1024]{1,0:T(8,128)(2,1)S(1)}, u32[]{:S(2)}, u32[]{:S(2)}) collective-permute-start(bf16[128,1024]{1,0:T(8,128)(2,1)S(1)} %pass_on.7), channel_id=1, source_target_pairs={{0,16},{1,9},{2,18},{3,11},{4,20},{5,13},{6,22},{7,15},{8,24},{9,1... | collective-permute-start | bytes 786440 | tf_op jit(solution)/shard_map/ppermute | solution.py:30
  65.3 12.4 %collective-permute-start.1 = (bf16[128,2048]{1,0:T(8,128)(2,1)S(1)}, bf16[128,2048]{1,0:T(8,128)(2,1)S(1)}, u32[]{:S(2)}, u32[]{:S(2)}) collective-permute-start(bf16[128,2048]{1,0:T(8,128)(2,1)S(1)} %copy-done.1), channel_id=1, source_target_pairs={{0,1},{1,0},{2,3},{3,2},{4,5},{5,4},{6,7},{7,6},{8,9},{9,8},{10,11... | collective-permute-start | bytes 1572872 | tf_op jit(solution)/shard_map/ppermute | solution.py:30
  68.2 9.9 %collective-permute-start.3 = (bf16[128,2048]{1,0:T(8,128)(2,1)S(1)}, bf16[128,2048]{1,0:T(8,128)(2,1)S(1)}, u32[]{:S(2)}, u32[]{:S(2)}) collective-permute-start(bf16[128,2048]{1,0:T(8,128)(2,1)S(1)} %collective-permute-done.2.refs_2_), channel_id=1, source_target_pairs={{0,1},{1,0},{2,3},{3,2},{4,5},{5,4},{6,7},{7,6},{8,9},{9,8},{10,11... | collective-permute-start | bytes 1572872 | tf_op jit(solution)/shard_map/ppermute | solution.py:30
  75.5 8.1 %collective-permute-start.5 = (bf16[128,2048]{1,0:T(8,128)(2,1)S(1)}, bf16[128,2048]{1,0:T(8,128)(2,1)S(1)}, u32[]{:S(2)}, u32[]{:S(2)}) collective-permute-start(bf16[128,2048]{1,0:T(8,128)(2,1)S(1)} %collective-permute-done.4.refs_0_), channel_id=1, source_target_pairs={{0,1},{1,0},{2,3},{3,2},{4,5},{5,4},{6,7},{7,6},{8,9},{9,8},{10,11... | collective-permute-start | bytes 1572872 | tf_op jit(solution)/shard_map/ppermute | solution.py:30
  75.5 8.2 %collective-permute-start.7 = (bf16[128,2048]{1,0:T(8,128)(2,1)S(1)}, bf16[128,2048]{1,0:T(8,128)(2,1)S(1)}, u32[]{:S(2)}, u32[]{:S(2)}) collective-permute-start(bf16[128,2048]{1,0:T(8,128)(2,1)S(1)} %collective-permute-done.6.refs_2_), channel_id=1, source_target_pairs={{0,1},{1,0},{2,3},{3,2},{4,5},{5,4},{6,7},{7,6},{8,9},{9,8},{10,11... | collective-permute-start | bytes 1572872 | tf_op jit(solution)/shard_map/ppermute | solution.py:30
  76.0 6.4 %collective-permute-start.20 = (bf16[128,1024]{1,0:T(8,128)(2,1)S(1)}, bf16[128,1024]{1,0:T(8,128)(2,1)S(1)}, u32[]{:S(2)}, u32[]{:S(2)}) collective-permute-start(bf16[128,1024]{1,0:T(8,128)(2,1)S(1)} %pass_on.5), channel_id=1, source_target_pairs={{0,16},{1,9},{2,18},{3,11},{4,20},{5,13},{6,22},{7,15},{8,24},{9,1... | collective-permute-start | bytes 786440 | tf_op jit(solution)/shard_map/ppermute | solution.py:30
  77.6 10.5 %copy-start.4 = (f32[2048]{0:T(1024)S(1)}, f32[2048]{0:T(1024)}, u32[]{:S(2)}) copy-start(f32[2048]{0:T(1024)} %param.17) | copy-start | bytes 24580
  77.7 9.3 %collective-permute-start.27 = (bf16[32,1024]{1,0:T(8,128)(2,1)S(1)}, bf16[32,1024]{1,0:T(8,128)(2,1)S(1)}, u32[]{:S(2)}, u32[]{:S(2)}) collective-permute-start(bf16[32,1024]{1,0:T(8,128)(2,1)S(1)} %get-tuple-element.47), channel_id=1, source_target_pairs={{0,2},{1,3},{2,0},{3,1},{4,6},{5,7},{6,4},{7,5},{8,10},{9,11},{10,... | collective-permute-start | bytes 196616 | tf_op jit(solution)/shard_map/ppermute | solution.py:30
  79.4 11.9 %collective-permute-start.28 = (bf16[32,1024]{1,0:T(8,128)(2,1)S(1)}, bf16[32,1024]{1,0:T(8,128)(2,1)S(1)}, u32[]{:S(2)}, u32[]{:S(2)}) collective-permute-start(bf16[32,1024]{1,0:T(8,128)(2,1)S(1)} %get-tuple-element.48), channel_id=1, source_target_pairs={{0,4},{1,5},{2,6},{3,7},{4,0},{5,1},{6,2},{7,3},{8,12},{9,13},{10,... | collective-permute-start | bytes 196616 | tf_op jit(solution)/shard_map/ppermute | solution.py:30
  82.4 8.9 %collective-permute-start.29 = (bf16[32,1024]{1,0:T(8,128)(2,1)S(1)}, bf16[32,1024]{1,0:T(8,128)(2,1)S(1)}, u32[]{:S(2)}, u32[]{:S(2)}) collective-permute-start(bf16[32,1024]{1,0:T(8,128)(2,1)S(1)} %get-tuple-element.49), channel_id=1, source_target_pairs={{0,6},{1,7},{2,4},{3,5},{4,2},{5,3},{6,0},{7,1},{8,14},{9,15},{10,... | collective-permute-start | bytes 196616 | tf_op jit(solution)/shard_map/ppermute | solution.py:30
  83.7 7.6 %collective-permute-start.21 = (bf16[32,1024]{1,0:T(8,128)(2,1)S(1)}, bf16[32,1024]{1,0:T(8,128)(2,1)S(1)}, u32[]{:S(2)}, u32[]{:S(2)}) collective-permute-start(bf16[32,1024]{1,0:T(8,128)(2,1)S(1)} %get-tuple-element.40), channel_id=1, source_target_pairs={{0,2},{1,3},{2,0},{3,1},{4,6},{5,7},{6,4},{7,5},{8,10},{9,11},{10,... | collective-permute-start | bytes 196616 | tf_op jit(solution)/shard_map/ppermute | solution.py:30
  83.7 8.6 %collective-permute-start.22 = (bf16[32,1024]{1,0:T(8,128)(2,1)S(1)}, bf16[32,1024]{1,0:T(8,128)(2,1)S(1)}, u32[]{:S(2)}, u32[]{:S(2)}) collective-permute-start(bf16[32,1024]{1,0:T(8,128)(2,1)S(1)} %get-tuple-element.41), channel_id=1, source_target_pairs={{0,4},{1,5},{2,6},{3,7},{4,0},{5,1},{6,2},{7,3},{8,12},{9,13},{10,... | collective-permute-start | bytes 196616 | tf_op jit(solution)/shard_map/ppermute | solution.py:30
  86.9 6.2 %collective-permute-start.23 = (bf16[32,1024]{1,0:T(8,128)(2,1)S(1)}, bf16[32,1024]{1,0:T(8,128)(2,1)S(1)}, u32[]{:S(2)}, u32[]{:S(2)}) collective-permute-start(bf16[32,1024]{1,0:T(8,128)(2,1)S(1)} %get-tuple-element.42), channel_id=1, source_target_pairs={{0,6},{1,7},{2,4},{3,5},{4,2},{5,3},{6,0},{7,1},{8,14},{9,15},{10,... | collective-permute-start | bytes 196616 | tf_op jit(solution)/shard_map/ppermute | solution.py:30
  88.1 5.0 %copy-start.3 = (f32[2048]{0:T(1024)S(1)}, f32[2048]{0:T(1024)}, u32[]{:S(2)}) copy-start(f32[2048]{0:T(1024)} %param.25) | copy-start | bytes 24580
